TPU v7x, 512 devices: a whole 4x8x8 slice. The times are simulated.
512 devices in a mesh: sp: 32 (over z, x), tp: 16 (over y, core).
Axes of the slice: x: 4, y: 8, z: 8, core: 2. Of those that a mesh axis runs over, the one named last changes fastest.
Arguments:
- mixer_out: bfloat16 [4096, 2048], P('sp'), may hold values from -6 to 6
- out_grad: bfloat16 [4096, 2048], P('sp'), may hold values from -2 to 2
- route_ids: int32 [4096, 2], P('sp'), may hold values from 0 to 31, all different within a row; in each aligned block of 128 rows (0 to 127, 128 to 255, ...) at most 16 rows name the same one
- route_weights: float32 [4096, 2], P('sp'), may hold values from 0.2 to 1.2
- gate_branch: bfloat16 [4096, 2048], P('sp', 'tp'), may hold values from -4 to 4
- states: float32 [4096, 2048], P('sp', 'tp'), may hold values from -6 to 6
- decay: float32 [4096, 2048], P('sp', 'tp'), may hold values from 0 to 1
- w_proj: bfloat16 [2048, 2048], P(None, 'tp'), may hold values from -0.125 to 0.125
- w_gate: bfloat16 [32, 2048, 2048], P('sp', 'tp'), may hold values from -0.125 to 0.125
- w_up: bfloat16 [32, 2048, 2048], P('sp', 'tp'), may hold values from -0.125 to 0.125
- w_down: bfloat16 [32, 2048, 2048], P('sp', 'tp'), may hold values from -0.125 to 0.125
Outputs:
- grad_w_gate: bfloat16 [32, 2048, 2048], P('sp', 'tp')
- grad_w_up: bfloat16 [32, 2048, 2048], P('sp', 'tp')
- grad_w_down: bfloat16 [32, 2048, 2048], P('sp', 'tp')
- grad_w_proj: float32 [2048, 2048], P('sp', 'tp')
- grad_branch: bfloat16 [4096, 2048], P('sp', 'tp')
- grad_drive: float32 [4096, 2048], P('sp', 'tp')
- grad_decay: float32 [4096, 2048], P('sp', 'tp')
Inputs may be any that keep to these rules, and one draw needn't show every extreme that they name: `route_ids`: each row names 2 different experts. In the rows of one index of sp no expert is named more than 16 times, a bound that some block reaches.
All inputs are finite; a program needn't handle non-finite values.
Results may differ from a plain program's by a relative error of at most 0.02.
Values may be sent and summed in bfloat16 or wider, within the bound.
No kernel may reach another device: no remote copies, remote signals or barrier semaphores. Data moves between devices by JAX's collectives and lax.ppermute only.
A program may use at most 64 MiB of HBM per device.

v0:
```python
import functools

import jax
import jax.numpy as jnp
from jax import lax
from jax.experimental import pallas as pl
from jax.experimental.pallas import tpu as pltpu
from jax.sharding import Mesh, PartitionSpec as P


SP = ("z", "x")
Y = ("yh", "yl")
TP = ("yh", "yl", "c")
F32, BF16 = jnp.float32, jnp.bfloat16


def nt(a, b):
    return lax.dot_general(a, b, (((1,), (1,)), ((), ())), preferred_element_type=F32)


def tn(a, b):
    return lax.dot_general(a, b, (((0,), (0,)), ((), ())), preferred_element_type=F32)


def nn(a, b):
    return jnp.dot(a, b, preferred_element_type=F32)


def copies(pairs, sems):
    started = [
        pltpu.make_async_copy(src, dst, sems.at[k]) for k, (src, dst) in enumerate(pairs)
    ]
    for copy in started:
        copy.start()
    return started


def move(pairs_of, out_shape, count, *args):
    def body(*refs):
        for copy in copies(pairs_of(*refs[:-1]), refs[-1]):
            copy.wait()

    anywhere = pl.BlockSpec(memory_space=pl.ANY)
    return pl.pallas_call(
        body,
        in_specs=[anywhere] * len(args),
        out_specs=[anywhere] * len(out_shape),
        out_shape=list(out_shape),
        scratch_shapes=[pltpu.SemaphoreType.DMA((count,))],
    )(*args)


def call(body, out_shape, place, *args, specs=None, outs_in=None, scratch=(), vmem=24 << 20):
    whole = lambda a: pl.BlockSpec(a.shape, lambda i, s, n=len(a.shape): (0,) * n)
    outs = out_shape if isinstance(out_shape, (list, tuple)) else [out_shape]
    in_specs = [whole(a) for a in args]
    out_specs = [whole(o) for o in outs]
    for k in specs or ():
        in_specs[k] = pl.BlockSpec(memory_space=pltpu.HBM)
    for k in outs_in or ():
        out_specs[k] = pl.BlockSpec(memory_space=pltpu.HBM)
    result = pl.pallas_call(
        body,
        grid_spec=pltpu.PrefetchScalarGridSpec(
            num_scalar_prefetch=1,
            grid=(1,),
            in_specs=in_specs,
            out_specs=out_specs,
            scratch_shapes=list(scratch),
        ),
        out_shape=list(outs),
        compiler_params=pltpu.CompilerParams(
            dimension_semantics=("arbitrary",), vmem_limit_bytes=vmem
        ),
    )(place, *args)
    return result if isinstance(out_shape, (list, tuple)) else result[0]


def dispatch_body(experts, cap, place, ids_h, wts_h, x_h, og_h, send_h, pick, ids, wts, x, og, send, sems):
    n, cols = x.shape
    half = cap // 2
    mine = pl.ds(pl.multiple_of(place[0] * cols, cols), cols)
    got = copies(
        ((ids_h, ids), (wts_h, wts), (x_h.at[:, mine], x), (og_h.at[:, mine], og)), sems
    )
    before = lax.broadcasted_iota(jnp.int32, (n, n), 0) < lax.broadcasted_iota(
        jnp.int32, (n, n), 1
    )
    before = jnp.where(before, 1.0, 0.0).astype(BF16)
    row = lax.broadcasted_iota(jnp.int32, (experts, n), 0)
    got[0].wait()
    got[1].wait()
    m0, m1 = ids[0:1, :] == row, ids[1:2, :] == row
    named = jnp.where(m0 | m1, 1.0, 0.0).astype(F32)
    wt = jnp.where(m0, wts[0:1, :], 0.0) + jnp.where(m1, wts[1:2, :], 0.0)
    position = nn(named.astype(BF16), before)
    position = jnp.where(named > 0.0, position, -1.0)
    slot = lax.broadcasted_iota(jnp.int32, (experts, half, n), 1).astype(F32)
    at = lambda first: jnp.where(position[:, None, :] == slot + first, 1.0, 0.0).astype(F32)
    pick[...] = (
        jnp.concatenate([at(0.0), at(float(half))], axis=1)
        .reshape(experts * cap, n)
        .astype(BF16)
    )
    hot = at((place[1] * half).astype(F32))
    scale = jnp.sum(hot * wt[:, None, :], axis=2, keepdims=True).reshape(experts * half, 1)
    hot = hot.reshape(experts * half, n).astype(BF16)
    got[2].wait()
    got[3].wait()
    steps, out = 2, []
    wide = cols // steps
    for k in range(steps):
        where = slice(k * wide, (k + 1) * wide)
        xs = nn(hot, x[:, where]).reshape(experts, 1, half, wide)
        cs = (nn(hot, og[:, where]) * scale).reshape(experts, 1, half, wide)
        send[:, where] = (
            jnp.concatenate([xs, cs], axis=1).reshape(experts * 2 * half, wide).astype(BF16)
        )
        copy = pltpu.make_async_copy(send.at[:, where], send_h.at[:, where], sems.at[4 + k])
        copy.start()
        out.append(copy)
    for copy in out:
        copy.wait()


def expert_body(half, place, own, par, g_s, u_s, d_s, psend, pkeep, mix):
    c = place[0]
    cols = own.shape[1]
    mine = pl.ds(pl.multiple_of(c * cols, cols), cols)
    other = pl.ds(pl.multiple_of((1 - c) * cols, cols), cols)
    units = g_s.shape[0]
    groups = own.shape[0] // (2 * half)

    def product(s, which):
        r = nt(own[...], s[:, mine]) + nt(par[...], s[:, other])
        return r.reshape(groups, 2, half, units)[:, which].reshape(groups * half, units)

    gate = product(g_s, 0)
    up = product(u_s, 0)
    grad = product(d_s, 1)
    sig = jax.nn.sigmoid(gate)
    silu = gate * sig
    hidden = silu * up
    up_grad = grad * silu
    gate_grad = grad * up * sig * (1.0 + gate * (1.0 - sig))
    gb, ub = gate_grad.astype(BF16), up_grad.astype(BF16)
    parts = psend.shape[0]
    width = cols // parts
    for ref, where in ((psend, other), (pkeep, mine)):
        p = nn(gb, g_s[:, where]) + nn(ub, u_s[:, where])
        for k in range(parts):
            ref[k] = p[:, k * width : (k + 1) * width].astype(ref.dtype)
    tile = lambda v: v.reshape(groups, 1, half, units)
    zero = jnp.zeros((groups, 1, half, units), F32)
    for k, pair in enumerate(
        ((tile(gate_grad), zero), (tile(up_grad), zero), (zero, tile(hidden)))
    ):
        v = jnp.concatenate(pair, axis=1).reshape(groups * 2 * half, units)
        mix[:, k * units : (k + 1) * units] = v.astype(BF16)


def weight_body(place, own, par, mix, gown, ga, gb):
    c = place[0]
    cols = own.shape[1]
    h, q = gown.shape[0] // 3, ga.shape[0] // 3
    units = h + 2 * q
    for src, start in ((own, c * cols), (par, (1 - c) * cols)):
        where = pl.ds(pl.multiple_of(start, cols), cols)
        for k in range(3):
            g = tn(mix[:, k * units : (k + 1) * units], src[...])
            gown[k * h : (k + 1) * h, where] = g[0:h]
            ga[k * q : (k + 1) * q, where] = g[h : h + q].astype(BF16)
            gb[k * q : (k + 1) * q, where] = g[h + q :].astype(BF16)


def fold_body(place, parts, out):
    members, _, ch = parts.shape
    dests, cap = out.shape[0], out.shape[1]
    both = []
    for low in range(2):
        total = parts[low].astype(F32)
        for m in range(low + 2, members, 2):
            total = total + parts[m].astype(F32)
        both.append(total.reshape(dests, cap // 2, ch))
    out[...] = jnp.concatenate(both, axis=1).astype(BF16)


def combine_body(place, pick, back, og_h, mid, og, sems):
    n = mid.shape[1]
    where = pl.ds(pl.multiple_of(place[3] * n, n), n)
    (copy,) = copies(((og_h.at[:, where], og),), sems)
    part = tn(pick[...], back[...])
    copy.wait()
    mid[...] = (og[...].astype(F32) + part).astype(BF16)


def split3(v):
    a = v.astype(BF16).astype(F32)
    b = (v - a).astype(BF16).astype(F32)
    return a, b, (v - a - b).astype(BF16).astype(F32)


def project_body(
    place, mid, w, gate_h, states_h, decay_h, out, branch, local, prod, gate, states, decay, sems
):
    got = copies(((gate_h, gate), (states_h, states), (decay_h, decay)), sems)
    pieces = mid.shape[0]
    ys = pieces // 2
    full = jnp.concatenate([mid[(b % ys) * 2 + b // ys] for b in range(pieces)], axis=1)
    act = nn(full, w[...])
    for copy in got:
        copy.wait()
    st, gt, dec = states[...], gate[...].astype(F32), decay[...]
    grad = tn(full, (gt * st).astype(BF16)).astype(BF16)
    dests, rows = out.shape[0], full.shape[1] // out.shape[0]
    branch[...] = (act * st).astype(BF16)
    n = st.shape[0]
    t = lax.broadcasted_iota(jnp.int32, st.shape, 0)
    ahead = lambda v, k, fill: jnp.where(t < n - k, pltpu.roll(v, n - k, 0), fill)
    b, a = act * gt, ahead(dec, 1, 1.0)
    k = 1
    while k < n:
        b, a = b + a * ahead(b, k, 0.0), a * ahead(a, k, 1.0)
        k *= 2
    local[...] = b
    prod[...] = a
    values = split3(dec[0:1] * b[0:1]) + split3(dec[0:1] * a[0:1])
    values = values + (None, None) + split3(st[n - 1 : n])
    tail = out.shape[1] - rows
    line = lax.broadcasted_iota(jnp.int32, (tail, st.shape[1]), 0)
    extra = jnp.zeros((tail, st.shape[1]), F32)
    for k, v in enumerate(values):
        if v is not None:
            extra = jnp.where(line == k, jnp.broadcast_to(v, extra.shape), extra)
    extra = extra.astype(BF16)
    for d in range(dests):
        out[d, 0:rows, :] = grad[d * rows : (d + 1) * rows]
        out[d, rows : rows + tail, :] = extra


def finish_body(place, got, local, prod, states, proj, drive, ddecay):
    rows = proj.shape[0]
    members = got.shape[0]
    s = place[2]
    total = got[0, 0:rows, :].astype(F32)
    for m in range(1, members):
        total = total + got[m, 0:rows, :].astype(F32)
    proj[...] = total
    carry = jnp.zeros((1, local.shape[1]), F32)
    before = jnp.zeros((1, local.shape[1]), F32)
    for m in range(members - 1, -1, -1):
        v = got[m, rows : rows + 16, :].astype(F32)
        later = m > s
        b = jnp.where(later, v[0:1] + v[1:2] + v[2:3], 0.0)
        a = jnp.where(later, v[3:4] + v[4:5] + v[5:6], 1.0)
        carry = b + a * carry
        before = jnp.where(m == s - 1, v[8:9] + v[9:10] + v[10:11], before)
    g = local[...] + prod[...] * carry
    drive[...] = g
    st = states[...]
    t = lax.broadcasted_iota(jnp.int32, st.shape, 0)
    previous = jnp.where(t == 0, jnp.broadcast_to(before, st.shape), pltpu.roll(st, 1, 0))
    ddecay[...] = g * previous


def local(
    sizes, mixer_out, out_grad, route_ids, route_weights, gate_branch, states, decay,
    w_proj, w_gate, w_up, w_down,
):
    n_sp, n_y = sizes
    tokens, width = mixer_out.shape
    ch = states.shape[1]
    hidden = w_gate.shape[1]
    cap = 2 * route_ids.shape[1] * tokens // n_sp
    half = cap // 2
    shape = jax.ShapeDtypeStruct
    c, yl, yh = lax.axis_index("c"), lax.axis_index("yl"), lax.axis_index("yh")
    place = jnp.stack([c, yl, lax.axis_index(SP), c * n_y + yh * 2 + yl]).astype(jnp.int32)
    ring = lambda k: [(i, (i + k) % n_y) for i in range(n_y)]
    swap = [(0, 1), (1, 0)]
    wg, wu, wd = w_gate[0], w_up[0], w_down[0]
    q = hidden // 2

    cols = width // 2
    small = pltpu.VMEM((2, tokens), jnp.int32), pltpu.VMEM((2, tokens), F32)
    block = pltpu.VMEM((tokens, cols), BF16)
    send, pick = call(
        functools.partial(dispatch_body, n_sp, cap),
        [shape((n_sp * cap, cols), BF16), shape((n_sp * cap, tokens), BF16)],
        place, route_ids.T, route_weights.T, mixer_out, out_grad,
        specs=(0, 1, 2, 3), outs_in=(0,),
        scratch=[
            *small, block, block,
            pltpu.VMEM((n_sp * cap, cols), BF16), pltpu.SemaphoreType.DMA((6,)),
        ],
    )
    own = lax.all_to_all(send.reshape(n_sp, cap, cols), SP, 0, 0, tiled=True)
    own = own.reshape(n_sp * cap, cols)

    def cut(*refs):
        w, (lo, hi) = refs[:3], refs[3:]
        return [
            (w[k].at[pl.ds(side * q, q)], to.at[pl.ds(k * q, q)])
            for side, to in enumerate((lo, hi))
            for k in range(3)
        ]

    w_lo, w_hi = move(cut, [shape((3 * q, width), BF16)] * 2, 6, wg, wu, wd)
    wa = lax.ppermute(w_lo, Y, ring(1))
    wb = lax.ppermute(w_hi, Y, ring(-1))
    par = lax.ppermute(own, "c", swap)

    units = hidden + 2 * q

    def joined(*refs):
        w, (lo, hi), to = refs[:3], refs[3:5], refs[5:]
        pairs = []
        for k in range(3):
            piece = pl.ds(k * q, q)
            pairs.append((w[k], to[k].at[pl.ds(0, hidden)]))
            pairs.append((lo.at[piece], to[k].at[pl.ds(hidden, q)]))
            pairs.append((hi.at[piece], to[k].at[pl.ds(hidden + q, q)]))
        return pairs

    weights = move(joined, [shape((units, width), BF16)] * 3, 9, wg, wu, wd, wa, wb)

    slots = n_sp * half
    wide = cols // n_y
    psend, pkeep, mix = call(
        functools.partial(expert_body, half),
        [
            shape((n_y, slots, wide), BF16),
            shape((n_y, slots, wide), F32),
            shape((n_sp * cap, 3 * units), BF16),
        ],
        place, own, par, *weights,
    )
    precv = lax.ppermute(psend, "c", swap)
    gown, ga, gb = call(
        weight_body,
        [shape((3 * hidden, width), F32), shape((3 * q, width), BF16), shape((3 * q, width), BF16)],
        place, own, par, mix,
    )
    back_lo = lax.ppermute(ga, Y, ring(-1))
    back_hi = lax.ppermute(gb, Y, ring(1))

    psum = (pkeep + precv.astype(F32)).astype(BF16)
    parts = lax.all_to_all(psum, Y, 0, 0, tiled=True)
    ret = call(fold_body, shape((n_sp, cap, wide), BF16), place, parts)
    back = lax.all_to_all(ret, SP, 0, 0, tiled=True)
    mid = call(
        combine_body,
        shape((tokens, ch), BF16),
        place, pick, back.reshape(n_sp * cap, wide), out_grad,
        specs=(2,),
        scratch=[pltpu.VMEM((tokens, ch), BF16), pltpu.SemaphoreType.DMA((1,))],
    )
    mid = lax.all_gather(mid, TP)

    rows = width // n_sp
    out, branch, loc, prod = call(
        project_body,
        [
            shape((n_sp, rows + 16, ch), BF16),
            shape((tokens, ch), BF16),
            shape((tokens, ch), F32),
            shape((tokens, ch), F32),
        ],
        place, mid, w_proj, gate_branch, states, decay,
        specs=(2, 3, 4),
        scratch=[
            pltpu.VMEM((tokens, ch), BF16), pltpu.VMEM((tokens, ch), F32),
            pltpu.VMEM((tokens, ch), F32), pltpu.SemaphoreType.DMA((3,)),
        ],
    )
    got = lax.all_to_all(out, SP, 0, 0, tiled=True)
    proj, drive, ddecay = call(
        finish_body,
        [shape((rows, ch), F32), shape((tokens, ch), F32), shape((tokens, ch), F32)],
        place, got, loc, prod, states,
    )

    def total(k):
        mine = gown[k * hidden : (k + 1) * hidden]
        other = jnp.concatenate(
            [back_lo[k * q : (k + 1) * q], back_hi[k * q : (k + 1) * q]], axis=0
        )
        return (mine + other.astype(F32)).astype(BF16)[None]

    return (total(0), total(1), total(2), proj, branch, drive, ddecay)


def solution(mesh):
    devices = mesh.devices
    n_sp, n_tp = devices.shape
    n_yh = n_tp // 4
    x = 4
    fine = Mesh(
        devices.reshape(n_sp // x, x, n_yh, 2, 2), ("z", "x", "yh", "yl", "c")
    )
    rows, both, weight = P(SP, None), P(SP, TP), P(SP, TP, None)
    return jax.shard_map(
        functools.partial(local, (n_sp, n_tp // 2)),
        mesh=fine,
        in_specs=(rows, rows, rows, rows, both, both, both, P(None, TP), weight, weight, weight),
        out_specs=(weight, weight, weight, both, both, both, both),
        check_vma=False,
    )
```

profile of v0, /device:TPU:8, one launch (start us, length us, event | category | flops | bytes accessed | tf_op | source)
XLA Modules:
  0.0 335.2 jit_solution(16348970464297476836)
XLA Ops:
  0.6 0.1 pad_add_fusion.place
  0.7 0.0 copy-start.2
  0.7 1.0 copy-done.2
  1.8 0.0 copy-start.11
  1.8 1.0 copy-done.11
  2.8 0.0 copy-start.15
  2.8 0.7 copy-done.15
  3.5 0.0 copy-start.16
  3.5 0.7 copy-done.16
  4.2 1.6 shard_map.162
  5.8 41.0 %all_to_all.20 = bf16[32,16,1024]{2,1,0:T(8,128)(2,1)S(1)} all-to-all(bf16[32,16,1024]{2,1,0:T(8,128)(2,1)S(1)} %bitcast.23), channel_id=1, replica_groups=mesh['z'=8,'x'=4,'yh'=4,'yl'=2,'c'=2] {'z','x'}, dimensions={0} | all-to-all | bytes 2097152 | tf_op jit(solution)/shard_map/all_to_all | solution.py:297
  46.8 1.9 collective-permute-start
  48.7 48.8 %shard_map.163 = (bf16[192,2048]{1,0:T(8,128)(2,1)}, bf16[192,2048]{1,0:T(8,128)(2,1)}) custom-call(bf16[128,2048]{1,0:T(8,128)(2,1)} %bitcast.27, bf16[128,2048]{1,0:T(8,128)(2,1)} %bitcast.29, bf16[128,2048]{1,0:T(8,128)(2,1)} %bitcast.31), custom_call_target="tpu_custom_call" | custom-call | tf_op jit(solution)/shard_map/pallas_call | solution.py:44
  97.5 3.5 %collective-permute-start.1 = (bf16[192,2048]{1,0:T(8,128)(2,1)}, bf16[192,2048]{1,0:T(8,128)(2,1)S(1)}, u32[]{:S(2)}, u32[]{:S(2)}) collective-permute-start(bf16[192,2048]{1,0:T(8,128)(2,1)} %get-tuple-element.28), channel_id=1, source_target_pairs={{0,2},{2,4},{4,6},{6,8},{8,10},{10,12},{12,14},{14,0},{1,3},{3,5},... | collective-permute-start | bytes 2359304 | tf_op jit(solution)/shard_map/ppermute | solution.py:309
  101.0 2.4 collective-permute-start.2
  103.4 16.2 %collective-permute-done.1.refs_3_ = bf16[192,2048]{1,0:T(8,128)(2,1)S(1)} collective-permute-done((bf16[192,2048]{1,0:T(8,128)(2,1)}, bf16[192,2048]{1,0:T(8,128)(2,1)S(1)}, u32[]{:S(2)}, u32[]{:S(2)}) %collective-permute-start.1) | collective-permute-done | bytes 786464 | tf_op jit(solution)/shard_map/ppermute | solution.py:309
  119.6 0.0 copy-start.18
  119.6 3.3 collective-permute-done.2.refs_4_
  122.9 0.0 copy-done.18
  122.9 96.5 %shard_map.164 = (bf16[256,2048]{1,0:T(8,128)(2,1)}, bf16[256,2048]{1,0:T(8,128)(2,1)}, bf16[256,2048]{1,0:T(8,128)(2,1)}) custom-call(bf16[128,2048]{1,0:T(8,128)(2,1)} %bitcast.28, bf16[128,2048]{1,0:T(8,128)(2,1)} %bitcast.30, bf16[128,2048]{1,0:T(8,128)(2,1)} %bitcast.32, bf16[192,2048]{1,0:T(8,128)(2,1)} %copy-done.18, ...), custom_call_target="tpu_custom_call" | custom-call | tf_op jit(solution)/shard_map/pallas_call | solution.py:44
  219.4 0.0 collective-permute-done.par
  219.4 0.0 copy-start.4
  219.4 1.2 copy-done.4
  220.6 0.0 copy-start.5
  220.6 1.2 copy-done.5
  221.9 0.0 copy-start.6
  221.9 1.2 copy-done.6
  223.1 4.0 %shard_map.165 = (bf16[8,256,128]{2,1,0:T(8,128)(2,1)S(1)}, f32[8,256,128]{2,1,0:T(8,128)S(1)}, bf16[512,768]{1,0:T(8,128)(2,1)S(1)}) custom-call(s32[4]{0:T(128)S(1)} %pad_add_fusion.place, bf16[512,1024]{1,0:T(8,128)(2,1)S(1)} %bitcast.20, bf16[512,1024]{1,0:T(8,128)(2,1)S(1)} %collective-permute-done.par, bf16[256,2048]{1,0:T(8,128)(2,1)S(1)} %copy-done.4, ...), custom_call_target="tpu_custom_call" | custom-call | tf_op jit(solution)/shard_map/pallas_call | solution.py:62
  227.1 0.0 copy-start.7
  227.1 0.9 copy-done.7
  228.0 1.9 collective-permute-start.5
  229.9 1.9 collective-permute-done.5
  231.8 0.9 add_convert_fusion
  232.7 7.9 %all-to-all-start.1 = ((bf16[8,256,128]{2,1,0:T(8,128)(2,1)}), bf16[8,256,128]{2,1,0:T(8,128)(2,1)S(1)}, u32[]{:S(2)}, u32[]{:S(2)}) async-start(bf16[8,256,128]{2,1,0:T(8,128)(2,1)} %add_convert_fusion), calls=%async_computation.1 | async-start | bytes 1048576 | tf_op jit(solution)/shard_map/all_to_all | solution.py:348
  240.6 1.1 copy-done.8
  241.7 3.2 shard_map.166
  245.0 1.6 copy-done
  246.6 0.9 copy-done.17
  247.5 1.9 collective-permute-start.3
  249.4 8.4 %all-to-all-done.1.parts = bf16[8,256,128]{2,1,0:T(8,128)(2,1)S(1)} async-done(((bf16[8,256,128]{2,1,0:T(8,128)(2,1)}), bf16[8,256,128]{2,1,0:T(8,128)(2,1)S(1)}, u32[]{:S(2)}, u32[]{:S(2)}) %all-to-all-start.1) | async-done | bytes 524320 | tf_op jit(solution)/shard_map/all_to_all | solution.py:348
  257.7 1.3 shard_map.167
  259.0 5.6 %all-to-all-start.2 = ((bf16[32,16,128]{2,1,0:T(8,128)(2,1)}), bf16[32,16,128]{2,1,0:T(8,128)(2,1)S(1)}, u32[]{:S(2)}, u32[]{:S(2)}) async-start(bf16[32,16,128]{2,1,0:T(8,128)(2,1)} %shard_map.167), calls=%async_computation.2 | async-start | bytes 262144 | tf_op jit(solution)/shard_map/all_to_all | solution.py:350
  264.6 1.9 collective-permute-start.4
  266.5 8.6 %all-to-all-done.2 = bf16[32,16,128]{2,1,0:T(8,128)(2,1)S(1)} async-done(((bf16[32,16,128]{2,1,0:T(8,128)(2,1)}), bf16[32,16,128]{2,1,0:T(8,128)(2,1)S(1)}, u32[]{:S(2)}, u32[]{:S(2)}) %all-to-all-start.2) | async-done | bytes 131104 | tf_op jit(solution)/shard_map/all_to_all | solution.py:350
  275.1 0.0 copy-done.3
  275.1 0.8 shard_map.168
  275.9 0.0 copy-start.1
  275.9 22.7 %all-gather = bf16[2048,128]{1,0:T(8,128)(2,1)S(1)} all-gather(bf16[128,128]{1,0:T(8,128)(2,1)S(1)} %shard_map.168), channel_id=2, replica_groups=mesh['z'=8,'x'=4,'yh'=4,'yl'=2,'c'=2] {'yh','yl','c'}, dimensions={0}, use_global_device_ids=true | all-gather | bytes 557056 | tf_op jit(solution)/shard_map/all_gather | solution.py:358
  298.6 0.0 copy-done.12
  298.6 0.0 copy-done.13
  298.6 0.0 copy-done.14
  298.6 1.0 copy-done.10
  299.6 1.8 shard_map.169
  301.4 0.0 copy-start.9
  301.4 0.8 copy-done.9
  302.3 9.6 %all-to-all-start.3 = ((bf16[32,80,128]{2,1,0:T(8,128)(2,1)}), bf16[32,80,128]{2,1,0:T(8,128)(2,1)}, u32[]{:S(2)}, u32[]{:S(2)}) async-start(bf16[32,80,128]{2,1,0:T(8,128)(2,1)} %copy-done.9), calls=%async_computation.3 | async-start | bytes 1310720 | tf_op jit(solution)/shard_map/all_to_all | solution.py:376
  311.9 0.0 collective-permute-done.3
  311.9 1.2 fusion.3
  313.1 0.0 collective-permute-done.4
  313.1 1.2 fusion.4
  314.3 0.0 copy-done.1
  314.3 1.4 fusion.2
  315.7 17.1 %all-to-all-done.3.got = bf16[32,80,128]{2,1,0:T(8,128)(2,1)} async-done(((bf16[32,80,128]{2,1,0:T(8,128)(2,1)}), bf16[32,80,128]{2,1,0:T(8,128)(2,1)}, u32[]{:S(2)}, u32[]{:S(2)}) %all-to-all-start.3) | async-done | bytes 655392 | tf_op jit(solution)/shard_map/all_to_all | solution.py:376
  332.8 2.4 shard_map.170
  (8 shorter events, 0.0 us)
Async XLA Ops:
  0.7 1.0 copy-start.2
  1.8 1.0 copy-start.11
  2.8 0.7 copy-start.15
  3.5 0.7 copy-start.16
  46.8 172.6 %collective-permute-start = (bf16[512,1024]{1,0:T(8,128)(2,1)S(1)}, bf16[512,1024]{1,0:T(8,128)(2,1)S(1)}, u32[]{:S(2)}, u32[]{:S(2)}) collective-permute-start(bf16[512,1024]{1,0:T(8,128)(2,1)S(1)} %bitcast.19), channel_id=1, source_target_pairs={{0,1},{1,0},{2,3},{3,2},{4,5},{5,4},{6,7},{7,6},{8,9},{9,8},{10,11... | collective-permute-start | bytes 3145736 | tf_op jit(solution)/shard_map/ppermute | solution.py:311
  97.5 22.0 %collective-permute-start.1 = (bf16[192,2048]{1,0:T(8,128)(2,1)}, bf16[192,2048]{1,0:T(8,128)(2,1)S(1)}, u32[]{:S(2)}, u32[]{:S(2)}) collective-permute-start(bf16[192,2048]{1,0:T(8,128)(2,1)} %get-tuple-element.28), channel_id=1, source_target_pairs={{0,2},{2,4},{4,6},{6,8},{8,10},{10,12},{12,14},{14,0},{1,3},{3,5},... | collective-permute-start | bytes 2359304 | tf_op jit(solution)/shard_map/ppermute | solution.py:309
  101.0 21.9 %collective-permute-start.2 = (bf16[192,2048]{1,0:T(8,128)(2,1)}, bf16[192,2048]{1,0:T(8,128)(2,1)}, u32[]{:S(2)}, u32[]{:S(2)}) collective-permute-start(bf16[192,2048]{1,0:T(8,128)(2,1)} %get-tuple-element.29), channel_id=1, source_target_pairs={{0,14},{2,0},{4,2},{6,4},{8,6},{10,8},{12,10},{14,12},{1,15},{3,1}... | collective-permute-start | bytes 2359304 | tf_op jit(solution)/shard_map/ppermute | solution.py:310
  119.6 3.3 copy-start.18
  219.4 1.2 copy-start.4
  220.6 1.2 copy-start.5
  221.9 1.2 copy-start.6
  227.1 0.9 copy-start.7
  228.0 3.8 %collective-permute-start.5 = (bf16[8,256,128]{2,1,0:T(8,128)(2,1)S(1)}, bf16[8,256,128]{2,1,0:T(8,128)(2,1)S(1)}, u32[]{:S(2)}, u32[]{:S(2)}) collective-permute-start(bf16[8,256,128]{2,1,0:T(8,128)(2,1)S(1)} %get-tuple-element.39), channel_id=1, source_target_pairs={{0,1},{1,0},{2,3},{3,2},{4,5},{5,4},{6,7},{7,6},{8,9},{9,8},{10,11... | collective-permute-start | bytes 1572872 | tf_op jit(solution)/shard_map/ppermute | solution.py:338
  231.8 43.3 %copy-start.3 = (bf16[128,2048]{1,0:T(8,128)(2,1)S(1)}, bf16[128,2048]{1,0:T(8,128)(2,1)}, u32[]{:S(2)}) copy-start(bf16[128,2048]{1,0:T(8,128)(2,1)} %og_h.3) | copy-start | bytes 1572868
  232.7 65.9 %copy-start.12 = (f32[128,128]{1,0:T(8,128)S(1)}, f32[128,128]{1,0:T(8,128)}, u32[]{:S(2)}) copy-start(f32[128,128]{1,0:T(8,128)} %states.1) | copy-start | bytes 196612
  232.7 65.9 %copy-start.13 = (f32[128,128]{1,0:T(8,128)S(1)}, f32[128,128]{1,0:T(8,128)}, u32[]{:S(2)}) copy-start(f32[128,128]{1,0:T(8,128)} %decay_h.1) | copy-start | bytes 196612
  232.7 65.9 %copy-start.14 = (bf16[128,128]{1,0:T(8,128)(2,1)S(1)}, bf16[128,128]{1,0:T(8,128)(2,1)}, u32[]{:S(2)}) copy-start(bf16[128,128]{1,0:T(8,128)(2,1)} %gate_h.1) | copy-start | bytes 98308
  232.7 25.0 %all-to-all-start.1 = ((bf16[8,256,128]{2,1,0:T(8,128)(2,1)}), bf16[8,256,128]{2,1,0:T(8,128)(2,1)S(1)}, u32[]{:S(2)}, u32[]{:S(2)}) async-start(bf16[8,256,128]{2,1,0:T(8,128)(2,1)} %add_convert_fusion), calls=%async_computation.1 | async-start | bytes 1048576 | tf_op jit(solution)/shard_map/all_to_all | solution.py:348
  240.6 1.1 copy-start.8
  245.0 1.6 copy-start
  246.6 0.9 copy-start.17
  247.5 64.4 %collective-permute-start.3 = (bf16[192,2048]{1,0:T(8,128)(2,1)}, bf16[192,2048]{1,0:T(8,128)(2,1)}, u32[]{:S(2)}, u32[]{:S(2)}) collective-permute-start(bf16[192,2048]{1,0:T(8,128)(2,1)} %get-tuple-element.35), channel_id=1, source_target_pairs={{0,14},{2,0},{4,2},{6,4},{8,6},{10,8},{12,10},{14,12},{1,15},{3,1}... | collective-permute-start | bytes 2359304 | tf_op jit(solution)/shard_map/ppermute | solution.py:344
  259.0 16.1 %all-to-all-start.2 = ((bf16[32,16,128]{2,1,0:T(8,128)(2,1)}), bf16[32,16,128]{2,1,0:T(8,128)(2,1)S(1)}, u32[]{:S(2)}, u32[]{:S(2)}) async-start(bf16[32,16,128]{2,1,0:T(8,128)(2,1)} %shard_map.167), calls=%async_computation.2 | async-start | bytes 262144 | tf_op jit(solution)/shard_map/all_to_all | solution.py:350
  264.6 48.5 %collective-permute-start.4 = (bf16[192,2048]{1,0:T(8,128)(2,1)}, bf16[192,2048]{1,0:T(8,128)(2,1)}, u32[]{:S(2)}, u32[]{:S(2)}) collective-permute-start(bf16[192,2048]{1,0:T(8,128)(2,1)} %copy-done.17), channel_id=1, source_target_pairs={{0,2},{2,4},{4,6},{6,8},{8,10},{10,12},{12,14},{14,0},{1,3},{3,5},... | collective-permute-start | bytes 2359304 | tf_op jit(solution)/shard_map/ppermute | solution.py:345
  275.9 38.4 %copy-start.1 = (f32[384,2048]{1,0:T(8,128)S(1)}, f32[384,2048]{1,0:T(8,128)}, u32[]{:S(2)}) copy-start(f32[384,2048]{1,0:T(8,128)} %copy-done) | copy-start | bytes 9437188
  298.6 1.0 copy-start.10
  301.4 0.8 copy-start.9
  302.3 30.5 %all-to-all-start.3 = ((bf16[32,80,128]{2,1,0:T(8,128)(2,1)}), bf16[32,80,128]{2,1,0:T(8,128)(2,1)}, u32[]{:S(2)}, u32[]{:S(2)}) async-start(bf16[32,80,128]{2,1,0:T(8,128)(2,1)} %copy-done.9), calls=%async_computation.3 | async-start | bytes 1310720 | tf_op jit(solution)/shard_map/all_to_all | solution.py:376
where the time goes:
time: 336 us; the launch traced here: 335 us
  Pallas kernels  160 us (48%)
  blocking collectives  63.7 us (19%)
  waiting for transfers between devices  55.4 us (16%)
  starting transfers between devices  36.6 us (11%)
  local copies, waits for them, and re-layouts  15.9 us (5%)
    pallas_call x2, Pallas kernels, move(): pl.pallas_call(body, in_specs=[anywhere] * len(args), out_specs=[anywhere...  145 us
    all_to_all x1, blocking collectives, local(): own = lax.all_to_all(send.reshape(n_sp, cap, cols), SP, 0, 0, tiled=True)  41 us
    all_gather x1, blocking collectives, local(): mid = lax.all_gather(mid, TP)  22.7 us
    all_to_all x1, waiting for transfers between devices, local(): got = lax.all_to_all(out, SP, 0, 0, tiled=True)  17.1 us
    ppermute x1, waiting for transfers between devices, local(): wa = lax.ppermute(w_lo, Y, ring(1))  16.2 us
    pallas_call x7, Pallas kernels, call(): pl.pallas_call(body, grid_spec=pltpu.PrefetchScalarGridSpec(num_scalar_pr...  15.2 us
    unnamed x38, local copies, waits for them, and re-layouts  13.5 us
    all_to_all x1, starting transfers between devices, local(): got = lax.all_to_all(out, SP, 0, 0, tiled=True)  9.61 us
  transfers between devices with their start and end apart: 9, of which 6 were waited for; matrix products, arithmetic and copies ran while one was open for 1% of the time, Pallas kernels for 45%

commit v1 on v0

--- a/solution.py
+++ b/solution.py
@@ -12,6 +12,9 @@
 Y = ("yh", "yl")
 TP = ("yh", "yl", "c")
 F32, BF16 = jnp.float32, jnp.bfloat16
+
+
+VMEM = 12 << 20
 
 
 def nt(a, b):
@@ -44,21 +47,25 @@
     return pl.pallas_call(
         body,
         in_specs=[anywhere] * len(args),
-        out_specs=[anywhere] * len(out_shape),
+        out_specs=[pl.BlockSpec(memory_space=pltpu.VMEM)] * len(out_shape),
         out_shape=list(out_shape),
         scratch_shapes=[pltpu.SemaphoreType.DMA((count,))],
+        compiler_params=pltpu.CompilerParams(vmem_limit_bytes=8 << 20),
     )(*args)
 
 
-def call(body, out_shape, place, *args, specs=None, outs_in=None, scratch=(), vmem=24 << 20):
+def call(body, out_shape, place, *args, specs=None, outs_in=None, scratch=(), vmem=VMEM):
     whole = lambda a: pl.BlockSpec(a.shape, lambda i, s, n=len(a.shape): (0,) * n)
     outs = out_shape if isinstance(out_shape, (list, tuple)) else [out_shape]
     in_specs = [whole(a) for a in args]
     out_specs = [whole(o) for o in outs]
+    args, outs = list(args), list(outs)
     for k in specs or ():
         in_specs[k] = pl.BlockSpec(memory_space=pltpu.HBM)
+        args[k] = pltpu.with_memory_space_constraint(args[k], pltpu.HBM)
     for k in outs_in or ():
         out_specs[k] = pl.BlockSpec(memory_space=pltpu.HBM)
+        outs[k] = pltpu.HBM(outs[k].shape, outs[k].dtype)
     result = pl.pallas_call(
         body,
         grid_spec=pltpu.PrefetchScalarGridSpec(
@@ -123,33 +130,44 @@
         copy.wait()
 
 
-def expert_body(half, place, own, par, g_s, u_s, d_s, psend, pkeep, mix):
+def prep_body(place, gate, states, gated):
+    gated[...] = (gate[...].astype(F32) * states[...]).astype(BF16)
+
+
+def expert_body(
+    half, place, own, par, wg_h, wu_h, wd_h, wa_h, wb_h, psend, pkeep, mix_h, w_s, mix, sems
+):
     c = place[0]
     cols = own.shape[1]
     mine = pl.ds(pl.multiple_of(c * cols, cols), cols)
     other = pl.ds(pl.multiple_of((1 - c) * cols, cols), cols)
-    units = g_s.shape[0]
+    units = w_s.shape[1]
+    h = wg_h.shape[0]
+    q = (units - h) // 2
     groups = own.shape[0] // (2 * half)
-
-    def product(s, which):
-        r = nt(own[...], s[:, mine]) + nt(par[...], s[:, other])
+    pairs = []
+    for k, w in enumerate((wg_h, wu_h, wd_h)):
+        piece = pl.ds(k * q, q)
+        pairs.append((w, w_s.at[k, pl.ds(0, h)]))
+        pairs.append((wa_h.at[piece], w_s.at[k, pl.ds(h, q)]))
+        pairs.append((wb_h.at[piece], w_s.at[k, pl.ds(h + q, q)]))
+    loads = copies(pairs, sems)
+
+    def product(k, which):
+        for copy in loads[3 * k : 3 * k + 3]:
+            copy.wait()
+        r = nt(own[...], w_s[k, :, mine]) + nt(par[...], w_s[k, :, other])
         return r.reshape(groups, 2, half, units)[:, which].reshape(groups * half, units)
 
-    gate = product(g_s, 0)
-    up = product(u_s, 0)
-    grad = product(d_s, 1)
+    gate = product(0, 0)
+    up = product(1, 0)
+    grad = product(2, 1)
     sig = jax.nn.sigmoid(gate)
     silu = gate * sig
     hidden = silu * up
     up_grad = grad * silu
     gate_grad = grad * up * sig * (1.0 + gate * (1.0 - sig))
     gb, ub = gate_grad.astype(BF16), up_grad.astype(BF16)
-    parts = psend.shape[0]
-    width = cols // parts
-    for ref, where in ((psend, other), (pkeep, mine)):
-        p = nn(gb, g_s[:, where]) + nn(ub, u_s[:, where])
-        for k in range(parts):
-            ref[k] = p[:, k * width : (k + 1) * width].astype(ref.dtype)
     tile = lambda v: v.reshape(groups, 1, half, units)
     zero = jnp.zeros((groups, 1, half, units), F32)
     for k, pair in enumerate(
@@ -157,20 +175,37 @@
     ):
         v = jnp.concatenate(pair, axis=1).reshape(groups * 2 * half, units)
         mix[:, k * units : (k + 1) * units] = v.astype(BF16)
-
-
-def weight_body(place, own, par, mix, gown, ga, gb):
+    (kept,) = copies(((mix, mix_h),), sems.at[pl.ds(9, 1)])
+    parts = psend.shape[0]
+    width = cols // parts
+    for ref, where in ((psend, other), (pkeep, mine)):
+        p = nn(gb, w_s[0, :, where]) + nn(ub, w_s[1, :, where])
+        for k in range(parts):
+            ref[k] = p[:, k * width : (k + 1) * width].astype(ref.dtype)
+    kept.wait()
+
+
+def weight_body(place, own, par, mix, gown_h, ga, gb, gown, sems):
     c = place[0]
     cols = own.shape[1]
-    h, q = gown.shape[0] // 3, ga.shape[0] // 3
+    h, q = gown.shape[1] // 3, ga.shape[0] // 3
     units = h + 2 * q
-    for src, start in ((own, c * cols), (par, (1 - c) * cols)):
+    stored = []
+    for n, (src, start) in enumerate(((own, c * cols), (par, (1 - c) * cols))):
         where = pl.ds(pl.multiple_of(start, cols), cols)
         for k in range(3):
             g = tn(mix[:, k * units : (k + 1) * units], src[...])
-            gown[k * h : (k + 1) * h, where] = g[0:h]
+            rows = pl.ds(k * h, h)
+            gown[n, rows, :] = g[0:h]
+            copy = pltpu.make_async_copy(
+                gown.at[n, rows], gown_h.at[rows, where], sems.at[3 * n + k]
+            )
+            copy.start()
+            stored.append(copy)
             ga[k * q : (k + 1) * q, where] = g[h : h + q].astype(BF16)
             gb[k * q : (k + 1) * q, where] = g[h + q :].astype(BF16)
+    for copy in stored:
+        copy.wait()
 
 
 def fold_body(place, parts, out):
@@ -201,18 +236,21 @@
 
 
 def project_body(
-    place, mid, w, gate_h, states_h, decay_h, out, branch, local, prod, gate, states, decay, sems
+    place, mid, gated, w_h, gate_h, states_h, decay_h, out_h, branch, local, prod,
+    w, gate, states, decay, out, sems,
 ):
-    got = copies(((gate_h, gate), (states_h, states), (decay_h, decay)), sems)
+    got = copies(((w_h, w), (gate_h, gate), (states_h, states), (decay_h, decay)), sems)
     pieces = mid.shape[0]
     ys = pieces // 2
     full = jnp.concatenate([mid[(b % ys) * 2 + b // ys] for b in range(pieces)], axis=1)
-    act = nn(full, w[...])
+    grad = tn(full, gated[...]).astype(BF16)
+    dests, rows = out.shape[0], full.shape[1] // out.shape[0]
+    for d in range(dests):
+        out[d, 0:rows, :] = grad[d * rows : (d + 1) * rows]
     for copy in got:
         copy.wait()
+    act = nn(full, w[...])
     st, gt, dec = states[...], gate[...].astype(F32), decay[...]
-    grad = tn(full, (gt * st).astype(BF16)).astype(BF16)
-    dests, rows = out.shape[0], full.shape[1] // out.shape[0]
     branch[...] = (act * st).astype(BF16)
     n = st.shape[0]
     t = lax.broadcasted_iota(jnp.int32, st.shape, 0)
@@ -234,8 +272,9 @@
             extra = jnp.where(line == k, jnp.broadcast_to(v, extra.shape), extra)
     extra = extra.astype(BF16)
     for d in range(dests):
-        out[d, 0:rows, :] = grad[d * rows : (d + 1) * rows]
         out[d, rows : rows + tail, :] = extra
+    (sent,) = copies(((out, out_h),), sems.at[pl.ds(4, 1)])
+    sent.wait()
 
 
 def finish_body(place, got, local, prod, states, proj, drive, ddecay):
@@ -311,18 +350,7 @@
     par = lax.ppermute(own, "c", swap)
 
     units = hidden + 2 * q
-
-    def joined(*refs):
-        w, (lo, hi), to = refs[:3], refs[3:5], refs[5:]
-        pairs = []
-        for k in range(3):
-            piece = pl.ds(k * q, q)
-            pairs.append((w[k], to[k].at[pl.ds(0, hidden)]))
-            pairs.append((lo.at[piece], to[k].at[pl.ds(hidden, q)]))
-            pairs.append((hi.at[piece], to[k].at[pl.ds(hidden + q, q)]))
-        return pairs
-
-    weights = move(joined, [shape((units, width), BF16)] * 3, 9, wg, wu, wd, wa, wb)
+    gated = call(prep_body, shape((tokens, ch), BF16), place, gate_branch, states)
 
     slots = n_sp * half
     wide = cols // n_y
@@ -333,13 +361,23 @@
             shape((n_y, slots, wide), F32),
             shape((n_sp * cap, 3 * units), BF16),
         ],
-        place, own, par, *weights,
+        place, own, par, wg, wu, wd, wa, wb,
+        specs=(2, 3, 4, 5, 6), outs_in=(2,),
+        scratch=[
+            pltpu.VMEM((3, units, width), BF16),
+            pltpu.VMEM((n_sp * cap, 3 * units), BF16),
+            pltpu.SemaphoreType.DMA((10,)),
+        ],
     )
     precv = lax.ppermute(psend, "c", swap)
     gown, ga, gb = call(
         weight_body,
         [shape((3 * hidden, width), F32), shape((3 * q, width), BF16), shape((3 * q, width), BF16)],
         place, own, par, mix,
+        outs_in=(0,),
+        scratch=[
+            pltpu.VMEM((2, 3 * hidden, cols), F32), pltpu.SemaphoreType.DMA((6,)),
+        ],
     )
     back_lo = lax.ppermute(ga, Y, ring(-1))
     back_hi = lax.ppermute(gb, Y, ring(1))
@@ -366,11 +404,12 @@
             shape((tokens, ch), F32),
             shape((tokens, ch), F32),
         ],
-        place, mid, w_proj, gate_branch, states, decay,
-        specs=(2, 3, 4),
+        place, mid, gated, w_proj, gate_branch, states, decay,
+        specs=(2, 3, 4, 5), outs_in=(0,),
         scratch=[
-            pltpu.VMEM((tokens, ch), BF16), pltpu.VMEM((tokens, ch), F32),
-            pltpu.VMEM((tokens, ch), F32), pltpu.SemaphoreType.DMA((3,)),
+            pltpu.VMEM((width, ch), BF16), pltpu.VMEM((tokens, ch), BF16),
+            pltpu.VMEM((tokens, ch), F32), pltpu.VMEM((tokens, ch), F32),
+            pltpu.VMEM((n_sp, rows + 16, ch), BF16), pltpu.SemaphoreType.DMA((5,)),
         ],
     )
     got = lax.all_to_all(out, SP, 0, 0, tiled=True)

time: 336 us -> 187 us (0.56)
  Pallas kernels: 160 us -> 23 us
  local copies, waits for them, and re-layouts: 15.9 us -> 4.83 us
    pallas_call x2 -> x1, Pallas kernels: 145 us -> 0.18 us  [move(): pl.pallas_call(body, in_specs=[anywhere] * len(args), out_specs=[pl.Block...]
    unnamed x38 -> x26, local copies, waits for them, and re-layouts: 13.5 us -> 3.45 us
    pallas_call x7 -> x8, Pallas kernels: 15.2 us -> 22.8 us  [call(): pl.pallas_call(body, grid_spec=pltpu.PrefetchScalarGridSpec(num_scalar_pr...]
  transfers between devices with their start and end apart: 9 -> 9, of which waited for: 6 -> 6; matrix products, arithmetic and copies ran while one was open for 1% -> 1% of each run, Pallas kernels for 45% -> 6%
where the time goes in v1:
time: 187 us
  blocking collectives  62.5 us (33%)
  waiting for transfers between devices  56.7 us (30%)
  starting transfers between devices  36.5 us (20%)
  Pallas kernels  23 us (12%)
  local copies, waits for them, and re-layouts  4.83 us (3%)
  other arithmetic  2.38 us (1%)
    all_to_all x1, blocking collectives, local(): own = lax.all_to_all(send.reshape(n_sp, cap, cols), SP, 0, 0, tiled=True)  41.2 us
    pallas_call x8, Pallas kernels, call(): pl.pallas_call(body, grid_spec=pltpu.PrefetchScalarGridSpec(num_scalar_pr...  22.8 us
    all_gather x1, blocking collectives, local(): mid = lax.all_gather(mid, TP)  21.2 us
    all_to_all x1, waiting for transfers between devices, local(): got = lax.all_to_all(out, SP, 0, 0, tiled=True)  17.4 us
    ppermute x1, waiting for transfers between devices, local(): wa = lax.ppermute(w_lo, Y, ring(1))  16 us
    all_to_all x1, waiting for transfers between devices, local(): parts = lax.all_to_all(psum, Y, 0, 0, tiled=True)  10.3 us
    all_to_all x1, starting transfers between devices, local(): got = lax.all_to_all(out, SP, 0, 0, tiled=True)  9.51 us
    all_to_all x1, waiting for transfers between devices, local(): back = lax.all_to_all(ret, SP, 0, 0, tiled=True)  7.99 us
  transfers between devices with their start and end apart: 9, of which 6 were waited for; matrix products, arithmetic and copies ran while one was open for 1% of the time, Pallas kernels for 6%

profile of v1, /device:TPU:8, one launch (start us, length us, event | category | flops | bytes accessed | tf_op | source)
XLA Modules:
  0.0 186.7 jit_solution(14897623977159128971)
XLA Ops:
  0.6 0.0 copy-start.1
  0.6 0.0 copy-start
  0.7 0.0 copy-start.2
  0.7 0.1 pad_add_fusion.place
  0.8 2.9 %shard_map.162 = (bf16[512,1024]{1,0:T(8,128)(2,1)}, bf16[512,128]{1,0:T(8,128)(2,1)S(1)}) custom-call(s32[4]{0:T(128)S(1)} %pad_add_fusion.place, s32[2,128]{1,0:T(2,128)} %bitcast.31, f32[2,128]{1,0:T(2,128)} %bitcast.32, bf16[128,2048]{1,0:T(8,128)(2,1)} %x_h.1, bf16[128,2048]{1,0:T(8,128)(2,1)} %og_h.3), custom_call_target="tpu_custom_call" | custom-call | tf_op jit(solution)/shard_map/pallas_call | solution.py:69
  3.7 0.0 copy-start.7
  3.7 41.2 %all_to_all.20 = bf16[32,16,1024]{2,1,0:T(8,128)(2,1)S(1)} all-to-all(bf16[32,16,1024]{2,1,0:T(8,128)(2,1)} %bitcast.30), channel_id=1, replica_groups=mesh['z'=8,'x'=4,'yh'=4,'yl'=2,'c'=2] {'z','x'}, dimensions={0} | all-to-all | bytes 2097152 | tf_op jit(solution)/shard_map/all_to_all | solution.py:336
  44.9 1.9 %collective-permute-start = (bf16[512,1024]{1,0:T(8,128)(2,1)S(1)}, bf16[512,1024]{1,0:T(8,128)(2,1)S(1)}, u32[]{:S(2)}, u32[]{:S(2)}) collective-permute-start(bf16[512,1024]{1,0:T(8,128)(2,1)S(1)} %bitcast.19), channel_id=1, source_target_pairs={{0,1},{1,0},{2,3},{3,2},{4,5},{5,4},{6,7},{7,6},{8,9},{9,8},{10,11... | collective-permute-start | bytes 3145736 | tf_op jit(solution)/shard_map/ppermute | solution.py:350
  46.9 0.0 copy-done.1
  46.9 0.0 copy-done
  46.9 0.0 copy-done.2
  46.9 0.2 shard_map.163
  47.1 3.5 %collective-permute-start.1 = (bf16[192,2048]{1,0:T(8,128)(2,1)S(1)}, bf16[192,2048]{1,0:T(8,128)(2,1)S(1)}, u32[]{:S(2)}, u32[]{:S(2)}) collective-permute-start(bf16[192,2048]{1,0:T(8,128)(2,1)S(1)} %get-tuple-element.25), channel_id=1, source_target_pairs={{0,2},{2,4},{4,6},{6,8},{8,10},{10,12},{12,14},{14,0},{1,3},{3,5},... | collective-permute-start | bytes 2359304 | tf_op jit(solution)/shard_map/ppermute | solution.py:348
  50.6 2.4 %collective-permute-start.2 = (bf16[192,2048]{1,0:T(8,128)(2,1)S(1)}, bf16[192,2048]{1,0:T(8,128)(2,1)S(1)}, u32[]{:S(2)}, u32[]{:S(2)}) collective-permute-start(bf16[192,2048]{1,0:T(8,128)(2,1)S(1)} %get-tuple-element.26), channel_id=1, source_target_pairs={{0,14},{2,0},{4,2},{6,4},{8,6},{10,8},{12,10},{14,12},{1,15},{3,1}... | collective-permute-start | bytes 2359304 | tf_op jit(solution)/shard_map/ppermute | solution.py:349
  52.9 16.0 %collective-permute-done.1.wa_h = bf16[192,2048]{1,0:T(8,128)(2,1)S(1)} collective-permute-done((bf16[192,2048]{1,0:T(8,128)(2,1)S(1)}, bf16[192,2048]{1,0:T(8,128)(2,1)S(1)}, u32[]{:S(2)}, u32[]{:S(2)}) %collective-permute-start.1) | collective-permute-done | bytes 786464 | tf_op jit(solution)/shard_map/ppermute | solution.py:348
  68.9 0.0 copy-start.11
  68.9 3.2 %collective-permute-done.2.wb_h = bf16[192,2048]{1,0:T(8,128)(2,1)S(1)} collective-permute-done((bf16[192,2048]{1,0:T(8,128)(2,1)S(1)}, bf16[192,2048]{1,0:T(8,128)(2,1)S(1)}, u32[]{:S(2)}, u32[]{:S(2)}) %collective-permute-start.2) | collective-permute-done | bytes 786464 | tf_op jit(solution)/shard_map/ppermute | solution.py:349
  72.1 0.0 copy-start.12
  72.1 0.0 collective-permute-done.par
  72.1 0.0 copy-done.11
  72.1 0.9 copy-done.12
  73.1 7.6 %shard_map.164 = (bf16[8,256,128]{2,1,0:T(8,128)(2,1)S(1)}, f32[8,256,128]{2,1,0:T(8,128)S(1)}, bf16[512,768]{1,0:T(8,128)(2,1)}) custom-call(s32[4]{0:T(128)S(1)} %pad_add_fusion.place, bf16[512,1024]{1,0:T(8,128)(2,1)S(1)} %bitcast.20, bf16[512,1024]{1,0:T(8,128)(2,1)S(1)} %collective-permute-done.par, bf16[128,2048]{1,0:T(8,128)(2,1)} %bitcast.23, ...), custom_call_target="tpu_custom_call" | custom-call | tf_op jit(solution)/shard_map/pallas_call | solution.py:69
  80.6 0.0 copy-done.7
  80.6 0.0 copy-start.3
  80.6 2.1 %collective-permute-start.5 = (bf16[8,256,128]{2,1,0:T(8,128)(2,1)S(1)}, bf16[8,256,128]{2,1,0:T(8,128)(2,1)S(1)}, u32[]{:S(2)}, u32[]{:S(2)}) collective-permute-start(bf16[8,256,128]{2,1,0:T(8,128)(2,1)S(1)} %get-tuple-element.33), channel_id=1, source_target_pairs={{0,1},{1,0},{2,3},{3,2},{4,5},{5,4},{6,7},{7,6},{8,9},{9,8},{10,11... | collective-permute-start | bytes 1572872 | tf_op jit(solution)/shard_map/ppermute | solution.py:372
  82.7 1.9 %collective-permute-done.5 = bf16[8,256,128]{2,1,0:T(8,128)(2,1)S(1)} collective-permute-done((bf16[8,256,128]{2,1,0:T(8,128)(2,1)S(1)}, bf16[8,256,128]{2,1,0:T(8,128)(2,1)S(1)}, u32[]{:S(2)}, u32[]{:S(2)}) %collective-permute-start.5) | collective-permute-done | bytes 524320 | tf_op jit(solution)/shard_map/ppermute | solution.py:372
  84.6 0.0 copy-start.4
  84.6 0.0 copy-start.6
  84.6 0.9 add_convert_fusion
  85.5 7.8 %all-to-all-start.1 = ((bf16[8,256,128]{2,1,0:T(8,128)(2,1)}), bf16[8,256,128]{2,1,0:T(8,128)(2,1)S(1)}, u32[]{:S(2)}, u32[]{:S(2)}) async-start(bf16[8,256,128]{2,1,0:T(8,128)(2,1)} %add_convert_fusion), calls=%async_computation.1 | async-start | bytes 1048576 | tf_op jit(solution)/shard_map/all_to_all | solution.py:386
  93.2 0.0 copy-done.3
  93.2 4.1 %shard_map.165 = (f32[384,2048]{1,0:T(8,128)}, bf16[192,2048]{1,0:T(8,128)(2,1)}, bf16[192,2048]{1,0:T(8,128)(2,1)S(1)}) custom-call(s32[4]{0:T(128)S(1)} %pad_add_fusion.place, bf16[512,1024]{1,0:T(8,128)(2,1)S(1)} %bitcast.21, bf16[512,1024]{1,0:T(8,128)(2,1)S(1)} %collective-permute-done.par, bf16[512,768]{1,0:T(8,128)(2,1)S(1)} %copy-done.3), custom_call_target="tpu_custom_call" | custom-call | tf_op jit(solution)/shard_map/pallas_call | solution.py:69
  97.3 0.0 copy-start.9
  97.3 0.9 copy-done.9
  98.2 1.9 %collective-permute-start.3 = (bf16[192,2048]{1,0:T(8,128)(2,1)}, bf16[192,2048]{1,0:T(8,128)(2,1)S(1)}, u32[]{:S(2)}, u32[]{:S(2)}) collective-permute-start(bf16[192,2048]{1,0:T(8,128)(2,1)} %get-tuple-element.29), channel_id=1, source_target_pairs={{0,14},{2,0},{4,2},{6,4},{8,6},{10,8},{12,10},{14,12},{1,15},{3,1}... | collective-permute-start | bytes 2359304 | tf_op jit(solution)/shard_map/ppermute | solution.py:382
  100.1 10.3 %all-to-all-done.1.parts = bf16[8,256,128]{2,1,0:T(8,128)(2,1)S(1)} async-done(((bf16[8,256,128]{2,1,0:T(8,128)(2,1)}), bf16[8,256,128]{2,1,0:T(8,128)(2,1)S(1)}, u32[]{:S(2)}, u32[]{:S(2)}) %all-to-all-start.1) | async-done | bytes 524320 | tf_op jit(solution)/shard_map/all_to_all | solution.py:386
  110.4 1.3 shard_map.166
  111.6 5.6 %all-to-all-start.2 = ((bf16[32,16,128]{2,1,0:T(8,128)(2,1)}), bf16[32,16,128]{2,1,0:T(8,128)(2,1)S(1)}, u32[]{:S(2)}, u32[]{:S(2)}) async-start(bf16[32,16,128]{2,1,0:T(8,128)(2,1)} %shard_map.166), calls=%async_computation.2 | async-start | bytes 262144 | tf_op jit(solution)/shard_map/all_to_all | solution.py:388
  117.2 1.9 %collective-permute-start.4 = (bf16[192,2048]{1,0:T(8,128)(2,1)}, bf16[192,2048]{1,0:T(8,128)(2,1)}, u32[]{:S(2)}, u32[]{:S(2)}) collective-permute-start(bf16[192,2048]{1,0:T(8,128)(2,1)} %copy-done.9), channel_id=1, source_target_pairs={{0,2},{2,4},{4,6},{6,8},{8,10},{10,12},{12,14},{14,0},{1,3},{3,5},... | collective-permute-start | bytes 2359304 | tf_op jit(solution)/shard_map/ppermute | solution.py:383
  119.1 0.0 copy-done.4
  119.2 0.0 copy-done.6
  119.2 0.5 shard_map.168.gated
  119.7 8.0 %all-to-all-done.2 = bf16[32,16,128]{2,1,0:T(8,128)(2,1)S(1)} async-done(((bf16[32,16,128]{2,1,0:T(8,128)(2,1)}), bf16[32,16,128]{2,1,0:T(8,128)(2,1)S(1)}, u32[]{:S(2)}, u32[]{:S(2)}) %all-to-all-start.2) | async-done | bytes 131104 | tf_op jit(solution)/shard_map/all_to_all | solution.py:388
  127.7 0.0 copy-start.8
  127.7 0.9 copy-done.8
  128.6 1.3 shard_map.167
  129.9 21.2 %all-gather = bf16[2048,128]{1,0:T(8,128)(2,1)S(1)} all-gather(bf16[128,128]{1,0:T(8,128)(2,1)S(1)} %shard_map.167), channel_id=2, replica_groups=mesh['z'=8,'x'=4,'yh'=4,'yl'=2,'c'=2] {'yh','yl','c'}, dimensions={0}, use_global_device_ids=true | all-gather | bytes 557056 | tf_op jit(solution)/shard_map/all_gather | solution.py:396
  151.2 3.7 %shard_map.169 = (bf16[32,80,128]{2,1,0:T(8,128)(2,1)}, bf16[128,128]{1,0:T(8,128)(2,1)}, f32[128,128]{1,0:T(8,128)S(1)}, f32[128,128]{1,0:T(8,128)S(1)}) custom-call(s32[4]{0:T(128)S(1)} %pad_add_fusion.place, bf16[16,128,128]{2,1,0:T(8,128)(2,1)S(1)} %bitcast.22, bf16[128,128]{1,0:T(8,128)(2,1)S(1)} %shard_map.168.gated, bf16[2048,128]{1,0:T(8,128)(2,1)} %w_h.1, ...), custom_call_target="tpu_custom_call" | custom-call | tf_op jit(solution)/shard_map/pallas_call | solution.py:69
  154.9 9.5 %all-to-all-start.3 = ((bf16[32,80,128]{2,1,0:T(8,128)(2,1)}), bf16[32,80,128]{2,1,0:T(8,128)(2,1)S(1)}, u32[]{:S(2)}, u32[]{:S(2)}) async-start(bf16[32,80,128]{2,1,0:T(8,128)(2,1)} %get-tuple-element.34), calls=%async_computation.3 | async-start | bytes 1310720 | tf_op jit(solution)/shard_map/all_to_all | solution.py:415
  164.5 0.0 copy-start.10
  164.5 0.0 collective-permute-done.3
  164.5 0.1 fusion.3
  164.6 0.0 collective-permute-done.4
  164.6 1.3 fusion.4
  165.9 0.7 copy-done.10
  166.6 0.0 copy-start.5
  166.6 1.4 fusion.2
  168.0 17.4 %all-to-all-done.3.got = bf16[32,80,128]{2,1,0:T(8,128)(2,1)S(1)} async-done(((bf16[32,80,128]{2,1,0:T(8,128)(2,1)}), bf16[32,80,128]{2,1,0:T(8,128)(2,1)S(1)}, u32[]{:S(2)}, u32[]{:S(2)}) %all-to-all-start.3) | async-done | bytes 655392 | tf_op jit(solution)/shard_map/all_to_all | solution.py:415
  185.4 0.0 copy-done.5
  185.4 1.4 shard_map.170
Async XLA Ops:
  0.6 46.2 %copy-start.1 = (bf16[1,128,2048]{2,1,0:T(8,128)(2,1)S(1)}, bf16[1,128,2048]{2,1,0:T(8,128)(2,1)}, u32[]{:S(2)}) copy-start(bf16[1,128,2048]{2,1,0:T(8,128)(2,1)} %param.20) | copy-start | bytes 1572868
  0.6 46.2 %copy-start = (bf16[1,128,2048]{2,1,0:T(8,128)(2,1)S(1)}, bf16[1,128,2048]{2,1,0:T(8,128)(2,1)}, u32[]{:S(2)}) copy-start(bf16[1,128,2048]{2,1,0:T(8,128)(2,1)} %param.19) | copy-start | bytes 1572868
  0.7 46.2 %copy-start.2 = (bf16[1,128,2048]{2,1,0:T(8,128)(2,1)S(1)}, bf16[1,128,2048]{2,1,0:T(8,128)(2,1)}, u32[]{:S(2)}) copy-start(bf16[1,128,2048]{2,1,0:T(8,128)(2,1)} %param.21) | copy-start | bytes 1572868
  3.7 76.9 %copy-start.7 = (bf16[512,128]{1,0:T(8,128)(2,1)}, bf16[512,128]{1,0:T(8,128)(2,1)S(1)}, u32[]{:S(2)}) copy-start(bf16[512,128]{1,0:T(8,128)(2,1)S(1)} %get-tuple-element.31.pick) | copy-start | bytes 393220
  44.9 27.2 %collective-permute-start = (bf16[512,1024]{1,0:T(8,128)(2,1)S(1)}, bf16[512,1024]{1,0:T(8,128)(2,1)S(1)}, u32[]{:S(2)}, u32[]{:S(2)}) collective-permute-start(bf16[512,1024]{1,0:T(8,128)(2,1)S(1)} %bitcast.19), channel_id=1, source_target_pairs={{0,1},{1,0},{2,3},{3,2},{4,5},{5,4},{6,7},{7,6},{8,9},{9,8},{10,11... | collective-permute-start | bytes 3145736 | tf_op jit(solution)/shard_map/ppermute | solution.py:350
  47.1 21.8 %collective-permute-start.1 = (bf16[192,2048]{1,0:T(8,128)(2,1)S(1)}, bf16[192,2048]{1,0:T(8,128)(2,1)S(1)}, u32[]{:S(2)}, u32[]{:S(2)}) collective-permute-start(bf16[192,2048]{1,0:T(8,128)(2,1)S(1)} %get-tuple-element.25), channel_id=1, source_target_pairs={{0,2},{2,4},{4,6},{6,8},{8,10},{10,12},{12,14},{14,0},{1,3},{3,5},... | collective-permute-start | bytes 2359304 | tf_op jit(solution)/shard_map/ppermute | solution.py:348
  50.6 21.6 %collective-permute-start.2 = (bf16[192,2048]{1,0:T(8,128)(2,1)S(1)}, bf16[192,2048]{1,0:T(8,128)(2,1)S(1)}, u32[]{:S(2)}, u32[]{:S(2)}) collective-permute-start(bf16[192,2048]{1,0:T(8,128)(2,1)S(1)} %get-tuple-element.26), channel_id=1, source_target_pairs={{0,14},{2,0},{4,2},{6,4},{8,6},{10,8},{12,10},{14,12},{1,15},{3,1}... | collective-permute-start | bytes 2359304 | tf_op jit(solution)/shard_map/ppermute | solution.py:349
  68.9 3.2 %copy-start.11 = (bf16[192,2048]{1,0:T(8,128)(2,1)}, bf16[192,2048]{1,0:T(8,128)(2,1)S(1)}, u32[]{:S(2)}) copy-start(bf16[192,2048]{1,0:T(8,128)(2,1)S(1)} %collective-permute-done.1.wa_h) | copy-start | bytes 2359300
  72.1 0.9 copy-start.12
  80.6 12.6 %copy-start.3 = (bf16[512,768]{1,0:T(8,128)(2,1)S(1)}, bf16[512,768]{1,0:T(8,128)(2,1)}, u32[]{:S(2)}) copy-start(bf16[512,768]{1,0:T(8,128)(2,1)} %get-tuple-element.27.mix) | copy-start | bytes 2359300
  80.6 3.9 %collective-permute-start.5 = (bf16[8,256,128]{2,1,0:T(8,128)(2,1)S(1)}, bf16[8,256,128]{2,1,0:T(8,128)(2,1)S(1)}, u32[]{:S(2)}, u32[]{:S(2)}) collective-permute-start(bf16[8,256,128]{2,1,0:T(8,128)(2,1)S(1)} %get-tuple-element.33), channel_id=1, source_target_pairs={{0,1},{1,0},{2,3},{3,2},{4,5},{5,4},{6,7},{7,6},{8,9},{9,8},{10,11... | collective-permute-start | bytes 1572872 | tf_op jit(solution)/shard_map/ppermute | solution.py:372
  84.6 34.6 %copy-start.4 = (f32[128,128]{1,0:T(8,128)S(1)}, f32[128,128]{1,0:T(8,128)}, u32[]{:S(2)}) copy-start(f32[128,128]{1,0:T(8,128)} %states.3) | copy-start | bytes 196612
  84.6 34.6 %copy-start.6 = (bf16[128,128]{1,0:T(8,128)(2,1)S(1)}, bf16[128,128]{1,0:T(8,128)(2,1)}, u32[]{:S(2)}) copy-start(bf16[128,128]{1,0:T(8,128)(2,1)} %gate_h.1) | copy-start | bytes 98308
  85.5 24.9 %all-to-all-start.1 = ((bf16[8,256,128]{2,1,0:T(8,128)(2,1)}), bf16[8,256,128]{2,1,0:T(8,128)(2,1)S(1)}, u32[]{:S(2)}, u32[]{:S(2)}) async-start(bf16[8,256,128]{2,1,0:T(8,128)(2,1)} %add_convert_fusion), calls=%async_computation.1 | async-start | bytes 1048576 | tf_op jit(solution)/shard_map/all_to_all | solution.py:386
  97.3 0.9 copy-start.9
  98.2 66.3 %collective-permute-start.3 = (bf16[192,2048]{1,0:T(8,128)(2,1)}, bf16[192,2048]{1,0:T(8,128)(2,1)S(1)}, u32[]{:S(2)}, u32[]{:S(2)}) collective-permute-start(bf16[192,2048]{1,0:T(8,128)(2,1)} %get-tuple-element.29), channel_id=1, source_target_pairs={{0,14},{2,0},{4,2},{6,4},{8,6},{10,8},{12,10},{14,12},{1,15},{3,1}... | collective-permute-start | bytes 2359304 | tf_op jit(solution)/shard_map/ppermute | solution.py:382
  111.6 16.1 %all-to-all-start.2 = ((bf16[32,16,128]{2,1,0:T(8,128)(2,1)}), bf16[32,16,128]{2,1,0:T(8,128)(2,1)S(1)}, u32[]{:S(2)}, u32[]{:S(2)}) async-start(bf16[32,16,128]{2,1,0:T(8,128)(2,1)} %shard_map.166), calls=%async_computation.2 | async-start | bytes 262144 | tf_op jit(solution)/shard_map/all_to_all | solution.py:388
  117.2 47.4 %collective-permute-start.4 = (bf16[192,2048]{1,0:T(8,128)(2,1)}, bf16[192,2048]{1,0:T(8,128)(2,1)}, u32[]{:S(2)}, u32[]{:S(2)}) collective-permute-start(bf16[192,2048]{1,0:T(8,128)(2,1)} %copy-done.9), channel_id=1, source_target_pairs={{0,2},{2,4},{4,6},{6,8},{8,10},{10,12},{12,14},{14,0},{1,3},{3,5},... | collective-permute-start | bytes 2359304 | tf_op jit(solution)/shard_map/ppermute | solution.py:383
  127.7 0.9 copy-start.8
  154.9 30.4 %all-to-all-start.3 = ((bf16[32,80,128]{2,1,0:T(8,128)(2,1)}), bf16[32,80,128]{2,1,0:T(8,128)(2,1)S(1)}, u32[]{:S(2)}, u32[]{:S(2)}) async-start(bf16[32,80,128]{2,1,0:T(8,128)(2,1)} %get-tuple-element.34), calls=%async_computation.3 | async-start | bytes 1310720 | tf_op jit(solution)/shard_map/all_to_all | solution.py:415
  164.5 2.1 %copy-start.10 = (f32[384,2048]{1,0:T(8,128)S(1)}, f32[384,2048]{1,0:T(8,128)}, u32[]{:S(2)}) copy-start(f32[384,2048]{1,0:T(8,128)} %get-tuple-element.28) | copy-start | bytes 9437188
  166.6 18.8 %copy-start.5 = (f32[128,128]{1,0:T(8,128)S(1)}, f32[128,128]{1,0:T(8,128)}, u32[]{:S(2)}) copy-start(f32[128,128]{1,0:T(8,128)} %states.3) | copy-start | bytes 196612

commit v2 on v1

--- a/solution.py
+++ b/solution.py
@@ -83,7 +83,7 @@
     return result if isinstance(out_shape, (list, tuple)) else result[0]
 
 
-def dispatch_body(experts, cap, place, ids_h, wts_h, x_h, og_h, send_h, pick, ids, wts, x, og, send, sems):
+def dispatch_body(experts, cap, place, ids_h, wts_h, x_h, og_h, send_h, pick_h, ids, wts, x, og, send, pick, sems):
     n, cols = x.shape
     half = cap // 2
     mine = pl.ds(pl.multiple_of(place[0] * cols, cols), cols)
@@ -114,87 +114,126 @@
     hot = hot.reshape(experts * half, n).astype(BF16)
     got[2].wait()
     got[3].wait()
-    steps, out = 2, []
-    wide = cols // steps
-    for k in range(steps):
+    out, wide = [], cols // 2
+    for k in range(2):
         where = slice(k * wide, (k + 1) * wide)
-        xs = nn(hot, x[:, where]).reshape(experts, 1, half, wide)
-        cs = (nn(hot, og[:, where]) * scale).reshape(experts, 1, half, wide)
-        send[:, where] = (
-            jnp.concatenate([xs, cs], axis=1).reshape(experts * 2 * half, wide).astype(BF16)
-        )
-        copy = pltpu.make_async_copy(send.at[:, where], send_h.at[:, where], sems.at[4 + k])
-        copy.start()
-        out.append(copy)
-    for copy in out:
+        send[:, where] = nn(hot, x[:, where]).astype(BF16)
+        there = slice(cols + k * wide, cols + (k + 1) * wide)
+        send[:, there] = (nn(hot, og[:, where]) * scale).astype(BF16)
+        for cut in (where, there):
+            copy = pltpu.make_async_copy(
+                send.at[:, cut], send_h.at[:, cut], sems.at[4 + len(out)]
+            )
+            copy.start()
+            out.append(copy)
+    kept = pltpu.make_async_copy(pick, pick_h, sems.at[8])
+    kept.start()
+    for copy in (*out, kept):
         copy.wait()
 
 
-def prep_body(place, gate, states, gated):
-    gated[...] = (gate[...].astype(F32) * states[...]).astype(BF16)
-
-
-def expert_body(
-    half, place, own, par, wg_h, wu_h, wd_h, wa_h, wb_h, psend, pkeep, mix_h, w_s, mix, sems
-):
-    c = place[0]
-    cols = own.shape[1]
-    mine = pl.ds(pl.multiple_of(c * cols, cols), cols)
-    other = pl.ds(pl.multiple_of((1 - c) * cols, cols), cols)
+def split3(v):
+    a = v.astype(BF16).astype(F32)
+    b = (v - a).astype(BF16).astype(F32)
+    return a, b, (v - a - b).astype(BF16).astype(F32)
+
+
+def prep_body(place, gate, states, decay, gated, weight, tail):
+    st, gt, dec = states[...], gate[...].astype(F32), decay[...]
+    gated[...] = (gt * st).astype(BF16)
+    n = st.shape[0]
+    t = lax.broadcasted_iota(jnp.int32, st.shape, 0)
+    prefix, k = dec, 1
+    while k < n:
+        prefix = prefix * jnp.where(t >= k, pltpu.roll(prefix, k, 0), 1.0)
+        k *= 2
+    weight[...] = prefix * gt
+    values = split3(prefix[n - 1 : n])
+    line = lax.broadcasted_iota(jnp.int32, tail.shape, 0)
+    rows = jnp.zeros(tail.shape, F32)
+    for k, v in enumerate(values):
+        rows = jnp.where(line == 3 + k, jnp.broadcast_to(v, tail.shape), rows)
+    for k, v in enumerate(split3(st[n - 1 : n])):
+        rows = jnp.where(line == 8 + k, jnp.broadcast_to(v, tail.shape), rows)
+    tail[...] = rows
+
+
+def weight_copies(wg, wu, wd, wa, wb, w_s, where, count):
+    h = wg.shape[0]
+    q = (w_s.shape[1] - h) // 2
+    pairs = []
+    for k, w in enumerate((wg, wu, wd)[:count]):
+        piece = pl.ds(k * q, q)
+        pairs.append((w.at[:, where], w_s.at[k, pl.ds(0, h)]))
+        pairs.append((wa.at[piece, where], w_s.at[k, pl.ds(h, q)]))
+        pairs.append((wb.at[piece, where], w_s.at[k, pl.ds(h + q, q)]))
+    return pairs
+
+
+def columns(core, cols):
+    return pl.ds(pl.multiple_of(core * cols, cols), cols)
+
+
+def product(k, rows, w_s, loads):
+    for copy in loads[3 * k : 3 * k + 3]:
+        copy.wait()
+    cols = w_s.shape[2]
+    side = rows[:, 0:cols] if k < 2 else rows[:, cols:]
+    return nt(side, w_s[k])
+
+
+def first_body(place, own, wg, wu, wd, wa, wb, part, w_s, sems):
+    where = columns(place[0], w_s.shape[2])
+    loads = copies(weight_copies(wg, wu, wd, wa, wb, w_s, where, 3), sems)
+    for k in range(3):
+        part[k] = product(k, own, w_s, loads)
+
+
+def partials(out, gb, ub, w_s):
+    width = out.shape[2]
+    p = nn(gb, w_s[0]) + nn(ub, w_s[1])
+    for k in range(out.shape[0]):
+        out[k] = p[:, k * width : (k + 1) * width].astype(out.dtype)
+
+
+def expert_body(place, par, part, wg, wu, wd, wa, wb, psend, mix_h, w_s, mix, sems):
+    where = columns(1 - place[0], w_s.shape[2])
+    loads = copies(weight_copies(wg, wu, wd, wa, wb, w_s, where, 3), sems)
     units = w_s.shape[1]
-    h = wg_h.shape[0]
-    q = (units - h) // 2
-    groups = own.shape[0] // (2 * half)
-    pairs = []
-    for k, w in enumerate((wg_h, wu_h, wd_h)):
-        piece = pl.ds(k * q, q)
-        pairs.append((w, w_s.at[k, pl.ds(0, h)]))
-        pairs.append((wa_h.at[piece], w_s.at[k, pl.ds(h, q)]))
-        pairs.append((wb_h.at[piece], w_s.at[k, pl.ds(h + q, q)]))
-    loads = copies(pairs, sems)
-
-    def product(k, which):
-        for copy in loads[3 * k : 3 * k + 3]:
-            copy.wait()
-        r = nt(own[...], w_s[k, :, mine]) + nt(par[...], w_s[k, :, other])
-        return r.reshape(groups, 2, half, units)[:, which].reshape(groups * half, units)
-
-    gate = product(0, 0)
-    up = product(1, 0)
-    grad = product(2, 1)
+    gate = part[0] + product(0, par, w_s, loads)
+    up = part[1] + product(1, par, w_s, loads)
+    grad = part[2] + product(2, par, w_s, loads)
     sig = jax.nn.sigmoid(gate)
     silu = gate * sig
-    hidden = silu * up
-    up_grad = grad * silu
-    gate_grad = grad * up * sig * (1.0 + gate * (1.0 - sig))
-    gb, ub = gate_grad.astype(BF16), up_grad.astype(BF16)
-    tile = lambda v: v.reshape(groups, 1, half, units)
-    zero = jnp.zeros((groups, 1, half, units), F32)
-    for k, pair in enumerate(
-        ((tile(gate_grad), zero), (tile(up_grad), zero), (zero, tile(hidden)))
-    ):
-        v = jnp.concatenate(pair, axis=1).reshape(groups * 2 * half, units)
-        mix[:, k * units : (k + 1) * units] = v.astype(BF16)
+    ub = (grad * silu).astype(BF16)
+    gb = (grad * up * sig * (1.0 + gate * (1.0 - sig))).astype(BF16)
+    mix[:, 0:units] = gb
+    mix[:, units : 2 * units] = ub
+    mix[:, 2 * units :] = (silu * up).astype(BF16)
     (kept,) = copies(((mix, mix_h),), sems.at[pl.ds(9, 1)])
-    parts = psend.shape[0]
-    width = cols // parts
-    for ref, where in ((psend, other), (pkeep, mine)):
-        p = nn(gb, w_s[0, :, where]) + nn(ub, w_s[1, :, where])
-        for k in range(parts):
-            ref[k] = p[:, k * width : (k + 1) * width].astype(ref.dtype)
+    partials(psend, gb, ub, w_s)
     kept.wait()
+
+
+def keep_body(place, mix_h, wg, wu, wd, wa, wb, pkeep, w_s, mix, sems):
+    where = columns(place[0], w_s.shape[2])
+    units = w_s.shape[1]
+    pairs = weight_copies(wg, wu, wd, wa, wb, w_s, where, 2)
+    for copy in copies([(mix_h.at[:, pl.ds(0, 2 * units)], mix)] + pairs, sems):
+        copy.wait()
+    partials(pkeep, mix[:, 0:units], mix[:, units:], w_s)
 
 
 def weight_body(place, own, par, mix, gown_h, ga, gb, gown, sems):
     c = place[0]
-    cols = own.shape[1]
     h, q = gown.shape[1] // 3, ga.shape[0] // 3
-    units = h + 2 * q
+    units, cols = h + 2 * q, gown.shape[2]
     stored = []
-    for n, (src, start) in enumerate(((own, c * cols), (par, (1 - c) * cols))):
-        where = pl.ds(pl.multiple_of(start, cols), cols)
+    for n, (src, core) in enumerate(((own, c), (par, 1 - c))):
+        where = columns(core, cols)
         for k in range(3):
-            g = tn(mix[:, k * units : (k + 1) * units], src[...])
+            side = src[:, 0:cols] if k < 2 else src[:, cols:]
+            g = tn(mix[:, k * units : (k + 1) * units], side)
             rows = pl.ds(k * h, h)
             gown[n, rows, :] = g[0:h]
             copy = pltpu.make_async_copy(
@@ -220,61 +259,62 @@
     out[...] = jnp.concatenate(both, axis=1).astype(BF16)
 
 
-def combine_body(place, pick, back, og_h, mid, og, sems):
+def combine_body(place, pick_h, back, og_h, mid, pick, og, sems):
     n = mid.shape[1]
-    where = pl.ds(pl.multiple_of(place[3] * n, n), n)
-    (copy,) = copies(((og_h.at[:, where], og),), sems)
+    got = copies(((pick_h, pick), (og_h.at[:, columns(place[3], n)], og)), sems)
+    got[0].wait()
     part = tn(pick[...], back[...])
-    copy.wait()
+    got[1].wait()
     mid[...] = (og[...].astype(F32) + part).astype(BF16)
 
 
-def split3(v):
-    a = v.astype(BF16).astype(F32)
-    b = (v - a).astype(BF16).astype(F32)
-    return a, b, (v - a - b).astype(BF16).astype(F32)
-
-
 def project_body(
-    place, mid, gated, w_h, gate_h, states_h, decay_h, out_h, branch, local, prod,
-    w, gate, states, decay, out, sems,
+    place, mid, gated_h, w_h, weight_h, tail_h, out_h, act_o, gated, w, weight, tail, out, sems
 ):
-    got = copies(((w_h, w), (gate_h, gate), (states_h, states), (decay_h, decay)), sems)
+    got = copies(
+        ((gated_h, gated), (w_h, w), (weight_h, weight), (tail_h, tail)), sems
+    )
     pieces = mid.shape[0]
     ys = pieces // 2
     full = jnp.concatenate([mid[(b % ys) * 2 + b // ys] for b in range(pieces)], axis=1)
+    dests, rows = out.shape[0], full.shape[1] // out.shape[0]
+    got[0].wait()
     grad = tn(full, gated[...]).astype(BF16)
-    dests, rows = out.shape[0], full.shape[1] // out.shape[0]
     for d in range(dests):
         out[d, 0:rows, :] = grad[d * rows : (d + 1) * rows]
-    for copy in got:
+    head, rest = pl.ds(0, rows), pl.ds(rows, out.shape[1] - rows)
+    sent = copies(((out.at[:, head], out_h.at[:, head]),), sems.at[pl.ds(4, 1)])
+    got[1].wait()
+    act = nn(full, w[...])
+    act_o[...] = act
+    got[2].wait()
+    got[3].wait()
+    total = jnp.sum(weight[...] * act, axis=0, keepdims=True)
+    extra = tail[...]
+    line = lax.broadcasted_iota(jnp.int32, extra.shape, 0)
+    for k, v in enumerate(split3(total)):
+        extra = jnp.where(line == k, jnp.broadcast_to(v, extra.shape), extra)
+    extra = extra.astype(BF16)
+    for d in range(dests):
+        out[d, rows:, :] = extra
+    sent += copies(((out.at[:, rest], out_h.at[:, rest]),), sems.at[pl.ds(5, 1)])
+    for copy in sent:
         copy.wait()
-    act = nn(full, w[...])
+
+
+def scan_body(place, act, gate, states, decay, branch, local, prod):
     st, gt, dec = states[...], gate[...].astype(F32), decay[...]
-    branch[...] = (act * st).astype(BF16)
+    branch[...] = (act[...] * st).astype(BF16)
     n = st.shape[0]
     t = lax.broadcasted_iota(jnp.int32, st.shape, 0)
     ahead = lambda v, k, fill: jnp.where(t < n - k, pltpu.roll(v, n - k, 0), fill)
-    b, a = act * gt, ahead(dec, 1, 1.0)
+    b, a = act[...] * gt, ahead(dec, 1, 1.0)
     k = 1
     while k < n:
         b, a = b + a * ahead(b, k, 0.0), a * ahead(a, k, 1.0)
         k *= 2
     local[...] = b
     prod[...] = a
-    values = split3(dec[0:1] * b[0:1]) + split3(dec[0:1] * a[0:1])
-    values = values + (None, None) + split3(st[n - 1 : n])
-    tail = out.shape[1] - rows
-    line = lax.broadcasted_iota(jnp.int32, (tail, st.shape[1]), 0)
-    extra = jnp.zeros((tail, st.shape[1]), F32)
-    for k, v in enumerate(values):
-        if v is not None:
-            extra = jnp.where(line == k, jnp.broadcast_to(v, extra.shape), extra)
-    extra = extra.astype(BF16)
-    for d in range(dests):
-        out[d, rows : rows + tail, :] = extra
-    (sent,) = copies(((out, out_h),), sems.at[pl.ds(4, 1)])
-    sent.wait()
 
 
 def finish_body(place, got, local, prod, states, proj, drive, ddecay):
@@ -325,16 +365,18 @@
     block = pltpu.VMEM((tokens, cols), BF16)
     send, pick = call(
         functools.partial(dispatch_body, n_sp, cap),
-        [shape((n_sp * cap, cols), BF16), shape((n_sp * cap, tokens), BF16)],
+        [shape((n_sp * half, width), BF16), shape((n_sp * cap, tokens), BF16)],
         place, route_ids.T, route_weights.T, mixer_out, out_grad,
-        specs=(0, 1, 2, 3), outs_in=(0,),
+        specs=(0, 1, 2, 3), outs_in=(0, 1),
         scratch=[
             *small, block, block,
-            pltpu.VMEM((n_sp * cap, cols), BF16), pltpu.SemaphoreType.DMA((6,)),
+            pltpu.VMEM((n_sp * half, width), BF16),
+            pltpu.VMEM((n_sp * cap, tokens), BF16),
+            pltpu.SemaphoreType.DMA((9,)),
         ],
     )
-    own = lax.all_to_all(send.reshape(n_sp, cap, cols), SP, 0, 0, tiled=True)
-    own = own.reshape(n_sp * cap, cols)
+    own = lax.all_to_all(send.reshape(n_sp, half, width), SP, 0, 0, tiled=True)
+    own = own.reshape(n_sp * half, width)
 
     def cut(*refs):
         w, (lo, hi) = refs[:3], refs[3:]
@@ -350,23 +392,36 @@
     par = lax.ppermute(own, "c", swap)
 
     units = hidden + 2 * q
-    gated = call(prep_body, shape((tokens, ch), BF16), place, gate_branch, states)
+    tail = 16
+    gated, weight, tails = call(
+        prep_body,
+        [shape((tokens, ch), BF16), shape((tokens, ch), F32), shape((tail, ch), F32)],
+        place, gate_branch, states, decay,
+    )
 
     slots = n_sp * half
     wide = cols // n_y
-    psend, pkeep, mix = call(
-        functools.partial(expert_body, half),
-        [
-            shape((n_y, slots, wide), BF16),
-            shape((n_y, slots, wide), F32),
-            shape((n_sp * cap, 3 * units), BF16),
+    held = pltpu.VMEM((3, units, cols), BF16)
+    weights = (wg, wu, wd, wa, wb)
+    part = call(
+        first_body, shape((3, slots, units), F32), place, own, *weights,
+        specs=(1, 2, 3, 4, 5), scratch=[held, pltpu.SemaphoreType.DMA((9,))],
+    )
+    psend, mix = call(
+        expert_body,
+        [shape((n_y, slots, wide), BF16), shape((slots, 3 * units), BF16)],
+        place, par, part, *weights,
+        specs=(2, 3, 4, 5, 6), outs_in=(1,),
+        scratch=[
+            held, pltpu.VMEM((slots, 3 * units), BF16), pltpu.SemaphoreType.DMA((10,)),
         ],
-        place, own, par, wg, wu, wd, wa, wb,
-        specs=(2, 3, 4, 5, 6), outs_in=(2,),
+    )
+    pkeep = call(
+        keep_body, shape((n_y, slots, wide), F32), place, mix, *weights,
+        specs=(0, 1, 2, 3, 4, 5),
         scratch=[
-            pltpu.VMEM((3, units, width), BF16),
-            pltpu.VMEM((n_sp * cap, 3 * units), BF16),
-            pltpu.SemaphoreType.DMA((10,)),
+            pltpu.VMEM((2, units, cols), BF16), pltpu.VMEM((slots, 2 * units), BF16),
+            pltpu.SemaphoreType.DMA((7,)),
         ],
     )
     precv = lax.ppermute(psend, "c", swap)
@@ -390,32 +445,34 @@
         combine_body,
         shape((tokens, ch), BF16),
         place, pick, back.reshape(n_sp * cap, wide), out_grad,
-        specs=(2,),
-        scratch=[pltpu.VMEM((tokens, ch), BF16), pltpu.SemaphoreType.DMA((1,))],
+        specs=(0, 2),
+        scratch=[
+            pltpu.VMEM((n_sp * cap, tokens), BF16), pltpu.VMEM((tokens, ch), BF16),
+            pltpu.SemaphoreType.DMA((2,)),
+        ],
     )
     mid = lax.all_gather(mid, TP)
 
     rows = width // n_sp
-    out, branch, loc, prod = call(
+    row = lambda t: shape((tokens, ch), t)
+    out, act = call(
         project_body,
-        [
-            shape((n_sp, rows + 16, ch), BF16),
-            shape((tokens, ch), BF16),
-            shape((tokens, ch), F32),
-            shape((tokens, ch), F32),
+        [shape((n_sp, rows + tail, ch), BF16), row(F32)],
+        place, mid, gated, w_proj, weight, tails,
+        specs=(1, 2, 3, 4), outs_in=(0,),
+        scratch=[
+            pltpu.VMEM((tokens, ch), BF16), pltpu.VMEM((width, ch), BF16),
+            pltpu.VMEM((tokens, ch), F32), pltpu.VMEM((tail, ch), F32),
+            pltpu.VMEM((n_sp, rows + tail, ch), BF16), pltpu.SemaphoreType.DMA((6,)),
         ],
-        place, mid, gated, w_proj, gate_branch, states, decay,
-        specs=(2, 3, 4, 5), outs_in=(0,),
-        scratch=[
-            pltpu.VMEM((width, ch), BF16), pltpu.VMEM((tokens, ch), BF16),
-            pltpu.VMEM((tokens, ch), F32), pltpu.VMEM((tokens, ch), F32),
-            pltpu.VMEM((n_sp, rows + 16, ch), BF16), pltpu.SemaphoreType.DMA((5,)),
-        ],
+    )
+    branch, loc, prod = call(
+        scan_body, [row(BF16), row(F32), row(F32)],
+        place, act, gate_branch, states, decay,
     )
     got = lax.all_to_all(out, SP, 0, 0, tiled=True)
     proj, drive, ddecay = call(
-        finish_body,
-        [shape((rows, ch), F32), shape((tokens, ch), F32), shape((tokens, ch), F32)],
+        finish_body, [shape((rows, ch), F32), row(F32), row(F32)],
         place, got, loc, prod, states,
     )
 

time: 187 us -> 187 us (level)
  waiting for transfers between devices: 56.7 us -> 52.3 us
    all_to_all x1, waiting for transfers between devices: 7.99 us -> 6.1 us  [local(): back = lax.all_to_all(ret, SP, 0, 0, tiled=True)]
    ppermute x1, waiting for transfers between devices: 1.88 us -> 0.01 us  [local(): precv = lax.ppermute(psend, 'c', swap)]
    pallas_call x8 -> x11, Pallas kernels: 22.8 us -> 24.3 us  [call(): pl.pallas_call(body, grid_spec=pltpu.PrefetchScalarGridSpec(num_scalar_pr...]
  transfers between devices with their start and end apart: 9 -> 9, of which waited for: 6 -> 5; matrix products, arithmetic and copies ran while one was open for 1% -> 2% of each run, Pallas kernels for 6% -> 9%
where the time goes in v2:
time: 187 us; the launch traced here: 186 us
  blocking collectives  63.1 us (34%)
  waiting for transfers between devices  52.3 us (28%)
  starting transfers between devices  36.3 us (19%)
  Pallas kernels  24.5 us (13%)
  local copies, waits for them, and re-layouts  6.13 us (3%)
  other arithmetic  2.41 us (1%)
    all_to_all x1, blocking collectives, local(): own = lax.all_to_all(send.reshape(n_sp, half, width), SP, 0, 0, tiled=True)  41.2 us
    pallas_call x11, Pallas kernels, call(): pl.pallas_call(body, grid_spec=pltpu.PrefetchScalarGridSpec(num_scalar_pr...  24.3 us
    all_gather x1, blocking collectives, local(): mid = lax.all_gather(mid, TP)  21.9 us
    ppermute x1, waiting for transfers between devices, local(): wa = lax.ppermute(w_lo, Y, ring(1))  16 us
    all_to_all x1, waiting for transfers between devices, local(): got = lax.all_to_all(out, SP, 0, 0, tiled=True)  15.8 us
    all_to_all x1, waiting for transfers between devices, local(): parts = lax.all_to_all(psum, Y, 0, 0, tiled=True)  11.2 us
    all_to_all x1, starting transfers between devices, local(): got = lax.all_to_all(out, SP, 0, 0, tiled=True)  9.5 us
    all_to_all x1, starting transfers between devices, local(): parts = lax.all_to_all(psum, Y, 0, 0, tiled=True)  7.75 us
  transfers between devices with their start and end apart: 9, of which 5 were waited for; matrix products, arithmetic and copies ran while one was open for 2% of the time, Pallas kernels for 9%

profile of v2, /device:TPU:8, one launch (start us, length us, event | category | flops | bytes accessed | tf_op | source)
XLA Modules:
  0.0 185.8 jit_solution(14173574742987416258)
XLA Ops:
  0.6 0.0 copy-start.2
  0.6 0.0 copy-start.1
  0.7 0.0 copy-start
  0.7 0.1 pad_add_fusion.place
  0.8 3.0 %shard_map.162 = (bf16[256,2048]{1,0:T(8,128)(2,1)}, bf16[512,128]{1,0:T(8,128)(2,1)}) custom-call(s32[4]{0:T(128)S(1)} %pad_add_fusion.place, s32[2,128]{1,0:T(2,128)} %bitcast.37, f32[2,128]{1,0:T(2,128)} %bitcast.38, bf16[128,2048]{1,0:T(8,128)(2,1)} %x_h.1, bf16[128,2048]{1,0:T(8,128)(2,1)} %og_h.3), custom_call_target="tpu_custom_call" | custom-call | tf_op jit(solution)/shard_map/pallas_call | solution.py:69
  3.7 41.2 %all_to_all.20 = bf16[32,8,2048]{2,1,0:T(8,128)(2,1)S(1)} all-to-all(bf16[32,8,2048]{2,1,0:T(8,128)(2,1)} %bitcast.36), channel_id=1, replica_groups=mesh['z'=8,'x'=4,'yh'=4,'yl'=2,'c'=2] {'z','x'}, dimensions={0} | all-to-all | bytes 2097152 | tf_op jit(solution)/shard_map/all_to_all | solution.py:378
  45.0 1.9 %collective-permute-start = (bf16[256,2048]{1,0:T(8,128)(2,1)S(1)}, bf16[256,2048]{1,0:T(8,128)(2,1)S(1)}, u32[]{:S(2)}, u32[]{:S(2)}) collective-permute-start(bf16[256,2048]{1,0:T(8,128)(2,1)S(1)} %bitcast.19), channel_id=1, source_target_pairs={{0,1},{1,0},{2,3},{3,2},{4,5},{5,4},{6,7},{7,6},{8,9},{9,8},{10,11... | collective-permute-start | bytes 3145736 | tf_op jit(solution)/shard_map/ppermute | solution.py:392
  46.9 0.0 copy-done.2
  46.9 0.0 copy-done.1
  46.9 0.0 copy-done
  46.9 0.2 shard_map.163
  47.1 3.5 %collective-permute-start.1 = (bf16[192,2048]{1,0:T(8,128)(2,1)S(1)}, bf16[192,2048]{1,0:T(8,128)(2,1)S(1)}, u32[]{:S(2)}, u32[]{:S(2)}) collective-permute-start(bf16[192,2048]{1,0:T(8,128)(2,1)S(1)} %get-tuple-element.28), channel_id=1, source_target_pairs={{0,2},{2,4},{4,6},{6,8},{8,10},{10,12},{12,14},{14,0},{1,3},{3,5},... | collective-permute-start | bytes 2359304 | tf_op jit(solution)/shard_map/ppermute | solution.py:390
  50.6 2.4 %collective-permute-start.2 = (bf16[192,2048]{1,0:T(8,128)(2,1)S(1)}, bf16[192,2048]{1,0:T(8,128)(2,1)S(1)}, u32[]{:S(2)}, u32[]{:S(2)}) collective-permute-start(bf16[192,2048]{1,0:T(8,128)(2,1)S(1)} %get-tuple-element.29), channel_id=1, source_target_pairs={{0,14},{2,0},{4,2},{6,4},{8,6},{10,8},{12,10},{14,12},{1,15},{3,1}... | collective-permute-start | bytes 2359304 | tf_op jit(solution)/shard_map/ppermute | solution.py:391
  52.9 16.0 %collective-permute-done.1.wa = bf16[192,2048]{1,0:T(8,128)(2,1)S(1)} collective-permute-done((bf16[192,2048]{1,0:T(8,128)(2,1)S(1)}, bf16[192,2048]{1,0:T(8,128)(2,1)S(1)}, u32[]{:S(2)}, u32[]{:S(2)}) %collective-permute-start.1) | collective-permute-done | bytes 786464 | tf_op jit(solution)/shard_map/ppermute | solution.py:390
  68.9 3.2 %collective-permute-done.2.wb = bf16[192,2048]{1,0:T(8,128)(2,1)S(1)} collective-permute-done((bf16[192,2048]{1,0:T(8,128)(2,1)S(1)}, bf16[192,2048]{1,0:T(8,128)(2,1)S(1)}, u32[]{:S(2)}, u32[]{:S(2)}) %collective-permute-start.2) | collective-permute-done | bytes 786464 | tf_op jit(solution)/shard_map/ppermute | solution.py:391
  72.1 0.0 copy-done.13
  72.1 0.9 copy-done.14
  73.0 2.9 %shard_map.164.part = f32[3,256,256]{2,1,0:T(8,128)S(1)} custom-call(s32[4]{0:T(128)S(1)} %pad_add_fusion.place, bf16[256,2048]{1,0:T(8,128)(2,1)S(1)} %bitcast.20, bf16[128,2048]{1,0:T(8,128)(2,1)} %bitcast.22, bf16[128,2048]{1,0:T(8,128)(2,1)} %bitcast.26, bf16[128,2048]{1,0:T(8,128)(2,1)} %bitcast.30, bf16[192,2048]{1,0:T(8,128)(2,1)} %copy-done.13, ...), custom_call_target="tpu_custom_call" | custom-call | tf_op jit(solution)/shard_map/pallas_call | solution.py:69
  76.0 0.0 collective-permute-done.par
  76.0 0.0 copy-start.3
  76.0 3.7 %shard_map.165 = (bf16[8,256,128]{2,1,0:T(8,128)(2,1)S(1)}, bf16[256,768]{1,0:T(8,128)(2,1)}) custom-call(s32[4]{0:T(128)S(1)} %pad_add_fusion.place, bf16[256,2048]{1,0:T(8,128)(2,1)S(1)} %collective-permute-done.par, f32[3,256,256]{2,1,0:T(8,128)S(1)} %shard_map.164.part, bf16[128,2048]{1,0:T(8,128)(2,1)} %bitcast.23, bf16[128,2048]{1,0:T(8,128)(2,1)} %bitcast.27, ...), custom_call_target="tpu_custom_call" | custom-call | tf_op jit(solution)/shard_map/pallas_call | solution.py:69
  79.7 1.9 %collective-permute-start.5 = (bf16[8,256,128]{2,1,0:T(8,128)(2,1)S(1)}, bf16[8,256,128]{2,1,0:T(8,128)(2,1)S(1)}, u32[]{:S(2)}, u32[]{:S(2)}) collective-permute-start(bf16[8,256,128]{2,1,0:T(8,128)(2,1)S(1)} %get-tuple-element.35), channel_id=1, source_target_pairs={{0,1},{1,0},{2,3},{3,2},{4,5},{5,4},{6,7},{7,6},{8,9},{9,8},{10,11... | collective-permute-start | bytes 1572872 | tf_op jit(solution)/shard_map/ppermute | solution.py:427
  81.7 0.0 copy-start.5
  81.7 2.3 %shard_map.167 = f32[8,256,128]{2,1,0:T(8,128)S(1)} custom-call(s32[4]{0:T(128)S(1)} %pad_add_fusion.place, bf16[256,768]{1,0:T(8,128)(2,1)} %get-tuple-element.30.mix.mix_h, bf16[128,2048]{1,0:T(8,128)(2,1)} %bitcast.24, bf16[128,2048]{1,0:T(8,128)(2,1)} %bitcast.28, bf16[128,2048]{1,0:T(8,128)(2,1)} %bitcast.32, bf16[192,2048]{1,0:T(8,128)(2,1)} %copy-done.13, ...), custom_call_target="tpu_custom_call" | custom-call | tf_op jit(solution)/shard_map/pallas_call | solution.py:69
  84.0 0.0 copy-done.3
  84.0 0.0 copy-start.6
  84.0 0.0 copy-start.7
  84.0 0.0 copy-start.8
  84.0 0.0 collective-permute-done.5
  84.0 0.0 copy-start.4
  84.0 0.9 add_convert_fusion
  85.0 7.7 %all-to-all-start.1 = ((bf16[8,256,128]{2,1,0:T(8,128)(2,1)}), bf16[8,256,128]{2,1,0:T(8,128)(2,1)S(1)}, u32[]{:S(2)}, u32[]{:S(2)}) async-start(bf16[8,256,128]{2,1,0:T(8,128)(2,1)} %add_convert_fusion), calls=%async_computation.1 | async-start | bytes 1048576 | tf_op jit(solution)/shard_map/all_to_all | solution.py:441
  92.7 0.0 copy-done.5
  92.7 0.0 copy-done.4
  92.7 3.4 %shard_map.166 = (f32[384,2048]{1,0:T(8,128)}, bf16[192,2048]{1,0:T(8,128)(2,1)}, bf16[192,2048]{1,0:T(8,128)(2,1)S(1)}) custom-call(s32[4]{0:T(128)S(1)} %pad_add_fusion.place, bf16[256,2048]{1,0:T(8,128)(2,1)S(1)} %bitcast.21, bf16[256,2048]{1,0:T(8,128)(2,1)S(1)} %copy-done.4, bf16[256,768]{1,0:T(8,128)(2,1)S(1)} %copy-done.5), custom_call_target="tpu_custom_call" | custom-call | tf_op jit(solution)/shard_map/pallas_call | solution.py:69
  96.2 0.0 copy-start.12
  96.2 0.9 copy-done.12
  97.0 1.9 %collective-permute-start.3 = (bf16[192,2048]{1,0:T(8,128)(2,1)}, bf16[192,2048]{1,0:T(8,128)(2,1)}, u32[]{:S(2)}, u32[]{:S(2)}) collective-permute-start(bf16[192,2048]{1,0:T(8,128)(2,1)} %get-tuple-element.32), channel_id=1, source_target_pairs={{0,14},{2,0},{4,2},{6,4},{8,6},{10,8},{12,10},{14,12},{1,15},{3,1}... | collective-permute-start | bytes 2359304 | tf_op jit(solution)/shard_map/ppermute | solution.py:437
  99.0 11.2 %all-to-all-done.1.parts = bf16[8,256,128]{2,1,0:T(8,128)(2,1)S(1)} async-done(((bf16[8,256,128]{2,1,0:T(8,128)(2,1)}), bf16[8,256,128]{2,1,0:T(8,128)(2,1)S(1)}, u32[]{:S(2)}, u32[]{:S(2)}) %all-to-all-start.1) | async-done | bytes 524320 | tf_op jit(solution)/shard_map/all_to_all | solution.py:441
  110.2 1.3 shard_map.168
  111.4 5.6 %all-to-all-start.2 = ((bf16[32,16,128]{2,1,0:T(8,128)(2,1)}), bf16[32,16,128]{2,1,0:T(8,128)(2,1)S(1)}, u32[]{:S(2)}, u32[]{:S(2)}) async-start(bf16[32,16,128]{2,1,0:T(8,128)(2,1)} %shard_map.168), calls=%async_computation.2 | async-start | bytes 262144 | tf_op jit(solution)/shard_map/all_to_all | solution.py:443
  117.0 1.9 %collective-permute-start.4 = (bf16[192,2048]{1,0:T(8,128)(2,1)}, bf16[192,2048]{1,0:T(8,128)(2,1)}, u32[]{:S(2)}, u32[]{:S(2)}) collective-permute-start(bf16[192,2048]{1,0:T(8,128)(2,1)} %copy-done.12), channel_id=1, source_target_pairs={{0,2},{2,4},{4,6},{6,8},{8,10},{10,12},{12,14},{14,0},{1,3},{3,5},... | collective-permute-start | bytes 2359304 | tf_op jit(solution)/shard_map/ppermute | solution.py:438
  118.9 0.0 copy-done.6
  118.9 0.0 copy-done.7
  119.0 0.0 copy-done.8
  119.0 0.6 shard_map.170
  119.6 0.0 copy-start.9
  119.6 0.6 copy-done.9
  120.2 0.6 copy-done.10
  120.8 0.6 copy-done.11
  121.4 6.1 %all-to-all-done.2 = bf16[32,16,128]{2,1,0:T(8,128)(2,1)S(1)} async-done(((bf16[32,16,128]{2,1,0:T(8,128)(2,1)}), bf16[32,16,128]{2,1,0:T(8,128)(2,1)S(1)}, u32[]{:S(2)}, u32[]{:S(2)}) %all-to-all-start.2) | async-done | bytes 131104 | tf_op jit(solution)/shard_map/all_to_all | solution.py:443
  127.5 1.7 shard_map.169
  129.2 21.9 %all-gather = bf16[2048,128]{1,0:T(8,128)(2,1)S(1)} all-gather(bf16[128,128]{1,0:T(8,128)(2,1)S(1)} %shard_map.169), channel_id=2, replica_groups=mesh['z'=8,'x'=4,'yh'=4,'yl'=2,'c'=2] {'yh','yl','c'}, dimensions={0}, use_global_device_ids=true | all-gather | bytes 557056 | tf_op jit(solution)/shard_map/all_gather | solution.py:454
  151.1 2.9 %shard_map.171 = (bf16[32,80,128]{2,1,0:T(8,128)(2,1)}, f32[128,128]{1,0:T(8,128)S(1)}) custom-call(s32[4]{0:T(128)S(1)} %pad_add_fusion.place, bf16[16,128,128]{2,1,0:T(8,128)(2,1)S(1)} %bitcast.34, bf16[128,128]{1,0:T(8,128)(2,1)} %copy-done.10, bf16[2048,128]{1,0:T(8,128)(2,1)} %w_h.1, f32[128,128]{1,0:T(8,128)} %copy-done.9, f32[16,128]{1,0:T(8,128)} %copy-done.11), custom_call_target="tpu_custom_call" | custom-call | tf_op jit(solution)/shard_map/pallas_call | solution.py:69
  154.0 9.5 %all-to-all-start.3 = ((bf16[32,80,128]{2,1,0:T(8,128)(2,1)}), bf16[32,80,128]{2,1,0:T(8,128)(2,1)S(1)}, u32[]{:S(2)}, u32[]{:S(2)}) async-start(bf16[32,80,128]{2,1,0:T(8,128)(2,1)} %get-tuple-element.39), calls=%async_computation.3 | async-start | bytes 1310720 | tf_op jit(solution)/shard_map/all_to_all | solution.py:473
  163.5 0.0 copy-start.15
  163.5 0.0 collective-permute-done.3
  163.5 1.3 fusion.3
  164.9 0.0 collective-permute-done.4
  164.9 1.2 fusion.4
  166.0 1.4 fusion.2
  167.5 1.2 shard_map.172
  168.6 15.8 %all-to-all-done.3.got = bf16[32,80,128]{2,1,0:T(8,128)(2,1)S(1)} async-done(((bf16[32,80,128]{2,1,0:T(8,128)(2,1)}), bf16[32,80,128]{2,1,0:T(8,128)(2,1)S(1)}, u32[]{:S(2)}, u32[]{:S(2)}) %all-to-all-start.3) | async-done | bytes 655392 | tf_op jit(solution)/shard_map/all_to_all | solution.py:473
  184.4 1.4 shard_map.173
  (5 shorter events, 0.0 us)
Async XLA Ops:
  0.6 46.2 %copy-start.2 = (bf16[1,128,2048]{2,1,0:T(8,128)(2,1)S(1)}, bf16[1,128,2048]{2,1,0:T(8,128)(2,1)}, u32[]{:S(2)}) copy-start(bf16[1,128,2048]{2,1,0:T(8,128)(2,1)} %param.21) | copy-start | bytes 1572868
  0.6 46.2 %copy-start.1 = (bf16[1,128,2048]{2,1,0:T(8,128)(2,1)S(1)}, bf16[1,128,2048]{2,1,0:T(8,128)(2,1)}, u32[]{:S(2)}) copy-start(bf16[1,128,2048]{2,1,0:T(8,128)(2,1)} %param.20) | copy-start | bytes 1572868
  0.7 46.2 %copy-start = (bf16[1,128,2048]{2,1,0:T(8,128)(2,1)S(1)}, bf16[1,128,2048]{2,1,0:T(8,128)(2,1)}, u32[]{:S(2)}) copy-start(bf16[1,128,2048]{2,1,0:T(8,128)(2,1)} %param.19) | copy-start | bytes 1572868
  45.0 31.0 %collective-permute-start = (bf16[256,2048]{1,0:T(8,128)(2,1)S(1)}, bf16[256,2048]{1,0:T(8,128)(2,1)S(1)}, u32[]{:S(2)}, u32[]{:S(2)}) collective-permute-start(bf16[256,2048]{1,0:T(8,128)(2,1)S(1)} %bitcast.19), channel_id=1, source_target_pairs={{0,1},{1,0},{2,3},{3,2},{4,5},{5,4},{6,7},{7,6},{8,9},{9,8},{10,11... | collective-permute-start | bytes 3145736 | tf_op jit(solution)/shard_map/ppermute | solution.py:392
  47.1 21.8 %collective-permute-start.1 = (bf16[192,2048]{1,0:T(8,128)(2,1)S(1)}, bf16[192,2048]{1,0:T(8,128)(2,1)S(1)}, u32[]{:S(2)}, u32[]{:S(2)}) collective-permute-start(bf16[192,2048]{1,0:T(8,128)(2,1)S(1)} %get-tuple-element.28), channel_id=1, source_target_pairs={{0,2},{2,4},{4,6},{6,8},{8,10},{10,12},{12,14},{14,0},{1,3},{3,5},... | collective-permute-start | bytes 2359304 | tf_op jit(solution)/shard_map/ppermute | solution.py:390
  50.6 21.6 %collective-permute-start.2 = (bf16[192,2048]{1,0:T(8,128)(2,1)S(1)}, bf16[192,2048]{1,0:T(8,128)(2,1)S(1)}, u32[]{:S(2)}, u32[]{:S(2)}) collective-permute-start(bf16[192,2048]{1,0:T(8,128)(2,1)S(1)} %get-tuple-element.29), channel_id=1, source_target_pairs={{0,14},{2,0},{4,2},{6,4},{8,6},{10,8},{12,10},{14,12},{1,15},{3,1}... | collective-permute-start | bytes 2359304 | tf_op jit(solution)/shard_map/ppermute | solution.py:391
  68.9 3.2 %copy-start.13 = (bf16[192,2048]{1,0:T(8,128)(2,1)}, bf16[192,2048]{1,0:T(8,128)(2,1)S(1)}, u32[]{:S(2)}) copy-start(bf16[192,2048]{1,0:T(8,128)(2,1)S(1)} %collective-permute-done.1.wa) | copy-start | bytes 2359300
  72.1 0.9 copy-start.14
  76.0 8.0 %copy-start.3 = (bf16[256,2048]{1,0:T(8,128)(2,1)}, bf16[256,2048]{1,0:T(8,128)(2,1)S(1)}, u32[]{:S(2)}) copy-start(bf16[256,2048]{1,0:T(8,128)(2,1)S(1)} %collective-permute-done.par) | copy-start | bytes 3145732
  79.7 4.3 %collective-permute-start.5 = (bf16[8,256,128]{2,1,0:T(8,128)(2,1)S(1)}, bf16[8,256,128]{2,1,0:T(8,128)(2,1)S(1)}, u32[]{:S(2)}, u32[]{:S(2)}) collective-permute-start(bf16[8,256,128]{2,1,0:T(8,128)(2,1)S(1)} %get-tuple-element.35), channel_id=1, source_target_pairs={{0,1},{1,0},{2,3},{3,2},{4,5},{5,4},{6,7},{7,6},{8,9},{9,8},{10,11... | collective-permute-start | bytes 1572872 | tf_op jit(solution)/shard_map/ppermute | solution.py:427
  81.7 11.1 %copy-start.5 = (bf16[256,768]{1,0:T(8,128)(2,1)S(1)}, bf16[256,768]{1,0:T(8,128)(2,1)}, u32[]{:S(2)}) copy-start(bf16[256,768]{1,0:T(8,128)(2,1)} %get-tuple-element.30.mix.mix_h) | copy-start | bytes 1179652
  84.0 34.9 %copy-start.6 = (f32[128,128]{1,0:T(8,128)S(1)}, f32[128,128]{1,0:T(8,128)}, u32[]{:S(2)}) copy-start(f32[128,128]{1,0:T(8,128)} %states.5) | copy-start | bytes 196612
  84.0 34.9 %copy-start.7 = (f32[128,128]{1,0:T(8,128)S(1)}, f32[128,128]{1,0:T(8,128)}, u32[]{:S(2)}) copy-start(f32[128,128]{1,0:T(8,128)} %decay.3) | copy-start | bytes 196612
  84.0 34.9 %copy-start.8 = (bf16[128,128]{1,0:T(8,128)(2,1)S(1)}, bf16[128,128]{1,0:T(8,128)(2,1)}, u32[]{:S(2)}) copy-start(bf16[128,128]{1,0:T(8,128)(2,1)} %gate.3) | copy-start | bytes 98308
  84.0 8.7 %copy-start.4 = (bf16[256,2048]{1,0:T(8,128)(2,1)S(1)}, bf16[256,2048]{1,0:T(8,128)(2,1)}, u32[]{:S(2)}) copy-start(bf16[256,2048]{1,0:T(8,128)(2,1)} %copy-done.3) | copy-start | bytes 3145732
  85.0 25.2 %all-to-all-start.1 = ((bf16[8,256,128]{2,1,0:T(8,128)(2,1)}), bf16[8,256,128]{2,1,0:T(8,128)(2,1)S(1)}, u32[]{:S(2)}, u32[]{:S(2)}) async-start(bf16[8,256,128]{2,1,0:T(8,128)(2,1)} %add_convert_fusion), calls=%async_computation.1 | async-start | bytes 1048576 | tf_op jit(solution)/shard_map/all_to_all | solution.py:441
  96.2 0.9 copy-start.12
  97.0 66.5 %collective-permute-start.3 = (bf16[192,2048]{1,0:T(8,128)(2,1)}, bf16[192,2048]{1,0:T(8,128)(2,1)}, u32[]{:S(2)}, u32[]{:S(2)}) collective-permute-start(bf16[192,2048]{1,0:T(8,128)(2,1)} %get-tuple-element.32), channel_id=1, source_target_pairs={{0,14},{2,0},{4,2},{6,4},{8,6},{10,8},{12,10},{14,12},{1,15},{3,1}... | collective-permute-start | bytes 2359304 | tf_op jit(solution)/shard_map/ppermute | solution.py:437
  111.4 16.1 %all-to-all-start.2 = ((bf16[32,16,128]{2,1,0:T(8,128)(2,1)}), bf16[32,16,128]{2,1,0:T(8,128)(2,1)S(1)}, u32[]{:S(2)}, u32[]{:S(2)}) async-start(bf16[32,16,128]{2,1,0:T(8,128)(2,1)} %shard_map.168), calls=%async_computation.2 | async-start | bytes 262144 | tf_op jit(solution)/shard_map/all_to_all | solution.py:443
  117.0 47.9 %collective-permute-start.4 = (bf16[192,2048]{1,0:T(8,128)(2,1)}, bf16[192,2048]{1,0:T(8,128)(2,1)}, u32[]{:S(2)}, u32[]{:S(2)}) collective-permute-start(bf16[192,2048]{1,0:T(8,128)(2,1)} %copy-done.12), channel_id=1, source_target_pairs={{0,2},{2,4},{4,6},{6,8},{8,10},{10,12},{12,14},{14,0},{1,3},{3,5},... | collective-permute-start | bytes 2359304 | tf_op jit(solution)/shard_map/ppermute | solution.py:438
  119.6 0.6 copy-start.9
  120.2 0.6 copy-start.10
  120.8 0.6 copy-start.11
  154.0 30.4 %all-to-all-start.3 = ((bf16[32,80,128]{2,1,0:T(8,128)(2,1)}), bf16[32,80,128]{2,1,0:T(8,128)(2,1)S(1)}, u32[]{:S(2)}, u32[]{:S(2)}) async-start(bf16[32,80,128]{2,1,0:T(8,128)(2,1)} %get-tuple-element.39), calls=%async_computation.3 | async-start | bytes 1310720 | tf_op jit(solution)/shard_map/all_to_all | solution.py:473
  163.5 2.5 %copy-start.15 = (f32[384,2048]{1,0:T(8,128)S(1)}, f32[384,2048]{1,0:T(8,128)}, u32[]{:S(2)}) copy-start(f32[384,2048]{1,0:T(8,128)} %get-tuple-element.31) | copy-start | bytes 9437188

commit v3 on v2

--- a/solution.py
+++ b/solution.py
@@ -54,7 +54,7 @@
     )(*args)
 
 
-def call(body, out_shape, place, *args, specs=None, outs_in=None, scratch=(), vmem=VMEM):
+def call(body, out_shape, place, *args, specs=None, free=(), outs_in=None, scratch=(), vmem=VMEM):
     whole = lambda a: pl.BlockSpec(a.shape, lambda i, s, n=len(a.shape): (0,) * n)
     outs = out_shape if isinstance(out_shape, (list, tuple)) else [out_shape]
     in_specs = [whole(a) for a in args]
@@ -63,6 +63,8 @@
     for k in specs or ():
         in_specs[k] = pl.BlockSpec(memory_space=pltpu.HBM)
         args[k] = pltpu.with_memory_space_constraint(args[k], pltpu.HBM)
+    for k in free:
+        in_specs[k] = pl.BlockSpec(memory_space=pl.ANY)
     for k in outs_in or ():
         out_specs[k] = pl.BlockSpec(memory_space=pltpu.HBM)
         outs[k] = pltpu.HBM(outs[k].shape, outs[k].dtype)
@@ -104,11 +106,6 @@
     position = jnp.where(named > 0.0, position, -1.0)
     slot = lax.broadcasted_iota(jnp.int32, (experts, half, n), 1).astype(F32)
     at = lambda first: jnp.where(position[:, None, :] == slot + first, 1.0, 0.0).astype(F32)
-    pick[...] = (
-        jnp.concatenate([at(0.0), at(float(half))], axis=1)
-        .reshape(experts * cap, n)
-        .astype(BF16)
-    )
     hot = at((place[1] * half).astype(F32))
     scale = jnp.sum(hot * wt[:, None, :], axis=2, keepdims=True).reshape(experts * half, 1)
     hot = hot.reshape(experts * half, n).astype(BF16)
@@ -126,6 +123,11 @@
             )
             copy.start()
             out.append(copy)
+    pick[...] = (
+        jnp.concatenate([at(0.0), at(float(half))], axis=1)
+        .reshape(experts * cap, n)
+        .astype(BF16)
+    )
     kept = pltpu.make_async_copy(pick, pick_h, sems.at[8])
     kept.start()
     for copy in (*out, kept):
@@ -138,9 +140,12 @@
     return a, b, (v - a - b).astype(BF16).astype(F32)
 
 
-def prep_body(place, gate, states, decay, gated, weight, tail):
+def prep_body(place, gate, states, gated):
+    gated[...] = (gate[...].astype(F32) * states[...]).astype(BF16)
+
+
+def past_body(place, gate, states, decay, weight, tail):
     st, gt, dec = states[...], gate[...].astype(F32), decay[...]
-    gated[...] = (gt * st).astype(BF16)
     n = st.shape[0]
     t = lax.broadcasted_iota(jnp.int32, st.shape, 0)
     prefix, k = dec, 1
@@ -148,13 +153,11 @@
         prefix = prefix * jnp.where(t >= k, pltpu.roll(prefix, k, 0), 1.0)
         k *= 2
     weight[...] = prefix * gt
-    values = split3(prefix[n - 1 : n])
     line = lax.broadcasted_iota(jnp.int32, tail.shape, 0)
     rows = jnp.zeros(tail.shape, F32)
-    for k, v in enumerate(values):
-        rows = jnp.where(line == 3 + k, jnp.broadcast_to(v, tail.shape), rows)
-    for k, v in enumerate(split3(st[n - 1 : n])):
-        rows = jnp.where(line == 8 + k, jnp.broadcast_to(v, tail.shape), rows)
+    for first, value in ((3, prefix[n - 1 : n]), (8, st[n - 1 : n])):
+        for k, v in enumerate(split3(value)):
+            rows = jnp.where(line == first + k, jnp.broadcast_to(v, tail.shape), rows)
     tail[...] = rows
 
 
@@ -196,6 +199,13 @@
         out[k] = p[:, k * width : (k + 1) * width].astype(out.dtype)
 
 
+def activations(gate, up, grad):
+    sig = jax.nn.sigmoid(gate)
+    silu = gate * sig
+    gate_grad = grad * up * sig * (1.0 + gate * (1.0 - sig))
+    return gate_grad.astype(BF16), (grad * silu).astype(BF16), (silu * up).astype(BF16)
+
+
 def expert_body(place, par, part, wg, wu, wd, wa, wb, psend, mix_h, w_s, mix, sems):
     where = columns(1 - place[0], w_s.shape[2])
     loads = copies(weight_copies(wg, wu, wd, wa, wb, w_s, where, 3), sems)
@@ -203,13 +213,10 @@
     gate = part[0] + product(0, par, w_s, loads)
     up = part[1] + product(1, par, w_s, loads)
     grad = part[2] + product(2, par, w_s, loads)
-    sig = jax.nn.sigmoid(gate)
-    silu = gate * sig
-    ub = (grad * silu).astype(BF16)
-    gb = (grad * up * sig * (1.0 + gate * (1.0 - sig))).astype(BF16)
+    gb, ub, hb = activations(gate, up, grad)
     mix[:, 0:units] = gb
     mix[:, units : 2 * units] = ub
-    mix[:, 2 * units :] = (silu * up).astype(BF16)
+    mix[:, 2 * units :] = hb
     (kept,) = copies(((mix, mix_h),), sems.at[pl.ds(9, 1)])
     partials(psend, gb, ub, w_s)
     kept.wait()
@@ -224,25 +231,62 @@
     partials(pkeep, mix[:, 0:units], mix[:, units:], w_s)
 
 
-def weight_body(place, own, par, mix, gown_h, ga, gb, gown, sems):
+def weight_body(place, own, par, mix, gown_h, gown, sems):
     c = place[0]
-    h, q = gown.shape[1] // 3, ga.shape[0] // 3
-    units, cols = h + 2 * q, gown.shape[2]
+    h, cols = gown.shape[1] // 3, gown.shape[2]
+    units = mix.shape[1] // 3
     stored = []
     for n, (src, core) in enumerate(((own, c), (par, 1 - c))):
-        where = columns(core, cols)
         for k in range(3):
             side = src[:, 0:cols] if k < 2 else src[:, cols:]
-            g = tn(mix[:, k * units : (k + 1) * units], side)
             rows = pl.ds(k * h, h)
-            gown[n, rows, :] = g[0:h]
+            gown[n, rows, :] = tn(mix[:, k * units : k * units + h], side)
             copy = pltpu.make_async_copy(
-                gown.at[n, rows], gown_h.at[rows, where], sems.at[3 * n + k]
+                gown.at[n, rows],
+                gown_h.at[rows, columns(core, cols)],
+                sems.at[3 * n + k],
             )
             copy.start()
             stored.append(copy)
-            ga[k * q : (k + 1) * q, where] = g[h : h + q].astype(BF16)
-            gb[k * q : (k + 1) * q, where] = g[h + q :].astype(BF16)
+    for copy in stored:
+        copy.wait()
+
+
+def rest_body(
+    place, xa_h, xb_h, pa_h, pb_h, wg, wu, wd, gown_h, dg_h, du_h, dd_h,
+    own, par, w_s, held, sum_s, sems,
+):
+    c = place[0]
+    rows, h = xa_h.shape[0], wg.shape[0]
+    cols = own.shape[1] // 2
+    top, low = pl.ds(0, rows), pl.ds(rows, rows)
+    loads = copies(
+        (
+            (xa_h, own.at[top]), (xb_h, own.at[low]), (pa_h, par.at[top]),
+            (pb_h, par.at[low]), (wg, w_s.at[0]), (wu, w_s.at[1]), (wd, w_s.at[2]),
+            (gown_h, held),
+        ),
+        sems,
+    )
+    for copy in loads[:7]:
+        copy.wait()
+    mine, other = columns(c, cols), columns(1 - c, cols)
+
+    def pre(k):
+        cut = slice(0, cols) if k < 2 else slice(cols, 2 * cols)
+        return nt(own[:, cut], w_s[k, :, mine]) + nt(par[:, cut], w_s[k, :, other])
+
+    three = activations(pre(0), pre(1), pre(2))
+    loads[7].wait()
+    stored = []
+    for k, to in enumerate((dg_h, du_h, dd_h)):
+        cut = slice(0, cols) if k < 2 else slice(cols, 2 * cols)
+        for src, where in ((own, mine), (par, other)):
+            total = held[k * h : (k + 1) * h, where] + tn(three[k], src[:, cut])
+            sum_s[k, :, where] = total.astype(BF16)
+        copy = pltpu.make_async_copy(sum_s.at[k], to.at[0], sems.at[8 + k])
+        copy.start()
+        stored.append(copy)
     for copy in stored:
         copy.wait()
 
@@ -393,9 +437,9 @@
 
     units = hidden + 2 * q
     tail = 16
-    gated, weight, tails = call(
-        prep_body,
-        [shape((tokens, ch), BF16), shape((tokens, ch), F32), shape((tail, ch), F32)],
+    gated = call(prep_body, shape((tokens, ch), BF16), place, gate_branch, states)
+    weight, tails = call(
+        past_body, [shape((tokens, ch), F32), shape((tail, ch), F32)],
         place, gate_branch, states, decay,
     )
 
@@ -405,37 +449,47 @@
     weights = (wg, wu, wd, wa, wb)
     part = call(
         first_body, shape((3, slots, units), F32), place, own, *weights,
-        specs=(1, 2, 3, 4, 5), scratch=[held, pltpu.SemaphoreType.DMA((9,))],
+        specs=(1, 2, 3), free=(4, 5), scratch=[held, pltpu.SemaphoreType.DMA((9,))],
     )
     psend, mix = call(
         expert_body,
         [shape((n_y, slots, wide), BF16), shape((slots, 3 * units), BF16)],
         place, par, part, *weights,
-        specs=(2, 3, 4, 5, 6), outs_in=(1,),
+        specs=(2, 3, 4), free=(5, 6), outs_in=(1,),
         scratch=[
             held, pltpu.VMEM((slots, 3 * units), BF16), pltpu.SemaphoreType.DMA((10,)),
         ],
     )
     pkeep = call(
         keep_body, shape((n_y, slots, wide), F32), place, mix, *weights,
-        specs=(0, 1, 2, 3, 4, 5),
+        specs=(0, 1, 2, 3), free=(4, 5),
         scratch=[
             pltpu.VMEM((2, units, cols), BF16), pltpu.VMEM((slots, 2 * units), BF16),
             pltpu.SemaphoreType.DMA((7,)),
         ],
     )
     precv = lax.ppermute(psend, "c", swap)
-    gown, ga, gb = call(
-        weight_body,
-        [shape((3 * hidden, width), F32), shape((3 * q, width), BF16), shape((3 * q, width), BF16)],
-        place, own, par, mix,
+    gown = call(
+        weight_body, [shape((3 * hidden, width), F32)], place, own, par, mix,
         outs_in=(0,),
         scratch=[
             pltpu.VMEM((2, 3 * hidden, cols), F32), pltpu.SemaphoreType.DMA((6,)),
         ],
-    )
-    back_lo = lax.ppermute(ga, Y, ring(-1))
-    back_hi = lax.ppermute(gb, Y, ring(1))
+    )[0]
+    xa = lax.ppermute(own[: slots // 2], Y, ring(1))
+    xb = lax.ppermute(own[slots // 2 :], Y, ring(-1))
+    pa = lax.ppermute(xa, "c", swap)
+    pb = lax.ppermute(xb, "c", swap)
+    grads = call(
+        rest_body, [shape((1, hidden, width), BF16)] * 3,
+        place, xa, xb, pa, pb, wg, wu, wd, gown,
+        specs=(4, 5, 6, 7), free=(0, 1, 2, 3), outs_in=(0, 1, 2),
+        scratch=[
+            pltpu.VMEM((slots, width), BF16), pltpu.VMEM((slots, width), BF16),
+            pltpu.VMEM((3, hidden, width), BF16), pltpu.VMEM((3 * hidden, width), F32),
+            pltpu.VMEM((3, hidden, width), BF16), pltpu.SemaphoreType.DMA((11,)),
+        ],
+    )
 
     psum = (pkeep + precv.astype(F32)).astype(BF16)
     parts = lax.all_to_all(psum, Y, 0, 0, tiled=True)
@@ -476,14 +530,7 @@
         place, got, loc, prod, states,
     )
 
-    def total(k):
-        mine = gown[k * hidden : (k + 1) * hidden]
-        other = jnp.concatenate(
-            [back_lo[k * q : (k + 1) * q], back_hi[k * q : (k + 1) * q]], axis=0
-        )
-        return (mine + other.astype(F32)).astype(BF16)[None]
-
-    return (total(0), total(1), total(2), proj, branch, drive, ddecay)
+    return (*grads, proj, branch, drive, ddecay)
 
 
 def solution(mesh):

time: 187 us -> 184 us (0.984)
  the two profiles are of different devices: /device:TPU:8 before, /device:TPU:1 now
where the time goes in v3:
time: 184 us; the launch traced here: 183 us
  blocking collectives  82.7 us (45%)
  starting transfers between devices  35.3 us (19%)
  waiting for transfers between devices  34.3 us (19%)
  Pallas kernels  28.9 us (16%)
    all_to_all x1, blocking collectives, local(): own = lax.all_to_all(send.reshape(n_sp, half, width), SP, 0, 0, tiled=True)  39.9 us
    pallas_call x13, Pallas kernels, call(): pl.pallas_call(body, grid_spec=pltpu.PrefetchScalarGridSpec(num_scalar_pr...  28.7 us
    all_to_all x1, blocking collectives, local(): parts = lax.all_to_all(psum, Y, 0, 0, tiled=True)  24.8 us
    all_gather x1, blocking collectives, local(): mid = lax.all_gather(mid, TP)  18 us
    ppermute x1, waiting for transfers between devices, local(): wa = lax.ppermute(w_lo, Y, ring(1))  16 us
    ppermute x1, waiting for transfers between devices, local(): xa = lax.ppermute(own[:slots // 2], Y, ring(1))  9.91 us
    all_to_all x1, waiting for transfers between devices, local(): back = lax.all_to_all(ret, SP, 0, 0, tiled=True)  7.5 us
    all_to_all x1, starting transfers between devices, local(): back = lax.all_to_all(ret, SP, 0, 0, tiled=True)  5.28 us
  transfers between devices with their start and end apart: 10, of which 4 were waited for; matrix products, arithmetic and copies ran while one was open for 0% of the time, Pallas kernels for 8%

profile of v3, /device:TPU:1, one launch (start us, length us, event | category | flops | bytes accessed | tf_op | source)
XLA Modules:
  0.0 183.3 jit_solution(1684081492657974389)
XLA Ops:
  0.6 0.0 copy-start.1
  0.6 0.0 copy-start.2
  0.7 0.0 copy-start
  0.7 0.1 pad_add_fusion.place
  0.8 3.0 %shard_map.162 = (bf16[256,2048]{1,0:T(8,128)(2,1)}, bf16[512,128]{1,0:T(8,128)(2,1)}) custom-call(s32[4]{0:T(128)S(1)} %pad_add_fusion.place, s32[2,128]{1,0:T(2,128)} %bitcast.38, f32[2,128]{1,0:T(2,128)} %bitcast.39, bf16[128,2048]{1,0:T(8,128)(2,1)} %x_h.1, bf16[128,2048]{1,0:T(8,128)(2,1)} %og_h.3), custom_call_target="tpu_custom_call" | custom-call | tf_op jit(solution)/shard_map/pallas_call | solution.py:71
  3.7 39.9 %all_to_all.20 = bf16[32,8,2048]{2,1,0:T(8,128)(2,1)S(1)} all-to-all(bf16[32,8,2048]{2,1,0:T(8,128)(2,1)} %bitcast.37), channel_id=1, replica_groups=mesh['z'=8,'x'=4,'yh'=4,'yl'=2,'c'=2] {'z','x'}, dimensions={0} | all-to-all | bytes 2097152 | tf_op jit(solution)/shard_map/all_to_all | solution.py:422
  43.6 4.7 %collective-permute-start.4 = (bf16[256,2048]{1,0:T(8,128)(2,1)S(1)}, bf16[256,2048]{1,0:T(8,128)(2,1)S(1)}, u32[]{:S(2)}, u32[]{:S(2)}) collective-permute-start(bf16[256,2048]{1,0:T(8,128)(2,1)S(1)} %bitcast.17), channel_id=1, source_target_pairs={{0,1},{1,0},{2,3},{3,2},{4,5},{5,4},{6,7},{7,6},{8,9},{9,8},{10,11... | collective-permute-start | bytes 3145736 | tf_op jit(solution)/shard_map/ppermute | solution.py:436
  48.4 0.0 copy-done.1
  48.4 0.0 copy-done.2
  48.4 0.0 copy-done
  48.4 0.2 shard_map.163
  48.6 3.2 %collective-permute-start.5 = (bf16[192,2048]{1,0:T(8,128)(2,1)S(1)}, bf16[192,2048]{1,0:T(8,128)(2,1)S(1)}, u32[]{:S(2)}, u32[]{:S(2)}) collective-permute-start(bf16[192,2048]{1,0:T(8,128)(2,1)S(1)} %get-tuple-element.27), channel_id=1, source_target_pairs={{0,2},{2,4},{4,6},{6,8},{8,10},{10,12},{12,14},{14,0},{1,3},{3,5},... | collective-permute-start | bytes 2359304 | tf_op jit(solution)/shard_map/ppermute | solution.py:434
  51.8 3.8 %collective-permute-start.6 = (bf16[192,2048]{1,0:T(8,128)(2,1)S(1)}, bf16[192,2048]{1,0:T(8,128)(2,1)S(1)}, u32[]{:S(2)}, u32[]{:S(2)}) collective-permute-start(bf16[192,2048]{1,0:T(8,128)(2,1)S(1)} %get-tuple-element.28), channel_id=1, source_target_pairs={{0,14},{2,0},{4,2},{6,4},{8,6},{10,8},{12,10},{14,12},{1,15},{3,1}... | collective-permute-start | bytes 2359304 | tf_op jit(solution)/shard_map/ppermute | solution.py:435
  55.6 16.0 %collective-permute-done.5.wa = bf16[192,2048]{1,0:T(8,128)(2,1)S(1)} collective-permute-done((bf16[192,2048]{1,0:T(8,128)(2,1)S(1)}, bf16[192,2048]{1,0:T(8,128)(2,1)S(1)}, u32[]{:S(2)}, u32[]{:S(2)}) %collective-permute-start.5) | collective-permute-done | bytes 786464 | tf_op jit(solution)/shard_map/ppermute | solution.py:434
  71.6 0.9 collective-permute-done.6.wb
  72.5 2.8 %shard_map.164.part = f32[3,256,256]{2,1,0:T(8,128)S(1)} custom-call(s32[4]{0:T(128)S(1)} %pad_add_fusion.place, bf16[256,2048]{1,0:T(8,128)(2,1)S(1)} %bitcast.18, bf16[128,2048]{1,0:T(8,128)(2,1)} %bitcast.20, bf16[128,2048]{1,0:T(8,128)(2,1)} %bitcast.25, bf16[128,2048]{1,0:T(8,128)(2,1)} %bitcast.30, bf16[192,2048]{1,0:T(8,128)(2,1)S(1)} %collective-permute-done.5.wa, ...), custom_call_target="tpu_custom_call" | custom-call | tf_op jit(solution)/shard_map/pallas_call | solution.py:71
  75.3 0.0 collective-permute-done.4.par
  75.3 0.0 copy-start.3
  75.3 3.6 %shard_map.165 = (bf16[8,256,128]{2,1,0:T(8,128)(2,1)S(1)}, bf16[256,768]{1,0:T(8,128)(2,1)}) custom-call(s32[4]{0:T(128)S(1)} %pad_add_fusion.place, bf16[256,2048]{1,0:T(8,128)(2,1)S(1)} %collective-permute-done.4.par, f32[3,256,256]{2,1,0:T(8,128)S(1)} %shard_map.164.part, bf16[128,2048]{1,0:T(8,128)(2,1)} %bitcast.21, bf16[128,2048]{1,0:T(8,128)(2,1)} %bitcast.26, ...), custom_call_target="tpu_custom_call" | custom-call | tf_op jit(solution)/shard_map/pallas_call | solution.py:71
  79.0 3.1 %collective-permute-start.7 = (bf16[8,256,128]{2,1,0:T(8,128)(2,1)S(1)}, bf16[8,256,128]{2,1,0:T(8,128)(2,1)S(1)}, u32[]{:S(2)}, u32[]{:S(2)}) collective-permute-start(bf16[8,256,128]{2,1,0:T(8,128)(2,1)S(1)} %get-tuple-element.34), channel_id=1, source_target_pairs={{0,1},{1,0},{2,3},{3,2},{4,5},{5,4},{6,7},{7,6},{8,9},{9,8},{10,11... | collective-permute-start | bytes 1572872 | tf_op jit(solution)/shard_map/ppermute | solution.py:471
  82.1 0.0 copy-done.3
  82.1 2.2 %shard_map.168 = f32[8,256,128]{2,1,0:T(8,128)S(1)} custom-call(s32[4]{0:T(128)S(1)} %pad_add_fusion.place, bf16[256,768]{1,0:T(8,128)(2,1)} %get-tuple-element.29.mix.mix_h, bf16[128,2048]{1,0:T(8,128)(2,1)} %bitcast.22, bf16[128,2048]{1,0:T(8,128)(2,1)} %bitcast.27, bf16[128,2048]{1,0:T(8,128)(2,1)} %bitcast.32, ...), custom_call_target="tpu_custom_call" | custom-call | tf_op jit(solution)/shard_map/pallas_call | solution.py:71
  84.2 0.0 copy-start.6
  84.2 0.0 copy-start.7
  84.3 0.0 copy-start.8
  84.3 0.0 collective-permute-done.7
  84.3 0.1 add_convert_fusion
  84.4 24.8 %all_to_all.21.parts = bf16[8,256,128]{2,1,0:T(8,128)(2,1)S(1)} all-to-all(bf16[8,256,128]{2,1,0:T(8,128)(2,1)S(1)} %add_convert_fusion), channel_id=1, replica_groups=mesh['z'=8,'x'=4,'yh'=4,'yl'=2,'c'=2] {'yh','yl'}, dimensions={0} | all-to-all | bytes 1048576 | tf_op jit(solution)/shard_map/all_to_all | solution.py:495
  109.2 1.3 shard_map.169
  110.5 5.3 %all-to-all-start.2 = ((bf16[32,16,128]{2,1,0:T(8,128)(2,1)}), bf16[32,16,128]{2,1,0:T(8,128)(2,1)S(1)}, u32[]{:S(2)}, u32[]{:S(2)}) async-start(bf16[32,16,128]{2,1,0:T(8,128)(2,1)} %shard_map.169), calls=%async_computation.2 | async-start | bytes 262144 | tf_op jit(solution)/shard_map/all_to_all | solution.py:497
  115.8 0.0 copy-done.6
  115.8 0.0 copy-done.7
  115.8 0.0 copy-start.4
  115.8 0.0 copy-start.5
  115.8 0.5 shard_map.171.gated_h
  116.4 0.0 copy-done.8
  116.4 0.0 copy-start.9
  116.4 0.6 shard_map.172
  117.0 0.0 copy-start.10
  117.0 0.6 copy-done.10
  117.6 0.0 copy-start.11
  117.6 7.5 %all-to-all-done.2 = bf16[32,16,128]{2,1,0:T(8,128)(2,1)S(1)} async-done(((bf16[32,16,128]{2,1,0:T(8,128)(2,1)}), bf16[32,16,128]{2,1,0:T(8,128)(2,1)S(1)}, u32[]{:S(2)}, u32[]{:S(2)}) %all-to-all-start.2) | async-done | bytes 131104 | tf_op jit(solution)/shard_map/all_to_all | solution.py:497
  125.1 0.0 copy-done.9
  125.1 1.7 shard_map.170
  126.8 18.0 %all-gather = bf16[2048,128]{1,0:T(8,128)(2,1)S(1)} all-gather(bf16[128,128]{1,0:T(8,128)(2,1)S(1)} %shard_map.170), channel_id=2, replica_groups=mesh['z'=8,'x'=4,'yh'=4,'yl'=2,'c'=2] {'yh','yl','c'}, dimensions={0}, use_global_device_ids=true | all-gather | bytes 557056 | tf_op jit(solution)/shard_map/all_gather | solution.py:508
  144.8 0.0 copy-done.11
  144.8 2.9 %shard_map.173 = (bf16[32,80,128]{2,1,0:T(8,128)(2,1)}, f32[128,128]{1,0:T(8,128)S(1)}) custom-call(s32[4]{0:T(128)S(1)} %pad_add_fusion.place, bf16[16,128,128]{2,1,0:T(8,128)(2,1)S(1)} %bitcast.35, bf16[128,128]{1,0:T(8,128)(2,1)} %copy-done.9, bf16[2048,128]{1,0:T(8,128)(2,1)} %w_h.1, f32[128,128]{1,0:T(8,128)} %copy-done.10, f32[16,128]{1,0:T(8,128)} %copy-done.11), custom_call_target="tpu_custom_call" | custom-call | tf_op jit(solution)/shard_map/pallas_call | solution.py:71
  147.8 3.9 %all-to-all-start.3 = ((bf16[32,80,128]{2,1,0:T(8,128)(2,1)}), bf16[32,80,128]{2,1,0:T(8,128)(2,1)S(1)}, u32[]{:S(2)}, u32[]{:S(2)}) async-start(bf16[32,80,128]{2,1,0:T(8,128)(2,1)} %get-tuple-element.37), calls=%async_computation.3 | async-start | bytes 1310720 | tf_op jit(solution)/shard_map/all_to_all | solution.py:527
  151.7 0.1 slice_bitcast_fusion
  151.8 3.1 %collective-permute-start = (bf16[128,2048]{1,0:T(8,128)(2,1)S(1)}, bf16[128,2048]{1,0:T(8,128)(2,1)S(1)}, u32[]{:S(2)}, u32[]{:S(2)}) collective-permute-start(bf16[128,2048]{1,0:T(8,128)(2,1)S(1)} %get-tuple-element.46), channel_id=1, source_target_pairs={{0,2},{2,4},{4,6},{6,8},{8,10},{10,12},{12,14},{14,0},{1,3},{3,5},... | collective-permute-start | bytes 1572872 | tf_op jit(solution)/shard_map/ppermute | solution.py:479
  154.9 3.3 %collective-permute-start.1 = (bf16[128,2048]{1,0:T(8,128)(2,1)S(1)}, bf16[128,2048]{1,0:T(8,128)(2,1)S(1)}, u32[]{:S(2)}, u32[]{:S(2)}) collective-permute-start(bf16[128,2048]{1,0:T(8,128)(2,1)S(1)} %get-tuple-element.45), channel_id=1, source_target_pairs={{0,14},{2,0},{4,2},{6,4},{8,6},{10,8},{12,10},{14,12},{1,15},{3,1}... | collective-permute-start | bytes 1572872 | tf_op jit(solution)/shard_map/ppermute | solution.py:480
  158.3 9.9 %collective-permute-done.xa_h = bf16[128,2048]{1,0:T(8,128)(2,1)S(1)} collective-permute-done((bf16[128,2048]{1,0:T(8,128)(2,1)S(1)}, bf16[128,2048]{1,0:T(8,128)(2,1)S(1)}, u32[]{:S(2)}, u32[]{:S(2)}) %collective-permute-start) | collective-permute-done | bytes 524320 | tf_op jit(solution)/shard_map/ppermute | solution.py:479
  168.2 2.9 %collective-permute-start.2 = (bf16[128,2048]{1,0:T(8,128)(2,1)S(1)}, bf16[128,2048]{1,0:T(8,128)(2,1)S(1)}, u32[]{:S(2)}, u32[]{:S(2)}) collective-permute-start(bf16[128,2048]{1,0:T(8,128)(2,1)S(1)} %collective-permute-done.xa_h), channel_id=1, source_target_pairs={{0,1},{1,0},{2,3},{3,2},{4,5},{5,4},{6,7},{7,6},{8,9},{9,8},{10,11... | collective-permute-start | bytes 1572872 | tf_op jit(solution)/shard_map/ppermute | solution.py:481
  171.1 0.0 collective-permute-done.1.xb_h
  171.2 1.9 %collective-permute-start.3 = (bf16[128,2048]{1,0:T(8,128)(2,1)S(1)}, bf16[128,2048]{1,0:T(8,128)(2,1)S(1)}, u32[]{:S(2)}, u32[]{:S(2)}) collective-permute-start(bf16[128,2048]{1,0:T(8,128)(2,1)S(1)} %collective-permute-done.1.xb_h), channel_id=1, source_target_pairs={{0,1},{1,0},{2,3},{3,2},{4,5},{5,4},{6,7},{7,6},{8,9},{9,8},{10,11... | collective-permute-start | bytes 1572872 | tf_op jit(solution)/shard_map/ppermute | solution.py:482
  173.1 0.0 copy-done.4
  173.1 0.0 copy-done.5
  173.1 2.5 %shard_map.166.gown_h = f32[384,2048]{1,0:T(8,128)} custom-call(s32[4]{0:T(128)S(1)} %pad_add_fusion.place, bf16[256,2048]{1,0:T(8,128)(2,1)S(1)} %bitcast.19, bf16[256,2048]{1,0:T(8,128)(2,1)S(1)} %copy-done.4, bf16[256,768]{1,0:T(8,128)(2,1)S(1)} %copy-done.5), custom_call_target="tpu_custom_call" | custom-call | tf_op jit(solution)/shard_map/pallas_call | solution.py:71
  175.6 0.0 collective-permute-done.2.pa_h
  175.6 0.0 collective-permute-done.3.pb_h
  175.6 5.1 %shard_map.167 = (bf16[1,128,2048]{2,1,0:T(8,128)(2,1)}, bf16[1,128,2048]{2,1,0:T(8,128)(2,1)}, bf16[1,128,2048]{2,1,0:T(8,128)(2,1)}) custom-call(s32[4]{0:T(128)S(1)} %pad_add_fusion.place, bf16[128,2048]{1,0:T(8,128)(2,1)S(1)} %collective-permute-done.xa_h, bf16[128,2048]{1,0:T(8,128)(2,1)S(1)} %collective-permute-done.1.xb_h, ...), custom_call_target="tpu_custom_call" | custom-call | tf_op jit(solution)/shard_map/pallas_call | solution.py:71
  180.7 1.2 shard_map.174
  181.9 0.0 all-to-all-done.3.got
  181.9 1.4 shard_map.175
Async XLA Ops:
  0.6 47.7 %copy-start.1 = (bf16[1,128,2048]{2,1,0:T(8,128)(2,1)S(1)}, bf16[1,128,2048]{2,1,0:T(8,128)(2,1)}, u32[]{:S(2)}) copy-start(bf16[1,128,2048]{2,1,0:T(8,128)(2,1)} %param.20) | copy-start | bytes 1572868
  0.6 47.7 %copy-start.2 = (bf16[1,128,2048]{2,1,0:T(8,128)(2,1)S(1)}, bf16[1,128,2048]{2,1,0:T(8,128)(2,1)}, u32[]{:S(2)}) copy-start(bf16[1,128,2048]{2,1,0:T(8,128)(2,1)} %param.21) | copy-start | bytes 1572868
  0.7 47.7 %copy-start = (bf16[1,128,2048]{2,1,0:T(8,128)(2,1)S(1)}, bf16[1,128,2048]{2,1,0:T(8,128)(2,1)}, u32[]{:S(2)}) copy-start(bf16[1,128,2048]{2,1,0:T(8,128)(2,1)} %param.19) | copy-start | bytes 1572868
  43.6 31.7 %collective-permute-start.4 = (bf16[256,2048]{1,0:T(8,128)(2,1)S(1)}, bf16[256,2048]{1,0:T(8,128)(2,1)S(1)}, u32[]{:S(2)}, u32[]{:S(2)}) collective-permute-start(bf16[256,2048]{1,0:T(8,128)(2,1)S(1)} %bitcast.17), channel_id=1, source_target_pairs={{0,1},{1,0},{2,3},{3,2},{4,5},{5,4},{6,7},{7,6},{8,9},{9,8},{10,11... | collective-permute-start | bytes 3145736 | tf_op jit(solution)/shard_map/ppermute | solution.py:436
  48.6 23.0 %collective-permute-start.5 = (bf16[192,2048]{1,0:T(8,128)(2,1)S(1)}, bf16[192,2048]{1,0:T(8,128)(2,1)S(1)}, u32[]{:S(2)}, u32[]{:S(2)}) collective-permute-start(bf16[192,2048]{1,0:T(8,128)(2,1)S(1)} %get-tuple-element.27), channel_id=1, source_target_pairs={{0,2},{2,4},{4,6},{6,8},{8,10},{10,12},{12,14},{14,0},{1,3},{3,5},... | collective-permute-start | bytes 2359304 | tf_op jit(solution)/shard_map/ppermute | solution.py:434
  51.8 20.7 %collective-permute-start.6 = (bf16[192,2048]{1,0:T(8,128)(2,1)S(1)}, bf16[192,2048]{1,0:T(8,128)(2,1)S(1)}, u32[]{:S(2)}, u32[]{:S(2)}) collective-permute-start(bf16[192,2048]{1,0:T(8,128)(2,1)S(1)} %get-tuple-element.28), channel_id=1, source_target_pairs={{0,14},{2,0},{4,2},{6,4},{8,6},{10,8},{12,10},{14,12},{1,15},{3,1}... | collective-permute-start | bytes 2359304 | tf_op jit(solution)/shard_map/ppermute | solution.py:435
  75.3 6.7 %copy-start.3 = (bf16[256,2048]{1,0:T(8,128)(2,1)}, bf16[256,2048]{1,0:T(8,128)(2,1)S(1)}, u32[]{:S(2)}) copy-start(bf16[256,2048]{1,0:T(8,128)(2,1)S(1)} %collective-permute-done.4.par) | copy-start | bytes 3145732
  79.0 5.3 %collective-permute-start.7 = (bf16[8,256,128]{2,1,0:T(8,128)(2,1)S(1)}, bf16[8,256,128]{2,1,0:T(8,128)(2,1)S(1)}, u32[]{:S(2)}, u32[]{:S(2)}) collective-permute-start(bf16[8,256,128]{2,1,0:T(8,128)(2,1)S(1)} %get-tuple-element.34), channel_id=1, source_target_pairs={{0,1},{1,0},{2,3},{3,2},{4,5},{5,4},{6,7},{7,6},{8,9},{9,8},{10,11... | collective-permute-start | bytes 1572872 | tf_op jit(solution)/shard_map/ppermute | solution.py:471
  84.2 31.5 %copy-start.6 = (f32[128,128]{1,0:T(8,128)S(1)}, f32[128,128]{1,0:T(8,128)}, u32[]{:S(2)}) copy-start(f32[128,128]{1,0:T(8,128)} %states.7) | copy-start | bytes 196612
  84.2 31.5 %copy-start.7 = (bf16[128,128]{1,0:T(8,128)(2,1)S(1)}, bf16[128,128]{1,0:T(8,128)(2,1)}, u32[]{:S(2)}) copy-start(bf16[128,128]{1,0:T(8,128)(2,1)} %gate.5) | copy-start | bytes 98308
  84.3 32.1 %copy-start.8 = (f32[128,128]{1,0:T(8,128)S(1)}, f32[128,128]{1,0:T(8,128)}, u32[]{:S(2)}) copy-start(f32[128,128]{1,0:T(8,128)} %decay.3) | copy-start | bytes 196612
  110.5 14.6 %all-to-all-start.2 = ((bf16[32,16,128]{2,1,0:T(8,128)(2,1)}), bf16[32,16,128]{2,1,0:T(8,128)(2,1)S(1)}, u32[]{:S(2)}, u32[]{:S(2)}) async-start(bf16[32,16,128]{2,1,0:T(8,128)(2,1)} %shard_map.169), calls=%async_computation.2 | async-start | bytes 262144 | tf_op jit(solution)/shard_map/all_to_all | solution.py:497
  115.8 57.3 %copy-start.4 = (bf16[256,2048]{1,0:T(8,128)(2,1)S(1)}, bf16[256,2048]{1,0:T(8,128)(2,1)}, u32[]{:S(2)}) copy-start(bf16[256,2048]{1,0:T(8,128)(2,1)} %copy-done.3) | copy-start | bytes 3145732
  115.8 57.3 %copy-start.5 = (bf16[256,768]{1,0:T(8,128)(2,1)S(1)}, bf16[256,768]{1,0:T(8,128)(2,1)}, u32[]{:S(2)}) copy-start(bf16[256,768]{1,0:T(8,128)(2,1)} %get-tuple-element.29.mix.mix_h) | copy-start | bytes 1179652
  116.4 8.7 %copy-start.9 = (bf16[128,128]{1,0:T(8,128)(2,1)}, bf16[128,128]{1,0:T(8,128)(2,1)S(1)}, u32[]{:S(2)}) copy-start(bf16[128,128]{1,0:T(8,128)(2,1)S(1)} %shard_map.171.gated_h) | copy-start | bytes 98308
  117.0 0.6 copy-start.10
  117.6 27.2 %copy-start.11 = (f32[16,128]{1,0:T(8,128)}, f32[16,128]{1,0:T(8,128)S(1)}, u32[]{:S(2)}) copy-start(f32[16,128]{1,0:T(8,128)S(1)} %get-tuple-element.36.tail_h) | copy-start | bytes 24580
  147.8 34.1 %all-to-all-start.3 = ((bf16[32,80,128]{2,1,0:T(8,128)(2,1)}), bf16[32,80,128]{2,1,0:T(8,128)(2,1)S(1)}, u32[]{:S(2)}, u32[]{:S(2)}) async-start(bf16[32,80,128]{2,1,0:T(8,128)(2,1)} %get-tuple-element.37), calls=%async_computation.3 | async-start | bytes 1310720 | tf_op jit(solution)/shard_map/all_to_all | solution.py:527
  151.8 16.4 %collective-permute-start = (bf16[128,2048]{1,0:T(8,128)(2,1)S(1)}, bf16[128,2048]{1,0:T(8,128)(2,1)S(1)}, u32[]{:S(2)}, u32[]{:S(2)}) collective-permute-start(bf16[128,2048]{1,0:T(8,128)(2,1)S(1)} %get-tuple-element.46), channel_id=1, source_target_pairs={{0,2},{2,4},{4,6},{6,8},{8,10},{10,12},{12,14},{14,0},{1,3},{3,5},... | collective-permute-start | bytes 1572872 | tf_op jit(solution)/shard_map/ppermute | solution.py:479
  154.9 16.2 %collective-permute-start.1 = (bf16[128,2048]{1,0:T(8,128)(2,1)S(1)}, bf16[128,2048]{1,0:T(8,128)(2,1)S(1)}, u32[]{:S(2)}, u32[]{:S(2)}) collective-permute-start(bf16[128,2048]{1,0:T(8,128)(2,1)S(1)} %get-tuple-element.45), channel_id=1, source_target_pairs={{0,14},{2,0},{4,2},{6,4},{8,6},{10,8},{12,10},{14,12},{1,15},{3,1}... | collective-permute-start | bytes 1572872 | tf_op jit(solution)/shard_map/ppermute | solution.py:480
  168.2 7.4 %collective-permute-start.2 = (bf16[128,2048]{1,0:T(8,128)(2,1)S(1)}, bf16[128,2048]{1,0:T(8,128)(2,1)S(1)}, u32[]{:S(2)}, u32[]{:S(2)}) collective-permute-start(bf16[128,2048]{1,0:T(8,128)(2,1)S(1)} %collective-permute-done.xa_h), channel_id=1, source_target_pairs={{0,1},{1,0},{2,3},{3,2},{4,5},{5,4},{6,7},{7,6},{8,9},{9,8},{10,11... | collective-permute-start | bytes 1572872 | tf_op jit(solution)/shard_map/ppermute | solution.py:481
  171.2 4.5 %collective-permute-start.3 = (bf16[128,2048]{1,0:T(8,128)(2,1)S(1)}, bf16[128,2048]{1,0:T(8,128)(2,1)S(1)}, u32[]{:S(2)}, u32[]{:S(2)}) collective-permute-start(bf16[128,2048]{1,0:T(8,128)(2,1)S(1)} %collective-permute-done.1.xb_h), channel_id=1, source_target_pairs={{0,1},{1,0},{2,3},{3,2},{4,5},{5,4},{6,7},{7,6},{8,9},{9,8},{10,11... | collective-permute-start | bytes 1572872 | tf_op jit(solution)/shard_map/ppermute | solution.py:482

commit v4 on v2

--- a/solution.py
+++ b/solution.py
@@ -54,7 +54,7 @@
     )(*args)
 
 
-def call(body, out_shape, place, *args, specs=None, outs_in=None, scratch=(), vmem=VMEM):
+def call(body, out_shape, place, *args, specs=None, free=(), outs_in=None, scratch=(), vmem=VMEM):
     whole = lambda a: pl.BlockSpec(a.shape, lambda i, s, n=len(a.shape): (0,) * n)
     outs = out_shape if isinstance(out_shape, (list, tuple)) else [out_shape]
     in_specs = [whole(a) for a in args]
@@ -63,6 +63,8 @@
     for k in specs or ():
         in_specs[k] = pl.BlockSpec(memory_space=pltpu.HBM)
         args[k] = pltpu.with_memory_space_constraint(args[k], pltpu.HBM)
+    for k in free:
+        in_specs[k] = pl.BlockSpec(memory_space=pl.ANY)
     for k in outs_in or ():
         out_specs[k] = pl.BlockSpec(memory_space=pltpu.HBM)
         outs[k] = pltpu.HBM(outs[k].shape, outs[k].dtype)
@@ -104,11 +106,6 @@
     position = jnp.where(named > 0.0, position, -1.0)
     slot = lax.broadcasted_iota(jnp.int32, (experts, half, n), 1).astype(F32)
     at = lambda first: jnp.where(position[:, None, :] == slot + first, 1.0, 0.0).astype(F32)
-    pick[...] = (
-        jnp.concatenate([at(0.0), at(float(half))], axis=1)
-        .reshape(experts * cap, n)
-        .astype(BF16)
-    )
     hot = at((place[1] * half).astype(F32))
     scale = jnp.sum(hot * wt[:, None, :], axis=2, keepdims=True).reshape(experts * half, 1)
     hot = hot.reshape(experts * half, n).astype(BF16)
@@ -126,6 +123,11 @@
             )
             copy.start()
             out.append(copy)
+    pick[...] = (
+        jnp.concatenate([at(0.0), at(float(half))], axis=1)
+        .reshape(experts * cap, n)
+        .astype(BF16)
+    )
     kept = pltpu.make_async_copy(pick, pick_h, sems.at[8])
     kept.start()
     for copy in (*out, kept):
@@ -153,8 +155,6 @@
     rows = jnp.zeros(tail.shape, F32)
     for k, v in enumerate(values):
         rows = jnp.where(line == 3 + k, jnp.broadcast_to(v, tail.shape), rows)
-    for k, v in enumerate(split3(st[n - 1 : n])):
-        rows = jnp.where(line == 8 + k, jnp.broadcast_to(v, tail.shape), rows)
     tail[...] = rows
 
 
@@ -182,11 +182,17 @@
     return nt(side, w_s[k])
 
 
-def first_body(place, own, wg, wu, wd, wa, wb, part, w_s, sems):
-    where = columns(place[0], w_s.shape[2])
-    loads = copies(weight_copies(wg, wu, wd, wa, wb, w_s, where, 3), sems)
+def first_body(place, own, wg, wu, wd, wa, wb, part, other, w_s, sems):
+    cols = w_s.shape[2]
+    sides = (w_s, columns(place[0], cols)), (other, columns(1 - place[0], cols))
+    pairs = []
+    for to, where in sides:
+        pairs += weight_copies(wg, wu, wd, wa, wb, to, where, 3)
+    loads = copies(pairs, sems)
     for k in range(3):
         part[k] = product(k, own, w_s, loads)
+    for copy in loads[9:]:
+        copy.wait()
 
 
 def partials(out, gb, ub, w_s):
@@ -196,13 +202,11 @@
         out[k] = p[:, k * width : (k + 1) * width].astype(out.dtype)
 
 
-def expert_body(place, par, part, wg, wu, wd, wa, wb, psend, mix_h, w_s, mix, sems):
-    where = columns(1 - place[0], w_s.shape[2])
-    loads = copies(weight_copies(wg, wu, wd, wa, wb, w_s, where, 3), sems)
+def expert_body(place, par, part, w_s, psend, mix_h, mix, sems):
     units = w_s.shape[1]
-    gate = part[0] + product(0, par, w_s, loads)
-    up = part[1] + product(1, par, w_s, loads)
-    grad = part[2] + product(2, par, w_s, loads)
+    gate = part[0] + product(0, par, w_s, ())
+    up = part[1] + product(1, par, w_s, ())
+    grad = part[2] + product(2, par, w_s, ())
     sig = jax.nn.sigmoid(gate)
     silu = gate * sig
     ub = (grad * silu).astype(BF16)
@@ -210,7 +214,7 @@
     mix[:, 0:units] = gb
     mix[:, units : 2 * units] = ub
     mix[:, 2 * units :] = (silu * up).astype(BF16)
-    (kept,) = copies(((mix, mix_h),), sems.at[pl.ds(9, 1)])
+    (kept,) = copies(((mix, mix_h),), sems)
     partials(psend, gb, ub, w_s)
     kept.wait()
 
@@ -317,7 +321,7 @@
     prod[...] = a
 
 
-def finish_body(place, got, local, prod, states, proj, drive, ddecay):
+def finish_body(place, got, local, prod, states, before, proj, drive, ddecay):
     rows = proj.shape[0]
     members = got.shape[0]
     s = place[2]
@@ -326,19 +330,17 @@
         total = total + got[m, 0:rows, :].astype(F32)
     proj[...] = total
     carry = jnp.zeros((1, local.shape[1]), F32)
-    before = jnp.zeros((1, local.shape[1]), F32)
     for m in range(members - 1, -1, -1):
-        v = got[m, rows : rows + 16, :].astype(F32)
+        v = got[m, rows : rows + 8, :].astype(F32)
         later = m > s
         b = jnp.where(later, v[0:1] + v[1:2] + v[2:3], 0.0)
         a = jnp.where(later, v[3:4] + v[4:5] + v[5:6], 1.0)
         carry = b + a * carry
-        before = jnp.where(m == s - 1, v[8:9] + v[9:10] + v[10:11], before)
     g = local[...] + prod[...] * carry
     drive[...] = g
     st = states[...]
     t = lax.broadcasted_iota(jnp.int32, st.shape, 0)
-    previous = jnp.where(t == 0, jnp.broadcast_to(before, st.shape), pltpu.roll(st, 1, 0))
+    previous = jnp.where(t == 0, jnp.broadcast_to(before[...], st.shape), pltpu.roll(st, 1, 0))
     ddecay[...] = g * previous
 
 
@@ -392,7 +394,8 @@
     par = lax.ppermute(own, "c", swap)
 
     units = hidden + 2 * q
-    tail = 16
+    tail = 8
+    before = lax.ppermute(states[tokens - 1 :], SP, [(k, k + 1) for k in range(n_sp - 1)])
     gated, weight, tails = call(
         prep_body,
         [shape((tokens, ch), BF16), shape((tokens, ch), F32), shape((tail, ch), F32)],
@@ -403,22 +406,23 @@
     wide = cols // n_y
     held = pltpu.VMEM((3, units, cols), BF16)
     weights = (wg, wu, wd, wa, wb)
-    part = call(
-        first_body, shape((3, slots, units), F32), place, own, *weights,
-        specs=(1, 2, 3, 4, 5), scratch=[held, pltpu.SemaphoreType.DMA((9,))],
+    part, other = call(
+        first_body,
+        [shape((3, slots, units), F32), shape((3, units, cols), BF16)],
+        place, own, *weights,
+        specs=(1, 2, 3), free=(4, 5),
+        scratch=[held, pltpu.SemaphoreType.DMA((18,))],
     )
     psend, mix = call(
         expert_body,
         [shape((n_y, slots, wide), BF16), shape((slots, 3 * units), BF16)],
-        place, par, part, *weights,
-        specs=(2, 3, 4, 5, 6), outs_in=(1,),
-        scratch=[
-            held, pltpu.VMEM((slots, 3 * units), BF16), pltpu.SemaphoreType.DMA((10,)),
-        ],
+        place, par, part, other,
+        outs_in=(1,),
+        scratch=[pltpu.VMEM((slots, 3 * units), BF16), pltpu.SemaphoreType.DMA((1,))],
     )
     pkeep = call(
         keep_body, shape((n_y, slots, wide), F32), place, mix, *weights,
-        specs=(0, 1, 2, 3, 4, 5),
+        specs=(0, 1, 2, 3), free=(4, 5),
         scratch=[
             pltpu.VMEM((2, units, cols), BF16), pltpu.VMEM((slots, 2 * units), BF16),
             pltpu.SemaphoreType.DMA((7,)),
@@ -473,7 +477,7 @@
     got = lax.all_to_all(out, SP, 0, 0, tiled=True)
     proj, drive, ddecay = call(
         finish_body, [shape((rows, ch), F32), row(F32), row(F32)],
-        place, got, loc, prod, states,
+        place, got, loc, prod, states, before,
     )
 
     def total(k):

time: 187 us -> 183 us (0.979)
  waiting for transfers between devices: 52.3 us -> 47.4 us
  starting transfers between devices: 36.3 us -> 40 us
    ppermute x0 -> x1, starting transfers between devices: none -> 3.69 us  [local(): lax.ppermute(states[tokens - 1:], SP, [(k, k + 1) for k in range(n_sp - 1)])]
    all_to_all x1, waiting for transfers between devices: 6.1 us -> 2.53 us  [local(): back = lax.all_to_all(ret, SP, 0, 0, tiled=True)]
  transfers between devices with their start and end apart: 9 -> 10, of which waited for: 5 -> 5; matrix products, arithmetic and copies ran while one was open for 2% -> 2% of each run, Pallas kernels for 9% -> 9%
where the time goes in v4:
time: 183 us; the launch traced here: 182 us
  blocking collectives  63 us (34%)
  waiting for transfers between devices  47.4 us (26%)
  starting transfers between devices  40 us (22%)
  Pallas kernels  22.8 us (12%)
  local copies, waits for them, and re-layouts  5.24 us (3%)
  other arithmetic  2.34 us (1%)
    all_to_all x1, blocking collectives, local(): own = lax.all_to_all(send.reshape(n_sp, half, width), SP, 0, 0, tiled=True)  41.2 us
    pallas_call x11, Pallas kernels, call(): pl.pallas_call(body, grid_spec=pltpu.PrefetchScalarGridSpec(num_scalar_pr...  22.6 us
    all_gather x1, blocking collectives, local(): mid = lax.all_gather(mid, TP)  21.8 us
    ppermute x1, waiting for transfers between devices, local(): wa = lax.ppermute(w_lo, Y, ring(1))  16 us
    all_to_all x1, waiting for transfers between devices, local(): got = lax.all_to_all(out, SP, 0, 0, tiled=True)  14.4 us
    all_to_all x1, waiting for transfers between devices, local(): parts = lax.all_to_all(psum, Y, 0, 0, tiled=True)  11.2 us
    all_to_all x1, starting transfers between devices, local(): got = lax.all_to_all(out, SP, 0, 0, tiled=True)  9.51 us
    all_to_all x1, starting transfers between devices, local(): parts = lax.all_to_all(psum, Y, 0, 0, tiled=True)  7.75 us
  transfers between devices with their start and end apart: 10, of which 5 were waited for; matrix products, arithmetic and copies ran while one was open for 2% of the time, Pallas kernels for 9%

profile of v4, /device:TPU:8, one launch (start us, length us, event | category | flops | bytes accessed | tf_op | source)
XLA Modules:
  0.0 181.8 jit_solution(5932358350113805493)
XLA Ops:
  0.6 0.0 copy-start.2
  0.6 0.0 copy-start.1
  0.7 0.0 copy-start
  0.7 0.1 pad_add_fusion.place
  0.8 3.0 %shard_map.162 = (bf16[256,2048]{1,0:T(8,128)(2,1)}, bf16[512,128]{1,0:T(8,128)(2,1)}) custom-call(s32[4]{0:T(128)S(1)} %pad_add_fusion.place, s32[2,128]{1,0:T(2,128)} %bitcast.34, f32[2,128]{1,0:T(2,128)} %bitcast.35, bf16[128,2048]{1,0:T(8,128)(2,1)} %x_h.1, bf16[128,2048]{1,0:T(8,128)(2,1)} %og_h.3), custom_call_target="tpu_custom_call" | custom-call | tf_op jit(solution)/shard_map/pallas_call | solution.py:71
  3.7 41.2 %all_to_all.20 = bf16[32,8,2048]{2,1,0:T(8,128)(2,1)S(1)} all-to-all(bf16[32,8,2048]{2,1,0:T(8,128)(2,1)} %bitcast.33), channel_id=1, replica_groups=mesh['z'=8,'x'=4,'yh'=4,'yl'=2,'c'=2] {'z','x'}, dimensions={0} | all-to-all | bytes 2097152 | tf_op jit(solution)/shard_map/all_to_all | solution.py:380
  45.0 1.9 %collective-permute-start = (bf16[256,2048]{1,0:T(8,128)(2,1)S(1)}, bf16[256,2048]{1,0:T(8,128)(2,1)S(1)}, u32[]{:S(2)}, u32[]{:S(2)}) collective-permute-start(bf16[256,2048]{1,0:T(8,128)(2,1)S(1)} %bitcast.19), channel_id=1, source_target_pairs={{0,1},{1,0},{2,3},{3,2},{4,5},{5,4},{6,7},{7,6},{8,9},{9,8},{10,11... | collective-permute-start | bytes 3145736 | tf_op jit(solution)/shard_map/ppermute | solution.py:394
  46.9 0.0 copy-done.2
  46.9 0.0 copy-done.1
  46.9 0.0 copy-done
  46.9 0.2 shard_map.163
  47.1 3.5 %collective-permute-start.1 = (bf16[192,2048]{1,0:T(8,128)(2,1)S(1)}, bf16[192,2048]{1,0:T(8,128)(2,1)S(1)}, u32[]{:S(2)}, u32[]{:S(2)}) collective-permute-start(bf16[192,2048]{1,0:T(8,128)(2,1)S(1)} %get-tuple-element.30), channel_id=1, source_target_pairs={{0,2},{2,4},{4,6},{6,8},{8,10},{10,12},{12,14},{14,0},{1,3},{3,5},... | collective-permute-start | bytes 2359304 | tf_op jit(solution)/shard_map/ppermute | solution.py:392
  50.6 2.4 %collective-permute-start.2 = (bf16[192,2048]{1,0:T(8,128)(2,1)S(1)}, bf16[192,2048]{1,0:T(8,128)(2,1)S(1)}, u32[]{:S(2)}, u32[]{:S(2)}) collective-permute-start(bf16[192,2048]{1,0:T(8,128)(2,1)S(1)} %get-tuple-element.31), channel_id=1, source_target_pairs={{0,14},{2,0},{4,2},{6,4},{8,6},{10,8},{12,10},{14,12},{1,15},{3,1}... | collective-permute-start | bytes 2359304 | tf_op jit(solution)/shard_map/ppermute | solution.py:393
  52.9 16.0 %collective-permute-done.1.wa = bf16[192,2048]{1,0:T(8,128)(2,1)S(1)} collective-permute-done((bf16[192,2048]{1,0:T(8,128)(2,1)S(1)}, bf16[192,2048]{1,0:T(8,128)(2,1)S(1)}, u32[]{:S(2)}, u32[]{:S(2)}) %collective-permute-start.1) | collective-permute-done | bytes 786464 | tf_op jit(solution)/shard_map/ppermute | solution.py:392
  68.9 3.2 %collective-permute-done.2.wb = bf16[192,2048]{1,0:T(8,128)(2,1)S(1)} collective-permute-done((bf16[192,2048]{1,0:T(8,128)(2,1)S(1)}, bf16[192,2048]{1,0:T(8,128)(2,1)S(1)}, u32[]{:S(2)}, u32[]{:S(2)}) %collective-permute-start.2) | collective-permute-done | bytes 786464 | tf_op jit(solution)/shard_map/ppermute | solution.py:393
  72.1 2.9 %shard_map.164 = (f32[3,256,256]{2,1,0:T(8,128)S(1)}, bf16[3,256,1024]{2,1,0:T(8,128)(2,1)S(1)}) custom-call(s32[4]{0:T(128)S(1)} %pad_add_fusion.place, bf16[256,2048]{1,0:T(8,128)(2,1)S(1)} %bitcast.20, bf16[128,2048]{1,0:T(8,128)(2,1)} %bitcast.22, bf16[128,2048]{1,0:T(8,128)(2,1)} %bitcast.25, bf16[128,2048]{1,0:T(8,128)(2,1)} %bitcast.28, ...), custom_call_target="tpu_custom_call" | custom-call | tf_op jit(solution)/shard_map/pallas_call | solution.py:71
  75.1 0.0 collective-permute-done.par
  75.1 0.0 copy-start.3
  75.1 2.2 %shard_map.165 = (bf16[8,256,128]{2,1,0:T(8,128)(2,1)S(1)}, bf16[256,768]{1,0:T(8,128)(2,1)}) custom-call(s32[4]{0:T(128)S(1)} %pad_add_fusion.place, bf16[256,2048]{1,0:T(8,128)(2,1)S(1)} %collective-permute-done.par, f32[3,256,256]{2,1,0:T(8,128)S(1)} %get-tuple-element.32.part, bf16[3,256,1024]{2,1,0:T(8,128)(2,1)S(1)} %get-tuple-element.33.w_s), custom_call_target="tpu_custom_call" | custom-call | tf_op jit(solution)/shard_map/pallas_call | solution.py:71
  77.3 1.9 %collective-permute-start.5 = (bf16[8,256,128]{2,1,0:T(8,128)(2,1)S(1)}, bf16[8,256,128]{2,1,0:T(8,128)(2,1)S(1)}, u32[]{:S(2)}, u32[]{:S(2)}) collective-permute-start(bf16[8,256,128]{2,1,0:T(8,128)(2,1)S(1)} %get-tuple-element.39), channel_id=1, source_target_pairs={{0,1},{1,0},{2,3},{3,2},{4,5},{5,4},{6,7},{7,6},{8,9},{9,8},{10,11... | collective-permute-start | bytes 1572872 | tf_op jit(solution)/shard_map/ppermute | solution.py:431
  79.2 0.0 copy-start.5
  79.3 2.2 %shard_map.167 = f32[8,256,128]{2,1,0:T(8,128)S(1)} custom-call(s32[4]{0:T(128)S(1)} %pad_add_fusion.place, bf16[256,768]{1,0:T(8,128)(2,1)} %get-tuple-element.34.mix.mix_h, bf16[128,2048]{1,0:T(8,128)(2,1)} %bitcast.23, bf16[128,2048]{1,0:T(8,128)(2,1)} %bitcast.26, bf16[128,2048]{1,0:T(8,128)(2,1)} %bitcast.29, ...), custom_call_target="tpu_custom_call" | custom-call | tf_op jit(solution)/shard_map/pallas_call | solution.py:71
  81.4 0.0 copy-done.3
  81.4 0.0 copy-start.6
  81.5 0.0 copy-start.7
  81.5 0.0 copy-start.8
  81.5 0.0 collective-permute-done.5
  81.5 0.0 copy-start.4
  81.5 0.9 add_convert_fusion
  82.4 7.8 %all-to-all-start.1 = ((bf16[8,256,128]{2,1,0:T(8,128)(2,1)}), bf16[8,256,128]{2,1,0:T(8,128)(2,1)S(1)}, u32[]{:S(2)}, u32[]{:S(2)}) async-start(bf16[8,256,128]{2,1,0:T(8,128)(2,1)} %add_convert_fusion), calls=%async_computation.1 | async-start | bytes 1048576 | tf_op jit(solution)/shard_map/all_to_all | solution.py:445
  90.1 0.0 copy-done.5
  90.2 0.0 copy-done.4
  90.2 3.4 %shard_map.166 = (f32[384,2048]{1,0:T(8,128)}, bf16[192,2048]{1,0:T(8,128)(2,1)}, bf16[192,2048]{1,0:T(8,128)(2,1)S(1)}) custom-call(s32[4]{0:T(128)S(1)} %pad_add_fusion.place, bf16[256,2048]{1,0:T(8,128)(2,1)S(1)} %bitcast.21, bf16[256,2048]{1,0:T(8,128)(2,1)S(1)} %copy-done.4, bf16[256,768]{1,0:T(8,128)(2,1)S(1)} %copy-done.5), custom_call_target="tpu_custom_call" | custom-call | tf_op jit(solution)/shard_map/pallas_call | solution.py:71
  93.6 0.0 copy-start.12
  93.6 0.9 copy-done.12
  94.5 1.9 %collective-permute-start.3 = (bf16[192,2048]{1,0:T(8,128)(2,1)}, bf16[192,2048]{1,0:T(8,128)(2,1)}, u32[]{:S(2)}, u32[]{:S(2)}) collective-permute-start(bf16[192,2048]{1,0:T(8,128)(2,1)} %get-tuple-element.36), channel_id=1, source_target_pairs={{0,14},{2,0},{4,2},{6,4},{8,6},{10,8},{12,10},{14,12},{1,15},{3,1}... | collective-permute-start | bytes 2359304 | tf_op jit(solution)/shard_map/ppermute | solution.py:441
  96.4 11.2 %all-to-all-done.1.parts = bf16[8,256,128]{2,1,0:T(8,128)(2,1)S(1)} async-done(((bf16[8,256,128]{2,1,0:T(8,128)(2,1)}), bf16[8,256,128]{2,1,0:T(8,128)(2,1)S(1)}, u32[]{:S(2)}, u32[]{:S(2)}) %all-to-all-start.1) | async-done | bytes 524320 | tf_op jit(solution)/shard_map/all_to_all | solution.py:445
  107.6 1.3 shard_map.168
  108.9 5.6 %all-to-all-start.2 = ((bf16[32,16,128]{2,1,0:T(8,128)(2,1)}), bf16[32,16,128]{2,1,0:T(8,128)(2,1)S(1)}, u32[]{:S(2)}, u32[]{:S(2)}) async-start(bf16[32,16,128]{2,1,0:T(8,128)(2,1)} %shard_map.168), calls=%async_computation.2 | async-start | bytes 262144 | tf_op jit(solution)/shard_map/all_to_all | solution.py:447
  114.4 1.9 %collective-permute-start.4 = (bf16[192,2048]{1,0:T(8,128)(2,1)}, bf16[192,2048]{1,0:T(8,128)(2,1)}, u32[]{:S(2)}, u32[]{:S(2)}) collective-permute-start(bf16[192,2048]{1,0:T(8,128)(2,1)} %copy-done.12), channel_id=1, source_target_pairs={{0,2},{2,4},{4,6},{6,8},{8,10},{10,12},{12,14},{14,0},{1,3},{3,5},... | collective-permute-start | bytes 2359304 | tf_op jit(solution)/shard_map/ppermute | solution.py:442
  116.4 0.0 copy-done.6
  116.4 3.7 %collective-permute-start.6 = (f32[1,128]{1,0:T(1,128)S(1)}, f32[1,128]{1,0:T(1,128)S(1)}, u32[]{:S(2)}, u32[]{:S(2)}) collective-permute-start(f32[1,128]{1,0:T(1,128)S(1)} %slice.39), channel_id=1, source_target_pairs={{0,16},{16,32},{32,48},{48,64},{64,80},{80,96},{96,112},{112,128},... | collective-permute-start | bytes 1544 | tf_op jit(solution)/shard_map/ppermute | solution.py:398
  120.1 0.0 copy-done.7
  120.1 0.6 shard_map.170
  120.7 0.0 copy-start.9
  120.7 0.6 copy-done.9
  121.3 0.6 copy-done.10
  121.9 0.6 copy-done.11
  122.5 2.5 %all-to-all-done.2 = bf16[32,16,128]{2,1,0:T(8,128)(2,1)S(1)} async-done(((bf16[32,16,128]{2,1,0:T(8,128)(2,1)}), bf16[32,16,128]{2,1,0:T(8,128)(2,1)S(1)}, u32[]{:S(2)}, u32[]{:S(2)}) %all-to-all-start.2) | async-done | bytes 131104 | tf_op jit(solution)/shard_map/all_to_all | solution.py:447
  125.1 1.7 shard_map.169
  126.8 21.8 %all-gather = bf16[2048,128]{1,0:T(8,128)(2,1)S(1)} all-gather(bf16[128,128]{1,0:T(8,128)(2,1)S(1)} %shard_map.169), channel_id=2, replica_groups=mesh['z'=8,'x'=4,'yh'=4,'yl'=2,'c'=2] {'yh','yl','c'}, dimensions={0}, use_global_device_ids=true | all-gather | bytes 557056 | tf_op jit(solution)/shard_map/all_gather | solution.py:458
  148.5 2.9 %shard_map.171 = (bf16[32,72,128]{2,1,0:T(8,128)(2,1)}, f32[128,128]{1,0:T(8,128)S(1)}) custom-call(s32[4]{0:T(128)S(1)} %pad_add_fusion.place, bf16[16,128,128]{2,1,0:T(8,128)(2,1)S(1)} %bitcast.31, bf16[128,128]{1,0:T(8,128)(2,1)} %copy-done.10, bf16[2048,128]{1,0:T(8,128)(2,1)} %w_h.1, f32[128,128]{1,0:T(8,128)} %copy-done.9, f32[8,128]{1,0:T(8,128)} %copy-done.11), custom_call_target="tpu_custom_call" | custom-call | tf_op jit(solution)/shard_map/pallas_call | solution.py:71
  151.4 9.5 %all-to-all-start.3 = ((bf16[32,72,128]{2,1,0:T(8,128)(2,1)}), bf16[32,72,128]{2,1,0:T(8,128)(2,1)S(1)}, u32[]{:S(2)}, u32[]{:S(2)}) async-start(bf16[32,72,128]{2,1,0:T(8,128)(2,1)} %get-tuple-element.43), calls=%async_computation.3 | async-start | bytes 1179648 | tf_op jit(solution)/shard_map/all_to_all | solution.py:477
  161.0 0.0 copy-start.13
  161.0 0.0 collective-permute-done.3
  161.0 1.3 fusion.3
  162.3 0.0 collective-permute-done.4
  162.3 1.2 fusion.4
  163.5 0.0 copy-done.13
  163.5 1.4 fusion.2
  164.8 1.2 shard_map.172
  166.0 0.0 collective-permute-done.6.before
  166.0 14.4 %all-to-all-done.3.got = bf16[32,72,128]{2,1,0:T(8,128)(2,1)S(1)} async-done(((bf16[32,72,128]{2,1,0:T(8,128)(2,1)}), bf16[32,72,128]{2,1,0:T(8,128)(2,1)S(1)}, u32[]{:S(2)}, u32[]{:S(2)}) %all-to-all-start.3) | async-done | bytes 589856 | tf_op jit(solution)/shard_map/all_to_all | solution.py:477
  180.4 1.3 shard_map.173
  (4 shorter events, 0.0 us)
Async XLA Ops:
  0.6 46.2 %copy-start.2 = (bf16[1,128,2048]{2,1,0:T(8,128)(2,1)S(1)}, bf16[1,128,2048]{2,1,0:T(8,128)(2,1)}, u32[]{:S(2)}) copy-start(bf16[1,128,2048]{2,1,0:T(8,128)(2,1)} %param.21) | copy-start | bytes 1572868
  0.6 46.2 %copy-start.1 = (bf16[1,128,2048]{2,1,0:T(8,128)(2,1)S(1)}, bf16[1,128,2048]{2,1,0:T(8,128)(2,1)}, u32[]{:S(2)}) copy-start(bf16[1,128,2048]{2,1,0:T(8,128)(2,1)} %param.20) | copy-start | bytes 1572868
  0.7 46.2 %copy-start = (bf16[1,128,2048]{2,1,0:T(8,128)(2,1)S(1)}, bf16[1,128,2048]{2,1,0:T(8,128)(2,1)}, u32[]{:S(2)}) copy-start(bf16[1,128,2048]{2,1,0:T(8,128)(2,1)} %param.19) | copy-start | bytes 1572868
  45.0 30.1 %collective-permute-start = (bf16[256,2048]{1,0:T(8,128)(2,1)S(1)}, bf16[256,2048]{1,0:T(8,128)(2,1)S(1)}, u32[]{:S(2)}, u32[]{:S(2)}) collective-permute-start(bf16[256,2048]{1,0:T(8,128)(2,1)S(1)} %bitcast.19), channel_id=1, source_target_pairs={{0,1},{1,0},{2,3},{3,2},{4,5},{5,4},{6,7},{7,6},{8,9},{9,8},{10,11... | collective-permute-start | bytes 3145736 | tf_op jit(solution)/shard_map/ppermute | solution.py:394
  47.1 21.8 %collective-permute-start.1 = (bf16[192,2048]{1,0:T(8,128)(2,1)S(1)}, bf16[192,2048]{1,0:T(8,128)(2,1)S(1)}, u32[]{:S(2)}, u32[]{:S(2)}) collective-permute-start(bf16[192,2048]{1,0:T(8,128)(2,1)S(1)} %get-tuple-element.30), channel_id=1, source_target_pairs={{0,2},{2,4},{4,6},{6,8},{8,10},{10,12},{12,14},{14,0},{1,3},{3,5},... | collective-permute-start | bytes 2359304 | tf_op jit(solution)/shard_map/ppermute | solution.py:392
  50.6 21.6 %collective-permute-start.2 = (bf16[192,2048]{1,0:T(8,128)(2,1)S(1)}, bf16[192,2048]{1,0:T(8,128)(2,1)S(1)}, u32[]{:S(2)}, u32[]{:S(2)}) collective-permute-start(bf16[192,2048]{1,0:T(8,128)(2,1)S(1)} %get-tuple-element.31), channel_id=1, source_target_pairs={{0,14},{2,0},{4,2},{6,4},{8,6},{10,8},{12,10},{14,12},{1,15},{3,1}... | collective-permute-start | bytes 2359304 | tf_op jit(solution)/shard_map/ppermute | solution.py:393
  75.1 6.4 %copy-start.3 = (bf16[256,2048]{1,0:T(8,128)(2,1)}, bf16[256,2048]{1,0:T(8,128)(2,1)S(1)}, u32[]{:S(2)}) copy-start(bf16[256,2048]{1,0:T(8,128)(2,1)S(1)} %collective-permute-done.par) | copy-start | bytes 3145732
  77.3 4.2 %collective-permute-start.5 = (bf16[8,256,128]{2,1,0:T(8,128)(2,1)S(1)}, bf16[8,256,128]{2,1,0:T(8,128)(2,1)S(1)}, u32[]{:S(2)}, u32[]{:S(2)}) collective-permute-start(bf16[8,256,128]{2,1,0:T(8,128)(2,1)S(1)} %get-tuple-element.39), channel_id=1, source_target_pairs={{0,1},{1,0},{2,3},{3,2},{4,5},{5,4},{6,7},{7,6},{8,9},{9,8},{10,11... | collective-permute-start | bytes 1572872 | tf_op jit(solution)/shard_map/ppermute | solution.py:431
  79.2 10.9 %copy-start.5 = (bf16[256,768]{1,0:T(8,128)(2,1)S(1)}, bf16[256,768]{1,0:T(8,128)(2,1)}, u32[]{:S(2)}) copy-start(bf16[256,768]{1,0:T(8,128)(2,1)} %get-tuple-element.34.mix.mix_h) | copy-start | bytes 1179652
  81.4 34.9 %copy-start.6 = (f32[128,128]{1,0:T(8,128)S(1)}, f32[128,128]{1,0:T(8,128)}, u32[]{:S(2)}) copy-start(f32[128,128]{1,0:T(8,128)} %states.5) | copy-start | bytes 196612
  81.5 38.6 %copy-start.7 = (f32[128,128]{1,0:T(8,128)S(1)}, f32[128,128]{1,0:T(8,128)}, u32[]{:S(2)}) copy-start(f32[128,128]{1,0:T(8,128)} %decay.3) | copy-start | bytes 196612
  81.5 38.6 %copy-start.8 = (bf16[128,128]{1,0:T(8,128)(2,1)S(1)}, bf16[128,128]{1,0:T(8,128)(2,1)}, u32[]{:S(2)}) copy-start(bf16[128,128]{1,0:T(8,128)(2,1)} %gate.3) | copy-start | bytes 98308
  81.5 8.7 %copy-start.4 = (bf16[256,2048]{1,0:T(8,128)(2,1)S(1)}, bf16[256,2048]{1,0:T(8,128)(2,1)}, u32[]{:S(2)}) copy-start(bf16[256,2048]{1,0:T(8,128)(2,1)} %copy-done.3) | copy-start | bytes 3145732
  82.4 25.2 %all-to-all-start.1 = ((bf16[8,256,128]{2,1,0:T(8,128)(2,1)}), bf16[8,256,128]{2,1,0:T(8,128)(2,1)S(1)}, u32[]{:S(2)}, u32[]{:S(2)}) async-start(bf16[8,256,128]{2,1,0:T(8,128)(2,1)} %add_convert_fusion), calls=%async_computation.1 | async-start | bytes 1048576 | tf_op jit(solution)/shard_map/all_to_all | solution.py:445
  93.6 0.9 copy-start.12
  94.5 66.5 %collective-permute-start.3 = (bf16[192,2048]{1,0:T(8,128)(2,1)}, bf16[192,2048]{1,0:T(8,128)(2,1)}, u32[]{:S(2)}, u32[]{:S(2)}) collective-permute-start(bf16[192,2048]{1,0:T(8,128)(2,1)} %get-tuple-element.36), channel_id=1, source_target_pairs={{0,14},{2,0},{4,2},{6,4},{8,6},{10,8},{12,10},{14,12},{1,15},{3,1}... | collective-permute-start | bytes 2359304 | tf_op jit(solution)/shard_map/ppermute | solution.py:441
  108.9 16.2 %all-to-all-start.2 = ((bf16[32,16,128]{2,1,0:T(8,128)(2,1)}), bf16[32,16,128]{2,1,0:T(8,128)(2,1)S(1)}, u32[]{:S(2)}, u32[]{:S(2)}) async-start(bf16[32,16,128]{2,1,0:T(8,128)(2,1)} %shard_map.168), calls=%async_computation.2 | async-start | bytes 262144 | tf_op jit(solution)/shard_map/all_to_all | solution.py:447
  114.4 47.9 %collective-permute-start.4 = (bf16[192,2048]{1,0:T(8,128)(2,1)}, bf16[192,2048]{1,0:T(8,128)(2,1)}, u32[]{:S(2)}, u32[]{:S(2)}) collective-permute-start(bf16[192,2048]{1,0:T(8,128)(2,1)} %copy-done.12), channel_id=1, source_target_pairs={{0,2},{2,4},{4,6},{6,8},{8,10},{10,12},{12,14},{14,0},{1,3},{3,5},... | collective-permute-start | bytes 2359304 | tf_op jit(solution)/shard_map/ppermute | solution.py:442
  116.4 49.6 %collective-permute-start.6 = (f32[1,128]{1,0:T(1,128)S(1)}, f32[1,128]{1,0:T(1,128)S(1)}, u32[]{:S(2)}, u32[]{:S(2)}) collective-permute-start(f32[1,128]{1,0:T(1,128)S(1)} %slice.39), channel_id=1, source_target_pairs={{0,16},{16,32},{32,48},{48,64},{64,80},{80,96},{96,112},{112,128},... | collective-permute-start | bytes 1544 | tf_op jit(solution)/shard_map/ppermute | solution.py:398
  120.7 0.6 copy-start.9
  121.3 0.6 copy-start.10
  121.9 0.6 copy-start.11
  151.4 29.0 %all-to-all-start.3 = ((bf16[32,72,128]{2,1,0:T(8,128)(2,1)}), bf16[32,72,128]{2,1,0:T(8,128)(2,1)S(1)}, u32[]{:S(2)}, u32[]{:S(2)}) async-start(bf16[32,72,128]{2,1,0:T(8,128)(2,1)} %get-tuple-element.43), calls=%async_computation.3 | async-start | bytes 1179648 | tf_op jit(solution)/shard_map/all_to_all | solution.py:477
  161.0 2.5 %copy-start.13 = (f32[384,2048]{1,0:T(8,128)S(1)}, f32[384,2048]{1,0:T(8,128)}, u32[]{:S(2)}) copy-start(f32[384,2048]{1,0:T(8,128)} %get-tuple-element.35) | copy-start | bytes 9437188

commit v5 on v4

--- a/solution.py
+++ b/solution.py
@@ -202,7 +202,7 @@
         out[k] = p[:, k * width : (k + 1) * width].astype(out.dtype)
 
 
-def expert_body(place, par, part, w_s, psend, mix_h, mix, sems):
+def expert_body(place, par, part, w_s, psend, pair, mix_h, mix, sems):
     units = w_s.shape[1]
     gate = part[0] + product(0, par, w_s, ())
     up = part[1] + product(1, par, w_s, ())
@@ -216,16 +216,26 @@
     mix[:, 2 * units :] = (silu * up).astype(BF16)
     (kept,) = copies(((mix, mix_h),), sems)
     partials(psend, gb, ub, w_s)
+    pair[:, 0:units] = gb
+    pair[:, units:] = ub
     kept.wait()
 
 
-def keep_body(place, mix_h, wg, wu, wd, wa, wb, pkeep, w_s, mix, sems):
-    where = columns(place[0], w_s.shape[2])
+def keep_body(place, pair, w_s, pkeep):
     units = w_s.shape[1]
-    pairs = weight_copies(wg, wu, wd, wa, wb, w_s, where, 2)
-    for copy in copies([(mix_h.at[:, pl.ds(0, 2 * units)], mix)] + pairs, sems):
+    partials(pkeep, pair[:, 0:units], pair[:, units:], w_s)
+
+
+def fetch_body(place, pick_h, og_h, w_h, gated_h, weight_h, tail_h, pick, og, w, gated, weight, tail, sems):
+    there = og_h.at[:, columns(place[3], og.shape[1])]
+    for copy in copies(
+        (
+            (pick_h, pick), (there, og), (w_h, w),
+            (gated_h, gated), (weight_h, weight), (tail_h, tail),
+        ),
+        sems,
+    ):
         copy.wait()
-    partials(pkeep, mix[:, 0:units], mix[:, units:], w_s)
 
 
 def weight_body(place, own, par, mix, gown_h, ga, gb, gown, sems):
@@ -263,36 +273,22 @@
     out[...] = jnp.concatenate(both, axis=1).astype(BF16)
 
 
-def combine_body(place, pick_h, back, og_h, mid, pick, og, sems):
-    n = mid.shape[1]
-    got = copies(((pick_h, pick), (og_h.at[:, columns(place[3], n)], og)), sems)
-    got[0].wait()
-    part = tn(pick[...], back[...])
-    got[1].wait()
-    mid[...] = (og[...].astype(F32) + part).astype(BF16)
-
-
-def project_body(
-    place, mid, gated_h, w_h, weight_h, tail_h, out_h, act_o, gated, w, weight, tail, out, sems
-):
-    got = copies(
-        ((gated_h, gated), (w_h, w), (weight_h, weight), (tail_h, tail)), sems
-    )
+def combine_body(place, pick, back, og, mid):
+    mid[...] = (og[...].astype(F32) + tn(pick[...], back[...])).astype(BF16)
+
+
+def project_body(place, mid, gated, w, weight, tail, out_h, act_o, out, sems):
     pieces = mid.shape[0]
     ys = pieces // 2
     full = jnp.concatenate([mid[(b % ys) * 2 + b // ys] for b in range(pieces)], axis=1)
     dests, rows = out.shape[0], full.shape[1] // out.shape[0]
-    got[0].wait()
     grad = tn(full, gated[...]).astype(BF16)
     for d in range(dests):
         out[d, 0:rows, :] = grad[d * rows : (d + 1) * rows]
     head, rest = pl.ds(0, rows), pl.ds(rows, out.shape[1] - rows)
-    sent = copies(((out.at[:, head], out_h.at[:, head]),), sems.at[pl.ds(4, 1)])
-    got[1].wait()
+    sent = copies(((out.at[:, head], out_h.at[:, head]),), sems.at[pl.ds(0, 1)])
     act = nn(full, w[...])
     act_o[...] = act
-    got[2].wait()
-    got[3].wait()
     total = jnp.sum(weight[...] * act, axis=0, keepdims=True)
     extra = tail[...]
     line = lax.broadcasted_iota(jnp.int32, extra.shape, 0)
@@ -301,7 +297,7 @@
     extra = extra.astype(BF16)
     for d in range(dests):
         out[d, rows:, :] = extra
-    sent += copies(((out.at[:, rest], out_h.at[:, rest]),), sems.at[pl.ds(5, 1)])
+    sent += copies(((out.at[:, rest], out_h.at[:, rest]),), sems.at[pl.ds(1, 1)])
     for copy in sent:
         copy.wait()
 
@@ -404,30 +400,24 @@
 
     slots = n_sp * half
     wide = cols // n_y
-    held = pltpu.VMEM((3, units, cols), BF16)
     weights = (wg, wu, wd, wa, wb)
-    part, other = call(
+    part, other, mine = call(
         first_body,
-        [shape((3, slots, units), F32), shape((3, units, cols), BF16)],
+        [shape((3, slots, units), F32)] + [shape((3, units, cols), BF16)] * 2,
         place, own, *weights,
-        specs=(1, 2, 3), free=(4, 5),
-        scratch=[held, pltpu.SemaphoreType.DMA((18,))],
-    )
-    psend, mix = call(
+        specs=(1, 2, 3), free=(4, 5), scratch=[pltpu.SemaphoreType.DMA((18,))],
+    )
+    psend, pair, mix = call(
         expert_body,
-        [shape((n_y, slots, wide), BF16), shape((slots, 3 * units), BF16)],
+        [
+            shape((n_y, slots, wide), BF16), shape((slots, 2 * units), BF16),
+            shape((slots, 3 * units), BF16),
+        ],
         place, par, part, other,
-        outs_in=(1,),
+        outs_in=(2,),
         scratch=[pltpu.VMEM((slots, 3 * units), BF16), pltpu.SemaphoreType.DMA((1,))],
     )
-    pkeep = call(
-        keep_body, shape((n_y, slots, wide), F32), place, mix, *weights,
-        specs=(0, 1, 2, 3), free=(4, 5),
-        scratch=[
-            pltpu.VMEM((2, units, cols), BF16), pltpu.VMEM((slots, 2 * units), BF16),
-            pltpu.SemaphoreType.DMA((7,)),
-        ],
-    )
+    pkeep = call(keep_body, shape((n_y, slots, wide), F32), place, pair, mine)
     precv = lax.ppermute(psend, "c", swap)
     gown, ga, gb = call(
         weight_body,
@@ -438,6 +428,15 @@
             pltpu.VMEM((2, 3 * hidden, cols), F32), pltpu.SemaphoreType.DMA((6,)),
         ],
     )
+    pick, og, w_p, gated, weight, tails = call(
+        fetch_body,
+        [
+            shape(pick.shape, BF16), shape((tokens, ch), BF16), shape(w_proj.shape, BF16),
+            shape(gated.shape, BF16), shape(weight.shape, F32), shape(tails.shape, F32),
+        ],
+        place, pick, out_grad, w_proj, gated, weight, tails,
+        specs=tuple(range(6)), scratch=[pltpu.SemaphoreType.DMA((6,))],
+    )
     back_lo = lax.ppermute(ga, Y, ring(-1))
     back_hi = lax.ppermute(gb, Y, ring(1))
 
@@ -448,12 +447,7 @@
     mid = call(
         combine_body,
         shape((tokens, ch), BF16),
-        place, pick, back.reshape(n_sp * cap, wide), out_grad,
-        specs=(0, 2),
-        scratch=[
-            pltpu.VMEM((n_sp * cap, tokens), BF16), pltpu.VMEM((tokens, ch), BF16),
-            pltpu.SemaphoreType.DMA((2,)),
-        ],
+        place, pick, back.reshape(n_sp * cap, wide), og,
     )
     mid = lax.all_gather(mid, TP)
 
@@ -462,12 +456,10 @@
     out, act = call(
         project_body,
         [shape((n_sp, rows + tail, ch), BF16), row(F32)],
-        place, mid, gated, w_proj, weight, tails,
-        specs=(1, 2, 3, 4), outs_in=(0,),
+        place, mid, gated, w_p, weight, tails,
+        outs_in=(0,),
         scratch=[
-            pltpu.VMEM((tokens, ch), BF16), pltpu.VMEM((width, ch), BF16),
-            pltpu.VMEM((tokens, ch), F32), pltpu.VMEM((tail, ch), F32),
-            pltpu.VMEM((n_sp, rows + tail, ch), BF16), pltpu.SemaphoreType.DMA((6,)),
+            pltpu.VMEM((n_sp, rows + tail, ch), BF16), pltpu.SemaphoreType.DMA((2,)),
         ],
     )
     branch, loc, prod = call(

time: 183 us -> 181 us (0.989)
    all_to_all x1, waiting for transfers between devices: 2.53 us -> 0.66 us  [local(): back = lax.all_to_all(ret, SP, 0, 0, tiled=True)]
    pallas_call x11 -> x12, Pallas kernels: 22.6 us -> 21.2 us  [call(): pl.pallas_call(body, grid_spec=pltpu.PrefetchScalarGridSpec(num_scalar_pr...]
  transfers between devices with their start and end apart: 10 -> 10, of which waited for: 5 -> 6; matrix products, arithmetic and copies ran while one was open for 2% -> 2% of each run, Pallas kernels for 9% -> 8%
where the time goes in v5:
time: 181 us; the launch traced here: 180 us
  blocking collectives  63.7 us (35%)
  waiting for transfers between devices  46.2 us (26%)
  starting transfers between devices  40.2 us (22%)
  Pallas kernels  21.4 us (12%)
  local copies, waits for them, and re-layouts  5.23 us (3%)
  other arithmetic  2.38 us (1%)
    all_to_all x1, blocking collectives, local(): own = lax.all_to_all(send.reshape(n_sp, half, width), SP, 0, 0, tiled=True)  41.2 us
    all_gather x1, blocking collectives, local(): mid = lax.all_gather(mid, TP)  22.5 us
    pallas_call x12, Pallas kernels, call(): pl.pallas_call(body, grid_spec=pltpu.PrefetchScalarGridSpec(num_scalar_pr...  21.2 us
    ppermute x1, waiting for transfers between devices, local(): wa = lax.ppermute(w_lo, Y, ring(1))  16 us
    all_to_all x1, waiting for transfers between devices, local(): got = lax.all_to_all(out, SP, 0, 0, tiled=True)  14.4 us
    all_to_all x1, waiting for transfers between devices, local(): parts = lax.all_to_all(psum, Y, 0, 0, tiled=True)  11.1 us
    all_to_all x1, starting transfers between devices, local(): got = lax.all_to_all(out, SP, 0, 0, tiled=True)  9.5 us
    all_to_all x1, starting transfers between devices, local(): parts = lax.all_to_all(psum, Y, 0, 0, tiled=True)  7.76 us
  transfers between devices with their start and end apart: 10, of which 6 were waited for; matrix products, arithmetic and copies ran while one was open for 2% of the time, Pallas kernels for 8%

profile of v5, /device:TPU:8, one launch (start us, length us, event | category | flops | bytes accessed | tf_op | source)
XLA Modules:
  0.0 180.1 jit_solution(17178475611648992371)
XLA Ops:
  0.6 0.0 copy-start
  0.6 0.0 copy-start.1
  0.7 0.0 copy-start.2
  0.7 0.1 pad_add_fusion.place
  0.8 3.0 %shard_map.162 = (bf16[256,2048]{1,0:T(8,128)(2,1)}, bf16[512,128]{1,0:T(8,128)(2,1)}) custom-call(s32[4]{0:T(128)S(1)} %pad_add_fusion.place, s32[2,128]{1,0:T(2,128)} %bitcast.31, f32[2,128]{1,0:T(2,128)} %bitcast.32, bf16[128,2048]{1,0:T(8,128)(2,1)} %x_h.1, bf16[128,2048]{1,0:T(8,128)(2,1)} %og_h.3), custom_call_target="tpu_custom_call" | custom-call | tf_op jit(solution)/shard_map/pallas_call | solution.py:71
  3.7 41.2 %all_to_all.20 = bf16[32,8,2048]{2,1,0:T(8,128)(2,1)S(1)} all-to-all(bf16[32,8,2048]{2,1,0:T(8,128)(2,1)} %bitcast.30), channel_id=1, replica_groups=mesh['z'=8,'x'=4,'yh'=4,'yl'=2,'c'=2] {'z','x'}, dimensions={0} | all-to-all | bytes 2097152 | tf_op jit(solution)/shard_map/all_to_all | solution.py:376
  45.0 1.9 %collective-permute-start = (bf16[256,2048]{1,0:T(8,128)(2,1)S(1)}, bf16[256,2048]{1,0:T(8,128)(2,1)S(1)}, u32[]{:S(2)}, u32[]{:S(2)}) collective-permute-start(bf16[256,2048]{1,0:T(8,128)(2,1)S(1)} %bitcast.19), channel_id=1, source_target_pairs={{0,1},{1,0},{2,3},{3,2},{4,5},{5,4},{6,7},{7,6},{8,9},{9,8},{10,11... | collective-permute-start | bytes 3145736 | tf_op jit(solution)/shard_map/ppermute | solution.py:390
  46.9 0.0 copy-done
  46.9 0.0 copy-done.1
  46.9 0.0 copy-done.2
  46.9 0.2 shard_map.163
  47.1 3.5 %collective-permute-start.1 = (bf16[192,2048]{1,0:T(8,128)(2,1)S(1)}, bf16[192,2048]{1,0:T(8,128)(2,1)S(1)}, u32[]{:S(2)}, u32[]{:S(2)}) collective-permute-start(bf16[192,2048]{1,0:T(8,128)(2,1)S(1)} %get-tuple-element.38), channel_id=1, source_target_pairs={{0,2},{2,4},{4,6},{6,8},{8,10},{10,12},{12,14},{14,0},{1,3},{3,5},... | collective-permute-start | bytes 2359304 | tf_op jit(solution)/shard_map/ppermute | solution.py:388
  50.6 2.4 %collective-permute-start.2 = (bf16[192,2048]{1,0:T(8,128)(2,1)S(1)}, bf16[192,2048]{1,0:T(8,128)(2,1)S(1)}, u32[]{:S(2)}, u32[]{:S(2)}) collective-permute-start(bf16[192,2048]{1,0:T(8,128)(2,1)S(1)} %get-tuple-element.39), channel_id=1, source_target_pairs={{0,14},{2,0},{4,2},{6,4},{8,6},{10,8},{12,10},{14,12},{1,15},{3,1}... | collective-permute-start | bytes 2359304 | tf_op jit(solution)/shard_map/ppermute | solution.py:389
  52.9 16.0 %collective-permute-done.1.wa = bf16[192,2048]{1,0:T(8,128)(2,1)S(1)} collective-permute-done((bf16[192,2048]{1,0:T(8,128)(2,1)S(1)}, bf16[192,2048]{1,0:T(8,128)(2,1)S(1)}, u32[]{:S(2)}, u32[]{:S(2)}) %collective-permute-start.1) | collective-permute-done | bytes 786464 | tf_op jit(solution)/shard_map/ppermute | solution.py:388
  68.9 3.2 %collective-permute-done.2.wb = bf16[192,2048]{1,0:T(8,128)(2,1)S(1)} collective-permute-done((bf16[192,2048]{1,0:T(8,128)(2,1)S(1)}, bf16[192,2048]{1,0:T(8,128)(2,1)S(1)}, u32[]{:S(2)}, u32[]{:S(2)}) %collective-permute-start.2) | collective-permute-done | bytes 786464 | tf_op jit(solution)/shard_map/ppermute | solution.py:389
  72.1 2.9 %shard_map.164 = (f32[3,256,256]{2,1,0:T(8,128)S(1)}, bf16[3,256,1024]{2,1,0:T(8,128)(2,1)S(1)}, bf16[3,256,1024]{2,1,0:T(8,128)(2,1)S(1)}) custom-call(s32[4]{0:T(128)S(1)} %pad_add_fusion.place, bf16[256,2048]{1,0:T(8,128)(2,1)S(1)} %bitcast.20, bf16[128,2048]{1,0:T(8,128)(2,1)} %bitcast.22, bf16[128,2048]{1,0:T(8,128)(2,1)} %bitcast.24, ...), custom_call_target="tpu_custom_call" | custom-call | tf_op jit(solution)/shard_map/pallas_call | solution.py:71
  75.1 0.0 collective-permute-done.par
  75.1 2.2 %shard_map.165 = (bf16[8,256,128]{2,1,0:T(8,128)(2,1)S(1)}, bf16[256,512]{1,0:T(8,128)(2,1)S(1)}, bf16[256,768]{1,0:T(8,128)(2,1)}) custom-call(s32[4]{0:T(128)S(1)} %pad_add_fusion.place, bf16[256,2048]{1,0:T(8,128)(2,1)S(1)} %collective-permute-done.par, f32[3,256,256]{2,1,0:T(8,128)S(1)} %get-tuple-element.40.part, ...), custom_call_target="tpu_custom_call" | custom-call | tf_op jit(solution)/shard_map/pallas_call | solution.py:71
  77.3 0.0 copy-start.4
  77.3 2.1 %collective-permute-start.5 = (bf16[8,256,128]{2,1,0:T(8,128)(2,1)S(1)}, bf16[8,256,128]{2,1,0:T(8,128)(2,1)S(1)}, u32[]{:S(2)}, u32[]{:S(2)}) collective-permute-start(bf16[8,256,128]{2,1,0:T(8,128)(2,1)S(1)} %get-tuple-element.53), channel_id=1, source_target_pairs={{0,1},{1,0},{2,3},{3,2},{4,5},{5,4},{6,7},{7,6},{8,9},{9,8},{10,11... | collective-permute-start | bytes 1572872 | tf_op jit(solution)/shard_map/ppermute | solution.py:421
  79.4 1.0 shard_map.169
  80.4 0.0 copy-start.3
  80.4 0.0 copy-start.5
  80.4 0.0 copy-start.6
  80.4 0.9 collective-permute-done.5
  81.3 0.9 add_convert_fusion
  82.2 7.8 %all-to-all-start.1 = ((bf16[8,256,128]{2,1,0:T(8,128)(2,1)}), bf16[8,256,128]{2,1,0:T(8,128)(2,1)S(1)}, u32[]{:S(2)}, u32[]{:S(2)}) async-start(bf16[8,256,128]{2,1,0:T(8,128)(2,1)} %add_convert_fusion), calls=%async_computation.1 | async-start | bytes 1048576 | tf_op jit(solution)/shard_map/all_to_all | solution.py:444
  89.9 0.0 copy-done.4
  89.9 3.4 %shard_map.166 = (f32[384,2048]{1,0:T(8,128)}, bf16[192,2048]{1,0:T(8,128)(2,1)}, bf16[192,2048]{1,0:T(8,128)(2,1)S(1)}) custom-call(s32[4]{0:T(128)S(1)} %pad_add_fusion.place, bf16[256,2048]{1,0:T(8,128)(2,1)S(1)} %bitcast.21, bf16[256,2048]{1,0:T(8,128)(2,1)S(1)} %collective-permute-done.par, bf16[256,768]{1,0:T(8,128)(2,1)S(1)} %copy-done.4), custom_call_target="tpu_custom_call" | custom-call | tf_op jit(solution)/shard_map/pallas_call | solution.py:71
  93.3 0.0 copy-start.10
  93.3 0.9 copy-done.10
  94.2 1.9 %collective-permute-start.3 = (bf16[192,2048]{1,0:T(8,128)(2,1)}, bf16[192,2048]{1,0:T(8,128)(2,1)}, u32[]{:S(2)}, u32[]{:S(2)}) collective-permute-start(bf16[192,2048]{1,0:T(8,128)(2,1)} %get-tuple-element.44), channel_id=1, source_target_pairs={{0,14},{2,0},{4,2},{6,4},{8,6},{10,8},{12,10},{14,12},{1,15},{3,1}... | collective-permute-start | bytes 2359304 | tf_op jit(solution)/shard_map/ppermute | solution.py:440
  96.1 11.1 %all-to-all-done.1.parts = bf16[8,256,128]{2,1,0:T(8,128)(2,1)S(1)} async-done(((bf16[8,256,128]{2,1,0:T(8,128)(2,1)}), bf16[8,256,128]{2,1,0:T(8,128)(2,1)S(1)}, u32[]{:S(2)}, u32[]{:S(2)}) %all-to-all-start.1) | async-done | bytes 524320 | tf_op jit(solution)/shard_map/all_to_all | solution.py:444
  107.3 1.3 shard_map.170
  108.5 5.6 %all-to-all-start.2 = ((bf16[32,16,128]{2,1,0:T(8,128)(2,1)}), bf16[32,16,128]{2,1,0:T(8,128)(2,1)S(1)}, u32[]{:S(2)}, u32[]{:S(2)}) async-start(bf16[32,16,128]{2,1,0:T(8,128)(2,1)} %shard_map.170), calls=%async_computation.2 | async-start | bytes 262144 | tf_op jit(solution)/shard_map/all_to_all | solution.py:446
  114.1 1.9 %collective-permute-start.4 = (bf16[192,2048]{1,0:T(8,128)(2,1)}, bf16[192,2048]{1,0:T(8,128)(2,1)}, u32[]{:S(2)}, u32[]{:S(2)}) collective-permute-start(bf16[192,2048]{1,0:T(8,128)(2,1)} %copy-done.10), channel_id=1, source_target_pairs={{0,2},{2,4},{4,6},{6,8},{8,10},{10,12},{12,14},{14,0},{1,3},{3,5},... | collective-permute-start | bytes 2359304 | tf_op jit(solution)/shard_map/ppermute | solution.py:441
  116.0 0.0 copy-done.3
  116.0 3.7 %collective-permute-start.6 = (f32[1,128]{1,0:T(1,128)S(1)}, f32[1,128]{1,0:T(1,128)S(1)}, u32[]{:S(2)}, u32[]{:S(2)}) collective-permute-start(f32[1,128]{1,0:T(1,128)S(1)} %slice.39), channel_id=1, source_target_pairs={{0,16},{16,32},{32,48},{48,64},{64,80},{80,96},{96,112},{112,128},... | collective-permute-start | bytes 1544 | tf_op jit(solution)/shard_map/ppermute | solution.py:394
  119.7 0.0 copy-done.5
  119.8 0.0 copy-done.6
  119.8 0.6 shard_map.167
  120.4 0.0 copy-start.7
  120.4 0.6 copy-done.7
  121.0 0.0 copy-start.8
  121.0 0.6 copy-done.8
  121.6 0.0 copy-start.9
  121.6 0.6 copy-done.9
  122.2 1.7 shard_map.168
  123.9 0.7 all-to-all-done.2
  124.6 0.8 shard_map.171
  125.4 22.5 %all-gather = bf16[2048,128]{1,0:T(8,128)(2,1)S(1)} all-gather(bf16[128,128]{1,0:T(8,128)(2,1)S(1)} %shard_map.171), channel_id=2, replica_groups=mesh['z'=8,'x'=4,'yh'=4,'yl'=2,'c'=2] {'yh','yl','c'}, dimensions={0}, use_global_device_ids=true | all-gather | bytes 557056 | tf_op jit(solution)/shard_map/all_gather | solution.py:452
  147.9 1.8 %shard_map.172 = (bf16[32,72,128]{2,1,0:T(8,128)(2,1)}, f32[128,128]{1,0:T(8,128)S(1)}) custom-call(s32[4]{0:T(128)S(1)} %pad_add_fusion.place, bf16[16,128,128]{2,1,0:T(8,128)(2,1)S(1)} %bitcast.28, bf16[128,128]{1,0:T(8,128)(2,1)S(1)} %get-tuple-element.55.gated, bf16[2048,128]{1,0:T(8,128)(2,1)S(1)} %get-tuple-element.56.w, ...), custom_call_target="tpu_custom_call" | custom-call | tf_op jit(solution)/shard_map/pallas_call | solution.py:71
  149.7 9.5 %all-to-all-start.3 = ((bf16[32,72,128]{2,1,0:T(8,128)(2,1)}), bf16[32,72,128]{2,1,0:T(8,128)(2,1)S(1)}, u32[]{:S(2)}, u32[]{:S(2)}) async-start(bf16[32,72,128]{2,1,0:T(8,128)(2,1)} %get-tuple-element.59), calls=%async_computation.3 | async-start | bytes 1179648 | tf_op jit(solution)/shard_map/all_to_all | solution.py:469
  159.2 0.0 copy-start.11
  159.2 0.0 collective-permute-done.3
  159.3 1.3 fusion.3
  160.6 0.0 collective-permute-done.4
  160.6 1.2 fusion.4
  161.7 0.0 copy-done.11
  161.8 1.4 fusion.2
  163.2 1.2 shard_map.173
  164.3 0.0 collective-permute-done.6.before
  164.3 14.4 %all-to-all-done.3.got = bf16[32,72,128]{2,1,0:T(8,128)(2,1)S(1)} async-done(((bf16[32,72,128]{2,1,0:T(8,128)(2,1)}), bf16[32,72,128]{2,1,0:T(8,128)(2,1)S(1)}, u32[]{:S(2)}, u32[]{:S(2)}) %all-to-all-start.3) | async-done | bytes 589856 | tf_op jit(solution)/shard_map/all_to_all | solution.py:469
  178.7 1.3 shard_map.174
  (1 shorter events, 0.0 us)
Async XLA Ops:
  0.6 46.2 %copy-start = (bf16[1,128,2048]{2,1,0:T(8,128)(2,1)S(1)}, bf16[1,128,2048]{2,1,0:T(8,128)(2,1)}, u32[]{:S(2)}) copy-start(bf16[1,128,2048]{2,1,0:T(8,128)(2,1)} %param.19) | copy-start | bytes 1572868
  0.6 46.2 %copy-start.1 = (bf16[1,128,2048]{2,1,0:T(8,128)(2,1)S(1)}, bf16[1,128,2048]{2,1,0:T(8,128)(2,1)}, u32[]{:S(2)}) copy-start(bf16[1,128,2048]{2,1,0:T(8,128)(2,1)} %param.20) | copy-start | bytes 1572868
  0.7 46.2 %copy-start.2 = (bf16[1,128,2048]{2,1,0:T(8,128)(2,1)S(1)}, bf16[1,128,2048]{2,1,0:T(8,128)(2,1)}, u32[]{:S(2)}) copy-start(bf16[1,128,2048]{2,1,0:T(8,128)(2,1)} %param.21) | copy-start | bytes 1572868
  45.0 30.1 %collective-permute-start = (bf16[256,2048]{1,0:T(8,128)(2,1)S(1)}, bf16[256,2048]{1,0:T(8,128)(2,1)S(1)}, u32[]{:S(2)}, u32[]{:S(2)}) collective-permute-start(bf16[256,2048]{1,0:T(8,128)(2,1)S(1)} %bitcast.19), channel_id=1, source_target_pairs={{0,1},{1,0},{2,3},{3,2},{4,5},{5,4},{6,7},{7,6},{8,9},{9,8},{10,11... | collective-permute-start | bytes 3145736 | tf_op jit(solution)/shard_map/ppermute | solution.py:390
  47.1 21.8 %collective-permute-start.1 = (bf16[192,2048]{1,0:T(8,128)(2,1)S(1)}, bf16[192,2048]{1,0:T(8,128)(2,1)S(1)}, u32[]{:S(2)}, u32[]{:S(2)}) collective-permute-start(bf16[192,2048]{1,0:T(8,128)(2,1)S(1)} %get-tuple-element.38), channel_id=1, source_target_pairs={{0,2},{2,4},{4,6},{6,8},{8,10},{10,12},{12,14},{14,0},{1,3},{3,5},... | collective-permute-start | bytes 2359304 | tf_op jit(solution)/shard_map/ppermute | solution.py:388
  50.6 21.6 %collective-permute-start.2 = (bf16[192,2048]{1,0:T(8,128)(2,1)S(1)}, bf16[192,2048]{1,0:T(8,128)(2,1)S(1)}, u32[]{:S(2)}, u32[]{:S(2)}) collective-permute-start(bf16[192,2048]{1,0:T(8,128)(2,1)S(1)} %get-tuple-element.39), channel_id=1, source_target_pairs={{0,14},{2,0},{4,2},{6,4},{8,6},{10,8},{12,10},{14,12},{1,15},{3,1}... | collective-permute-start | bytes 2359304 | tf_op jit(solution)/shard_map/ppermute | solution.py:389
  77.3 12.6 %copy-start.4 = (bf16[256,768]{1,0:T(8,128)(2,1)S(1)}, bf16[256,768]{1,0:T(8,128)(2,1)}, u32[]{:S(2)}) copy-start(bf16[256,768]{1,0:T(8,128)(2,1)} %get-tuple-element.42.mix) | copy-start | bytes 1179652
  77.3 3.9 %collective-permute-start.5 = (bf16[8,256,128]{2,1,0:T(8,128)(2,1)S(1)}, bf16[8,256,128]{2,1,0:T(8,128)(2,1)S(1)}, u32[]{:S(2)}, u32[]{:S(2)}) collective-permute-start(bf16[8,256,128]{2,1,0:T(8,128)(2,1)S(1)} %get-tuple-element.53), channel_id=1, source_target_pairs={{0,1},{1,0},{2,3},{3,2},{4,5},{5,4},{6,7},{7,6},{8,9},{9,8},{10,11... | collective-permute-start | bytes 1572872 | tf_op jit(solution)/shard_map/ppermute | solution.py:421
  80.4 35.7 %copy-start.3 = (f32[128,128]{1,0:T(8,128)S(1)}, f32[128,128]{1,0:T(8,128)}, u32[]{:S(2)}) copy-start(f32[128,128]{1,0:T(8,128)} %states.5) | copy-start | bytes 196612
  80.4 39.4 %copy-start.5 = (f32[128,128]{1,0:T(8,128)S(1)}, f32[128,128]{1,0:T(8,128)}, u32[]{:S(2)}) copy-start(f32[128,128]{1,0:T(8,128)} %decay.3) | copy-start | bytes 196612
  80.4 39.4 %copy-start.6 = (bf16[128,128]{1,0:T(8,128)(2,1)S(1)}, bf16[128,128]{1,0:T(8,128)(2,1)}, u32[]{:S(2)}) copy-start(bf16[128,128]{1,0:T(8,128)(2,1)} %gate.3) | copy-start | bytes 98308
  82.2 25.1 %all-to-all-start.1 = ((bf16[8,256,128]{2,1,0:T(8,128)(2,1)}), bf16[8,256,128]{2,1,0:T(8,128)(2,1)S(1)}, u32[]{:S(2)}, u32[]{:S(2)}) async-start(bf16[8,256,128]{2,1,0:T(8,128)(2,1)} %add_convert_fusion), calls=%async_computation.1 | async-start | bytes 1048576 | tf_op jit(solution)/shard_map/all_to_all | solution.py:444
  93.3 0.9 copy-start.10
  94.2 65.0 %collective-permute-start.3 = (bf16[192,2048]{1,0:T(8,128)(2,1)}, bf16[192,2048]{1,0:T(8,128)(2,1)}, u32[]{:S(2)}, u32[]{:S(2)}) collective-permute-start(bf16[192,2048]{1,0:T(8,128)(2,1)} %get-tuple-element.44), channel_id=1, source_target_pairs={{0,14},{2,0},{4,2},{6,4},{8,6},{10,8},{12,10},{14,12},{1,15},{3,1}... | collective-permute-start | bytes 2359304 | tf_op jit(solution)/shard_map/ppermute | solution.py:440
  108.5 16.1 %all-to-all-start.2 = ((bf16[32,16,128]{2,1,0:T(8,128)(2,1)}), bf16[32,16,128]{2,1,0:T(8,128)(2,1)S(1)}, u32[]{:S(2)}, u32[]{:S(2)}) async-start(bf16[32,16,128]{2,1,0:T(8,128)(2,1)} %shard_map.170), calls=%async_computation.2 | async-start | bytes 262144 | tf_op jit(solution)/shard_map/all_to_all | solution.py:446
  114.1 46.5 %collective-permute-start.4 = (bf16[192,2048]{1,0:T(8,128)(2,1)}, bf16[192,2048]{1,0:T(8,128)(2,1)}, u32[]{:S(2)}, u32[]{:S(2)}) collective-permute-start(bf16[192,2048]{1,0:T(8,128)(2,1)} %copy-done.10), channel_id=1, source_target_pairs={{0,2},{2,4},{4,6},{6,8},{8,10},{10,12},{12,14},{14,0},{1,3},{3,5},... | collective-permute-start | bytes 2359304 | tf_op jit(solution)/shard_map/ppermute | solution.py:441
  116.0 48.3 %collective-permute-start.6 = (f32[1,128]{1,0:T(1,128)S(1)}, f32[1,128]{1,0:T(1,128)S(1)}, u32[]{:S(2)}, u32[]{:S(2)}) collective-permute-start(f32[1,128]{1,0:T(1,128)S(1)} %slice.39), channel_id=1, source_target_pairs={{0,16},{16,32},{32,48},{48,64},{64,80},{80,96},{96,112},{112,128},... | collective-permute-start | bytes 1544 | tf_op jit(solution)/shard_map/ppermute | solution.py:394
  120.4 0.6 copy-start.7
  121.0 0.6 copy-start.8
  121.6 0.6 copy-start.9
  149.7 29.0 %all-to-all-start.3 = ((bf16[32,72,128]{2,1,0:T(8,128)(2,1)}), bf16[32,72,128]{2,1,0:T(8,128)(2,1)S(1)}, u32[]{:S(2)}, u32[]{:S(2)}) async-start(bf16[32,72,128]{2,1,0:T(8,128)(2,1)} %get-tuple-element.59), calls=%async_computation.3 | async-start | bytes 1179648 | tf_op jit(solution)/shard_map/all_to_all | solution.py:469
  159.2 2.5 %copy-start.11 = (f32[384,2048]{1,0:T(8,128)S(1)}, f32[384,2048]{1,0:T(8,128)}, u32[]{:S(2)}) copy-start(f32[384,2048]{1,0:T(8,128)} %get-tuple-element.43) | copy-start | bytes 9437188

commit v6 on v5

--- a/solution.py
+++ b/solution.py
@@ -182,7 +182,13 @@
     return nt(side, w_s[k])
 
 
-def first_body(place, own, wg, wu, wd, wa, wb, part, other, w_s, sems):
+def hold_body(place, wg, wu, wd, w, sems):
+    for copy in copies([(v, w.at[k]) for k, v in enumerate((wg, wu, wd))], sems):
+        copy.wait()
+
+
+def first_body(place, own, w, wa, wb, part, other, w_s, sems):
+    wg, wu, wd = (w.at[k] for k in range(3))
     cols = w_s.shape[2]
     sides = (w_s, columns(place[0], cols)), (other, columns(1 - place[0], cols))
     pairs = []
@@ -400,12 +406,15 @@
 
     slots = n_sp * half
     wide = cols // n_y
-    weights = (wg, wu, wd, wa, wb)
+    held = call(
+        hold_body, shape((3, hidden, width), BF16), place, wg, wu, wd,
+        specs=(0, 1, 2), scratch=[pltpu.SemaphoreType.DMA((3,))],
+    )
     part, other, mine = call(
         first_body,
         [shape((3, slots, units), F32)] + [shape((3, units, cols), BF16)] * 2,
-        place, own, *weights,
-        specs=(1, 2, 3), free=(4, 5), scratch=[pltpu.SemaphoreType.DMA((18,))],
+        place, own, held, wa, wb,
+        free=(1, 2, 3), scratch=[pltpu.SemaphoreType.DMA((18,))],
     )
     psend, pair, mix = call(
         expert_body,

time: 181 us -> 180 us (level)
    ppermute x1, waiting for transfers between devices: 16 us -> 14 us  [local(): wa = lax.ppermute(w_lo, Y, ring(1))]
    pallas_call x12 -> x13, Pallas kernels: 21.2 us -> 22.6 us  [call(): pl.pallas_call(body, grid_spec=pltpu.PrefetchScalarGridSpec(num_scalar_pr...]
  transfers between devices with their start and end apart: 10 -> 10, of which waited for: 6 -> 6; matrix products, arithmetic and copies ran while one was open for 2% -> 1% of each run, Pallas kernels for 8% -> 9%
where the time goes in v6:
time: 180 us; the launch traced here: 179 us
  blocking collectives  63.8 us (35%)
  waiting for transfers between devices  44.9 us (25%)
  starting transfers between devices  40 us (22%)
  Pallas kernels  22.7 us (13%)
  local copies, waits for them, and re-layouts  4.59 us (3%)
  other arithmetic  2.33 us (1%)
    all_to_all x1, blocking collectives, local(): own = lax.all_to_all(send.reshape(n_sp, half, width), SP, 0, 0, tiled=True)  41.2 us
    pallas_call x13, Pallas kernels, call(): pl.pallas_call(body, grid_spec=pltpu.PrefetchScalarGridSpec(num_scalar_pr...  22.6 us
    all_gather x1, blocking collectives, local(): mid = lax.all_gather(mid, TP)  22.5 us
    all_to_all x1, waiting for transfers between devices, local(): got = lax.all_to_all(out, SP, 0, 0, tiled=True)  15.1 us
    ppermute x1, waiting for transfers between devices, local(): wa = lax.ppermute(w_lo, Y, ring(1))  14 us
    all_to_all x1, waiting for transfers between devices, local(): parts = lax.all_to_all(psum, Y, 0, 0, tiled=True)  11.1 us
    all_to_all x1, starting transfers between devices, local(): got = lax.all_to_all(out, SP, 0, 0, tiled=True)  9.51 us
    all_to_all x1, starting transfers between devices, local(): parts = lax.all_to_all(psum, Y, 0, 0, tiled=True)  7.75 us
  transfers between devices with their start and end apart: 10, of which 6 were waited for; matrix products, arithmetic and copies ran while one was open for 1% of the time, Pallas kernels for 9%

profile of v6, /device:TPU:8, one launch (start us, length us, event | category | flops | bytes accessed | tf_op | source)
XLA Modules:
  0.0 179.3 jit_solution(11584233795113812581)
XLA Ops:
  0.6 0.1 pad_add_fusion.place
  0.7 0.0 copy-start
  0.7 0.0 copy-start.1
  0.7 0.0 copy-start.2
  0.7 3.0 %shard_map.162 = (bf16[256,2048]{1,0:T(8,128)(2,1)}, bf16[512,128]{1,0:T(8,128)(2,1)}) custom-call(s32[4]{0:T(128)S(1)} %pad_add_fusion.place, s32[2,128]{1,0:T(2,128)} %bitcast.31, f32[2,128]{1,0:T(2,128)} %bitcast.32, bf16[128,2048]{1,0:T(8,128)(2,1)} %x_h.1, bf16[128,2048]{1,0:T(8,128)(2,1)} %og_h.3), custom_call_target="tpu_custom_call" | custom-call | tf_op jit(solution)/shard_map/pallas_call | solution.py:71
  3.7 41.2 %all_to_all.20 = bf16[32,8,2048]{2,1,0:T(8,128)(2,1)S(1)} all-to-all(bf16[32,8,2048]{2,1,0:T(8,128)(2,1)} %bitcast.30), channel_id=1, replica_groups=mesh['z'=8,'x'=4,'yh'=4,'yl'=2,'c'=2] {'z','x'}, dimensions={0} | all-to-all | bytes 2097152 | tf_op jit(solution)/shard_map/all_to_all | solution.py:382
  44.9 1.9 %collective-permute-start = (bf16[256,2048]{1,0:T(8,128)(2,1)S(1)}, bf16[256,2048]{1,0:T(8,128)(2,1)S(1)}, u32[]{:S(2)}, u32[]{:S(2)}) collective-permute-start(bf16[256,2048]{1,0:T(8,128)(2,1)S(1)} %bitcast.19), channel_id=1, source_target_pairs={{0,1},{1,0},{2,3},{3,2},{4,5},{5,4},{6,7},{7,6},{8,9},{9,8},{10,11... | collective-permute-start | bytes 3145736 | tf_op jit(solution)/shard_map/ppermute | solution.py:396
  46.9 0.0 copy-done
  46.9 0.0 copy-done.1
  46.9 0.0 copy-done.2
  46.9 0.2 shard_map.164
  47.1 3.5 %collective-permute-start.1 = (bf16[192,2048]{1,0:T(8,128)(2,1)S(1)}, bf16[192,2048]{1,0:T(8,128)(2,1)S(1)}, u32[]{:S(2)}, u32[]{:S(2)}) collective-permute-start(bf16[192,2048]{1,0:T(8,128)(2,1)S(1)} %get-tuple-element.38), channel_id=1, source_target_pairs={{0,2},{2,4},{4,6},{6,8},{8,10},{10,12},{12,14},{14,0},{1,3},{3,5},... | collective-permute-start | bytes 2359304 | tf_op jit(solution)/shard_map/ppermute | solution.py:394
  50.5 2.4 %collective-permute-start.2 = (bf16[192,2048]{1,0:T(8,128)(2,1)S(1)}, bf16[192,2048]{1,0:T(8,128)(2,1)S(1)}, u32[]{:S(2)}, u32[]{:S(2)}) collective-permute-start(bf16[192,2048]{1,0:T(8,128)(2,1)S(1)} %get-tuple-element.39), channel_id=1, source_target_pairs={{0,14},{2,0},{4,2},{6,4},{8,6},{10,8},{12,10},{14,12},{1,15},{3,1}... | collective-permute-start | bytes 2359304 | tf_op jit(solution)/shard_map/ppermute | solution.py:395
  52.9 1.9 %shard_map.163.w = bf16[3,128,2048]{2,1,0:T(8,128)(2,1)S(1)} custom-call(s32[4]{0:T(128)S(1)} %pad_add_fusion.place, bf16[128,2048]{1,0:T(8,128)(2,1)} %bitcast.22, bf16[128,2048]{1,0:T(8,128)(2,1)} %bitcast.24, bf16[128,2048]{1,0:T(8,128)(2,1)} %bitcast.26), custom_call_target="tpu_custom_call" | custom-call | tf_op jit(solution)/shard_map/pallas_call | solution.py:71
  54.9 14.0 %collective-permute-done.1.wa = bf16[192,2048]{1,0:T(8,128)(2,1)S(1)} collective-permute-done((bf16[192,2048]{1,0:T(8,128)(2,1)S(1)}, bf16[192,2048]{1,0:T(8,128)(2,1)S(1)}, u32[]{:S(2)}, u32[]{:S(2)}) %collective-permute-start.1) | collective-permute-done | bytes 786464 | tf_op jit(solution)/shard_map/ppermute | solution.py:394
  68.9 3.2 %collective-permute-done.2.wb = bf16[192,2048]{1,0:T(8,128)(2,1)S(1)} collective-permute-done((bf16[192,2048]{1,0:T(8,128)(2,1)S(1)}, bf16[192,2048]{1,0:T(8,128)(2,1)S(1)}, u32[]{:S(2)}, u32[]{:S(2)}) %collective-permute-start.2) | collective-permute-done | bytes 786464 | tf_op jit(solution)/shard_map/ppermute | solution.py:395
  72.1 2.3 %shard_map.165 = (f32[3,256,256]{2,1,0:T(8,128)S(1)}, bf16[3,256,1024]{2,1,0:T(8,128)(2,1)S(1)}, bf16[3,256,1024]{2,1,0:T(8,128)(2,1)S(1)}) custom-call(s32[4]{0:T(128)S(1)} %pad_add_fusion.place, bf16[256,2048]{1,0:T(8,128)(2,1)S(1)} %bitcast.20, bf16[3,128,2048]{2,1,0:T(8,128)(2,1)S(1)} %shard_map.163.w, bf16[192,2048]{1,0:T(8,128)(2,1)S(1)} %collective-permute-done.1.wa, ...), custom_call_target="tpu_custom_call" | custom-call | tf_op jit(solution)/shard_map/pallas_call | solution.py:71
  74.5 0.0 collective-permute-done.par
  74.5 2.2 %shard_map.166 = (bf16[8,256,128]{2,1,0:T(8,128)(2,1)S(1)}, bf16[256,512]{1,0:T(8,128)(2,1)S(1)}, bf16[256,768]{1,0:T(8,128)(2,1)}) custom-call(s32[4]{0:T(128)S(1)} %pad_add_fusion.place, bf16[256,2048]{1,0:T(8,128)(2,1)S(1)} %collective-permute-done.par, f32[3,256,256]{2,1,0:T(8,128)S(1)} %get-tuple-element.40.part, ...), custom_call_target="tpu_custom_call" | custom-call | tf_op jit(solution)/shard_map/pallas_call | solution.py:71
  76.7 1.9 %collective-permute-start.5 = (bf16[8,256,128]{2,1,0:T(8,128)(2,1)S(1)}, bf16[8,256,128]{2,1,0:T(8,128)(2,1)S(1)}, u32[]{:S(2)}, u32[]{:S(2)}) collective-permute-start(bf16[8,256,128]{2,1,0:T(8,128)(2,1)S(1)} %get-tuple-element.53), channel_id=1, source_target_pairs={{0,1},{1,0},{2,3},{3,2},{4,5},{5,4},{6,7},{7,6},{8,9},{9,8},{10,11... | collective-permute-start | bytes 1572872 | tf_op jit(solution)/shard_map/ppermute | solution.py:430
  78.6 1.0 shard_map.170
  79.6 0.0 copy-start.4
  79.6 0.9 collective-permute-done.5
  80.5 0.9 add_convert_fusion
  81.4 7.8 %all-to-all-start.1 = ((bf16[8,256,128]{2,1,0:T(8,128)(2,1)}), bf16[8,256,128]{2,1,0:T(8,128)(2,1)S(1)}, u32[]{:S(2)}, u32[]{:S(2)}) async-start(bf16[8,256,128]{2,1,0:T(8,128)(2,1)} %add_convert_fusion), calls=%async_computation.1 | async-start | bytes 1048576 | tf_op jit(solution)/shard_map/all_to_all | solution.py:453
  89.2 0.0 copy-done.4
  89.2 0.0 copy-start.3
  89.2 0.0 copy-start.5
  89.2 0.0 copy-start.6
  89.2 3.4 %shard_map.167 = (f32[384,2048]{1,0:T(8,128)}, bf16[192,2048]{1,0:T(8,128)(2,1)}, bf16[192,2048]{1,0:T(8,128)(2,1)S(1)}) custom-call(s32[4]{0:T(128)S(1)} %pad_add_fusion.place, bf16[256,2048]{1,0:T(8,128)(2,1)S(1)} %bitcast.21, bf16[256,2048]{1,0:T(8,128)(2,1)S(1)} %collective-permute-done.par, bf16[256,768]{1,0:T(8,128)(2,1)S(1)} %copy-done.4), custom_call_target="tpu_custom_call" | custom-call | tf_op jit(solution)/shard_map/pallas_call | solution.py:71
  92.6 0.0 copy-start.10
  92.6 0.9 copy-done.10
  93.5 1.9 %collective-permute-start.3 = (bf16[192,2048]{1,0:T(8,128)(2,1)}, bf16[192,2048]{1,0:T(8,128)(2,1)S(1)}, u32[]{:S(2)}, u32[]{:S(2)}) collective-permute-start(bf16[192,2048]{1,0:T(8,128)(2,1)} %get-tuple-element.44), channel_id=1, source_target_pairs={{0,14},{2,0},{4,2},{6,4},{8,6},{10,8},{12,10},{14,12},{1,15},{3,1}... | collective-permute-start | bytes 2359304 | tf_op jit(solution)/shard_map/ppermute | solution.py:449
  95.4 11.1 %all-to-all-done.1.parts = bf16[8,256,128]{2,1,0:T(8,128)(2,1)S(1)} async-done(((bf16[8,256,128]{2,1,0:T(8,128)(2,1)}), bf16[8,256,128]{2,1,0:T(8,128)(2,1)S(1)}, u32[]{:S(2)}, u32[]{:S(2)}) %all-to-all-start.1) | async-done | bytes 524320 | tf_op jit(solution)/shard_map/all_to_all | solution.py:453
  106.5 1.3 shard_map.171
  107.8 5.6 %all-to-all-start.2 = ((bf16[32,16,128]{2,1,0:T(8,128)(2,1)}), bf16[32,16,128]{2,1,0:T(8,128)(2,1)S(1)}, u32[]{:S(2)}, u32[]{:S(2)}) async-start(bf16[32,16,128]{2,1,0:T(8,128)(2,1)} %shard_map.171), calls=%async_computation.2 | async-start | bytes 262144 | tf_op jit(solution)/shard_map/all_to_all | solution.py:455
  113.4 1.9 %collective-permute-start.4 = (bf16[192,2048]{1,0:T(8,128)(2,1)}, bf16[192,2048]{1,0:T(8,128)(2,1)S(1)}, u32[]{:S(2)}, u32[]{:S(2)}) collective-permute-start(bf16[192,2048]{1,0:T(8,128)(2,1)} %copy-done.10), channel_id=1, source_target_pairs={{0,2},{2,4},{4,6},{6,8},{8,10},{10,12},{12,14},{14,0},{1,3},{3,5},... | collective-permute-start | bytes 2359304 | tf_op jit(solution)/shard_map/ppermute | solution.py:450
  115.3 0.0 copy-done.3
  115.3 3.7 %collective-permute-start.6 = (f32[1,128]{1,0:T(1,128)S(1)}, f32[1,128]{1,0:T(1,128)S(1)}, u32[]{:S(2)}, u32[]{:S(2)}) collective-permute-start(f32[1,128]{1,0:T(1,128)S(1)} %slice.39), channel_id=1, source_target_pairs={{0,16},{16,32},{32,48},{48,64},{64,80},{80,96},{96,112},{112,128},... | collective-permute-start | bytes 1544 | tf_op jit(solution)/shard_map/ppermute | solution.py:400
  119.0 0.0 copy-done.5
  119.0 0.0 copy-done.6
  119.0 0.6 shard_map.168
  119.6 0.0 copy-start.7
  119.6 0.6 copy-done.7
  120.2 0.0 copy-start.8
  120.3 0.6 copy-done.8
  120.9 0.6 copy-done.9
  121.5 1.7 shard_map.169
  123.2 0.7 all-to-all-done.2
  123.9 0.8 shard_map.172
  124.6 22.5 %all-gather = bf16[2048,128]{1,0:T(8,128)(2,1)S(1)} all-gather(bf16[128,128]{1,0:T(8,128)(2,1)S(1)} %shard_map.172), channel_id=2, replica_groups=mesh['z'=8,'x'=4,'yh'=4,'yl'=2,'c'=2] {'yh','yl','c'}, dimensions={0}, use_global_device_ids=true | all-gather | bytes 557056 | tf_op jit(solution)/shard_map/all_gather | solution.py:461
  147.1 1.8 %shard_map.173 = (bf16[32,72,128]{2,1,0:T(8,128)(2,1)}, f32[128,128]{1,0:T(8,128)S(1)}) custom-call(s32[4]{0:T(128)S(1)} %pad_add_fusion.place, bf16[16,128,128]{2,1,0:T(8,128)(2,1)S(1)} %bitcast.28, bf16[128,128]{1,0:T(8,128)(2,1)S(1)} %get-tuple-element.55.gated, bf16[2048,128]{1,0:T(8,128)(2,1)S(1)} %get-tuple-element.56.w, ...), custom_call_target="tpu_custom_call" | custom-call | tf_op jit(solution)/shard_map/pallas_call | solution.py:71
  149.0 9.5 %all-to-all-start.3 = ((bf16[32,72,128]{2,1,0:T(8,128)(2,1)}), bf16[32,72,128]{2,1,0:T(8,128)(2,1)S(1)}, u32[]{:S(2)}, u32[]{:S(2)}) async-start(bf16[32,72,128]{2,1,0:T(8,128)(2,1)} %get-tuple-element.59), calls=%async_computation.3 | async-start | bytes 1179648 | tf_op jit(solution)/shard_map/all_to_all | solution.py:478
  158.5 0.0 copy-start.11
  158.5 0.0 collective-permute-done.3
  158.5 0.1 fusion.3
  158.6 0.0 collective-permute-done.4
  158.6 0.1 fusion.4
  158.7 1.7 copy-done.11
  160.4 1.4 fusion.2
  161.8 1.2 shard_map.174
  162.9 0.0 collective-permute-done.6.before
  162.9 15.1 %all-to-all-done.3.got = bf16[32,72,128]{2,1,0:T(8,128)(2,1)S(1)} async-done(((bf16[32,72,128]{2,1,0:T(8,128)(2,1)}), bf16[32,72,128]{2,1,0:T(8,128)(2,1)S(1)}, u32[]{:S(2)}, u32[]{:S(2)}) %all-to-all-start.3) | async-done | bytes 589856 | tf_op jit(solution)/shard_map/all_to_all | solution.py:478
  178.0 1.3 shard_map.175
  (2 shorter events, 0.0 us)
Async XLA Ops:
  0.7 46.1 %copy-start = (bf16[1,128,2048]{2,1,0:T(8,128)(2,1)S(1)}, bf16[1,128,2048]{2,1,0:T(8,128)(2,1)}, u32[]{:S(2)}) copy-start(bf16[1,128,2048]{2,1,0:T(8,128)(2,1)} %param.19) | copy-start | bytes 1572868
  0.7 46.1 %copy-start.1 = (bf16[1,128,2048]{2,1,0:T(8,128)(2,1)S(1)}, bf16[1,128,2048]{2,1,0:T(8,128)(2,1)}, u32[]{:S(2)}) copy-start(bf16[1,128,2048]{2,1,0:T(8,128)(2,1)} %param.20) | copy-start | bytes 1572868
  0.7 46.2 %copy-start.2 = (bf16[1,128,2048]{2,1,0:T(8,128)(2,1)S(1)}, bf16[1,128,2048]{2,1,0:T(8,128)(2,1)}, u32[]{:S(2)}) copy-start(bf16[1,128,2048]{2,1,0:T(8,128)(2,1)} %param.21) | copy-start | bytes 1572868
  44.9 29.5 %collective-permute-start = (bf16[256,2048]{1,0:T(8,128)(2,1)S(1)}, bf16[256,2048]{1,0:T(8,128)(2,1)S(1)}, u32[]{:S(2)}, u32[]{:S(2)}) collective-permute-start(bf16[256,2048]{1,0:T(8,128)(2,1)S(1)} %bitcast.19), channel_id=1, source_target_pairs={{0,1},{1,0},{2,3},{3,2},{4,5},{5,4},{6,7},{7,6},{8,9},{9,8},{10,11... | collective-permute-start | bytes 3145736 | tf_op jit(solution)/shard_map/ppermute | solution.py:396
  47.1 21.8 %collective-permute-start.1 = (bf16[192,2048]{1,0:T(8,128)(2,1)S(1)}, bf16[192,2048]{1,0:T(8,128)(2,1)S(1)}, u32[]{:S(2)}, u32[]{:S(2)}) collective-permute-start(bf16[192,2048]{1,0:T(8,128)(2,1)S(1)} %get-tuple-element.38), channel_id=1, source_target_pairs={{0,2},{2,4},{4,6},{6,8},{8,10},{10,12},{12,14},{14,0},{1,3},{3,5},... | collective-permute-start | bytes 2359304 | tf_op jit(solution)/shard_map/ppermute | solution.py:394
  50.5 21.6 %collective-permute-start.2 = (bf16[192,2048]{1,0:T(8,128)(2,1)S(1)}, bf16[192,2048]{1,0:T(8,128)(2,1)S(1)}, u32[]{:S(2)}, u32[]{:S(2)}) collective-permute-start(bf16[192,2048]{1,0:T(8,128)(2,1)S(1)} %get-tuple-element.39), channel_id=1, source_target_pairs={{0,14},{2,0},{4,2},{6,4},{8,6},{10,8},{12,10},{14,12},{1,15},{3,1}... | collective-permute-start | bytes 2359304 | tf_op jit(solution)/shard_map/ppermute | solution.py:395
  76.7 3.8 %collective-permute-start.5 = (bf16[8,256,128]{2,1,0:T(8,128)(2,1)S(1)}, bf16[8,256,128]{2,1,0:T(8,128)(2,1)S(1)}, u32[]{:S(2)}, u32[]{:S(2)}) collective-permute-start(bf16[8,256,128]{2,1,0:T(8,128)(2,1)S(1)} %get-tuple-element.53), channel_id=1, source_target_pairs={{0,1},{1,0},{2,3},{3,2},{4,5},{5,4},{6,7},{7,6},{8,9},{9,8},{10,11... | collective-permute-start | bytes 1572872 | tf_op jit(solution)/shard_map/ppermute | solution.py:430
  79.6 9.6 %copy-start.4 = (bf16[256,768]{1,0:T(8,128)(2,1)S(1)}, bf16[256,768]{1,0:T(8,128)(2,1)}, u32[]{:S(2)}) copy-start(bf16[256,768]{1,0:T(8,128)(2,1)} %get-tuple-element.42.mix) | copy-start | bytes 1179652
  81.4 25.1 %all-to-all-start.1 = ((bf16[8,256,128]{2,1,0:T(8,128)(2,1)}), bf16[8,256,128]{2,1,0:T(8,128)(2,1)S(1)}, u32[]{:S(2)}, u32[]{:S(2)}) async-start(bf16[8,256,128]{2,1,0:T(8,128)(2,1)} %add_convert_fusion), calls=%async_computation.1 | async-start | bytes 1048576 | tf_op jit(solution)/shard_map/all_to_all | solution.py:453
  89.2 26.1 %copy-start.3 = (f32[128,128]{1,0:T(8,128)S(1)}, f32[128,128]{1,0:T(8,128)}, u32[]{:S(2)}) copy-start(f32[128,128]{1,0:T(8,128)} %states.5) | copy-start | bytes 196612
  89.2 29.8 %copy-start.5 = (f32[128,128]{1,0:T(8,128)S(1)}, f32[128,128]{1,0:T(8,128)}, u32[]{:S(2)}) copy-start(f32[128,128]{1,0:T(8,128)} %decay.3) | copy-start | bytes 196612
  89.2 29.8 %copy-start.6 = (bf16[128,128]{1,0:T(8,128)(2,1)S(1)}, bf16[128,128]{1,0:T(8,128)(2,1)}, u32[]{:S(2)}) copy-start(bf16[128,128]{1,0:T(8,128)(2,1)} %gate.3) | copy-start | bytes 98308
  92.6 0.9 copy-start.10
  93.5 65.0 %collective-permute-start.3 = (bf16[192,2048]{1,0:T(8,128)(2,1)}, bf16[192,2048]{1,0:T(8,128)(2,1)S(1)}, u32[]{:S(2)}, u32[]{:S(2)}) collective-permute-start(bf16[192,2048]{1,0:T(8,128)(2,1)} %get-tuple-element.44), channel_id=1, source_target_pairs={{0,14},{2,0},{4,2},{6,4},{8,6},{10,8},{12,10},{14,12},{1,15},{3,1}... | collective-permute-start | bytes 2359304 | tf_op jit(solution)/shard_map/ppermute | solution.py:449
  107.8 16.1 %all-to-all-start.2 = ((bf16[32,16,128]{2,1,0:T(8,128)(2,1)}), bf16[32,16,128]{2,1,0:T(8,128)(2,1)S(1)}, u32[]{:S(2)}, u32[]{:S(2)}) async-start(bf16[32,16,128]{2,1,0:T(8,128)(2,1)} %shard_map.171), calls=%async_computation.2 | async-start | bytes 262144 | tf_op jit(solution)/shard_map/all_to_all | solution.py:455
  113.4 45.2 %collective-permute-start.4 = (bf16[192,2048]{1,0:T(8,128)(2,1)}, bf16[192,2048]{1,0:T(8,128)(2,1)S(1)}, u32[]{:S(2)}, u32[]{:S(2)}) collective-permute-start(bf16[192,2048]{1,0:T(8,128)(2,1)} %copy-done.10), channel_id=1, source_target_pairs={{0,2},{2,4},{4,6},{6,8},{8,10},{10,12},{12,14},{14,0},{1,3},{3,5},... | collective-permute-start | bytes 2359304 | tf_op jit(solution)/shard_map/ppermute | solution.py:450
  115.3 47.6 %collective-permute-start.6 = (f32[1,128]{1,0:T(1,128)S(1)}, f32[1,128]{1,0:T(1,128)S(1)}, u32[]{:S(2)}, u32[]{:S(2)}) collective-permute-start(f32[1,128]{1,0:T(1,128)S(1)} %slice.39), channel_id=1, source_target_pairs={{0,16},{16,32},{32,48},{48,64},{64,80},{80,96},{96,112},{112,128},... | collective-permute-start | bytes 1544 | tf_op jit(solution)/shard_map/ppermute | solution.py:400
  119.6 0.6 copy-start.7
  120.2 0.6 copy-start.8
  120.9 0.6 copy-start.9
  149.0 29.0 %all-to-all-start.3 = ((bf16[32,72,128]{2,1,0:T(8,128)(2,1)}), bf16[32,72,128]{2,1,0:T(8,128)(2,1)S(1)}, u32[]{:S(2)}, u32[]{:S(2)}) async-start(bf16[32,72,128]{2,1,0:T(8,128)(2,1)} %get-tuple-element.59), calls=%async_computation.3 | async-start | bytes 1179648 | tf_op jit(solution)/shard_map/all_to_all | solution.py:478
  158.5 1.9 %copy-start.11 = (f32[384,2048]{1,0:T(8,128)S(1)}, f32[384,2048]{1,0:T(8,128)}, u32[]{:S(2)}) copy-start(f32[384,2048]{1,0:T(8,128)} %get-tuple-element.43) | copy-start | bytes 9437188

commit v7 on v5

--- a/solution.py
+++ b/solution.py
@@ -238,25 +238,27 @@
         copy.wait()
 
 
-def weight_body(place, own, par, mix, gown_h, ga, gb, gown, sems):
+def weight_body(place, own, par, mix, gown_h, ga_h, gb_h, gown, ga, gb, sems):
     c = place[0]
-    h, q = gown.shape[1] // 3, ga.shape[0] // 3
-    units, cols = h + 2 * q, gown.shape[2]
+    h, q = gown.shape[0] // 3, ga.shape[0] // 3
+    units, cols = h + 2 * q, gown.shape[1] // 2
     stored = []
-    for n, (src, core) in enumerate(((own, c), (par, 1 - c))):
-        where = columns(core, cols)
-        for k in range(3):
+    for k in range(3):
+        mine, near = pl.ds(k * h, h), pl.ds(k * q, q)
+        for src, core in ((own, c), (par, 1 - c)):
+            where = columns(core, cols)
             side = src[:, 0:cols] if k < 2 else src[:, cols:]
             g = tn(mix[:, k * units : (k + 1) * units], side)
-            rows = pl.ds(k * h, h)
-            gown[n, rows, :] = g[0:h]
-            copy = pltpu.make_async_copy(
-                gown.at[n, rows], gown_h.at[rows, where], sems.at[3 * n + k]
-            )
-            copy.start()
-            stored.append(copy)
-            ga[k * q : (k + 1) * q, where] = g[h : h + q].astype(BF16)
-            gb[k * q : (k + 1) * q, where] = g[h + q :].astype(BF16)
+            gown[mine, where] = g[0:h]
+            ga[near, where] = g[h : h + q].astype(BF16)
+            gb[near, where] = g[h + q :].astype(BF16)
+        stored += copies(
+            (
+                (ga.at[near], ga_h.at[near]), (gb.at[near], gb_h.at[near]),
+                (gown.at[mine], gown_h.at[mine]),
+            ),
+            sems.at[pl.ds(3 * k, 3)],
+        )
     for copy in stored:
         copy.wait()
 
@@ -423,9 +425,10 @@
         weight_body,
         [shape((3 * hidden, width), F32), shape((3 * q, width), BF16), shape((3 * q, width), BF16)],
         place, own, par, mix,
-        outs_in=(0,),
+        outs_in=(0, 1, 2),
         scratch=[
-            pltpu.VMEM((2, 3 * hidden, cols), F32), pltpu.SemaphoreType.DMA((6,)),
+            pltpu.VMEM((3 * hidden, width), F32), pltpu.VMEM((3 * q, width), BF16),
+            pltpu.VMEM((3 * q, width), BF16), pltpu.SemaphoreType.DMA((9,)),
         ],
     )
     pick, og, w_p, gated, weight, tails = call(

time: 181 us -> 181 us (level)
  no operation moved by 1% of the time
where the time goes in v7:
time: 181 us; the launch traced here: 180 us
  blocking collectives  63.7 us (35%)
  waiting for transfers between devices  47.3 us (26%)
  starting transfers between devices  40.2 us (22%)
  Pallas kernels  21.1 us (12%)
  local copies, waits for them, and re-layouts  4.35 us (2%)
  other arithmetic  2.38 us (1%)
    all_to_all x1, blocking collectives, local(): own = lax.all_to_all(send.reshape(n_sp, half, width), SP, 0, 0, tiled=True)  41.2 us
    all_gather x1, blocking collectives, local(): mid = lax.all_gather(mid, TP)  22.5 us
    pallas_call x12, Pallas kernels, call(): pl.pallas_call(body, grid_spec=pltpu.PrefetchScalarGridSpec(num_scalar_pr...  21 us
    ppermute x1, waiting for transfers between devices, local(): wa = lax.ppermute(w_lo, Y, ring(1))  16 us
    all_to_all x1, waiting for transfers between devices, local(): got = lax.all_to_all(out, SP, 0, 0, tiled=True)  14.4 us
    all_to_all x1, waiting for transfers between devices, local(): parts = lax.all_to_all(psum, Y, 0, 0, tiled=True)  12.2 us
    all_to_all x1, starting transfers between devices, local(): got = lax.all_to_all(out, SP, 0, 0, tiled=True)  9.51 us
    all_to_all x1, starting transfers between devices, local(): parts = lax.all_to_all(psum, Y, 0, 0, tiled=True)  7.76 us
  transfers between devices with their start and end apart: 10, of which 6 were waited for; matrix products, arithmetic and copies ran while one was open for 2% of the time, Pallas kernels for 8%

profile of v7, /device:TPU:8, one launch (start us, length us, event | category | flops | bytes accessed | tf_op | source)
XLA Modules:
  0.0 180.0 jit_solution(1075284082541912137)
XLA Ops:
  0.6 0.0 copy-start
  0.6 0.0 copy-start.1
  0.7 0.0 copy-start.2
  0.7 0.1 pad_add_fusion.place
  0.8 3.0 %shard_map.162 = (bf16[256,2048]{1,0:T(8,128)(2,1)}, bf16[512,128]{1,0:T(8,128)(2,1)}) custom-call(s32[4]{0:T(128)S(1)} %pad_add_fusion.place, s32[2,128]{1,0:T(2,128)} %bitcast.31, f32[2,128]{1,0:T(2,128)} %bitcast.32, bf16[128,2048]{1,0:T(8,128)(2,1)} %x_h.1, bf16[128,2048]{1,0:T(8,128)(2,1)} %og_h.3), custom_call_target="tpu_custom_call" | custom-call | tf_op jit(solution)/shard_map/pallas_call | solution.py:71
  3.7 41.2 %all_to_all.20 = bf16[32,8,2048]{2,1,0:T(8,128)(2,1)S(1)} all-to-all(bf16[32,8,2048]{2,1,0:T(8,128)(2,1)} %bitcast.30), channel_id=1, replica_groups=mesh['z'=8,'x'=4,'yh'=4,'yl'=2,'c'=2] {'z','x'}, dimensions={0} | all-to-all | bytes 2097152 | tf_op jit(solution)/shard_map/all_to_all | solution.py:378
  45.0 1.9 %collective-permute-start = (bf16[256,2048]{1,0:T(8,128)(2,1)S(1)}, bf16[256,2048]{1,0:T(8,128)(2,1)S(1)}, u32[]{:S(2)}, u32[]{:S(2)}) collective-permute-start(bf16[256,2048]{1,0:T(8,128)(2,1)S(1)} %bitcast.19), channel_id=1, source_target_pairs={{0,1},{1,0},{2,3},{3,2},{4,5},{5,4},{6,7},{7,6},{8,9},{9,8},{10,11... | collective-permute-start | bytes 3145736 | tf_op jit(solution)/shard_map/ppermute | solution.py:392
  46.9 0.0 copy-done
  46.9 0.0 copy-done.1
  46.9 0.0 copy-done.2
  46.9 0.2 shard_map.163
  47.1 3.5 %collective-permute-start.1 = (bf16[192,2048]{1,0:T(8,128)(2,1)S(1)}, bf16[192,2048]{1,0:T(8,128)(2,1)S(1)}, u32[]{:S(2)}, u32[]{:S(2)}) collective-permute-start(bf16[192,2048]{1,0:T(8,128)(2,1)S(1)} %get-tuple-element.38), channel_id=1, source_target_pairs={{0,2},{2,4},{4,6},{6,8},{8,10},{10,12},{12,14},{14,0},{1,3},{3,5},... | collective-permute-start | bytes 2359304 | tf_op jit(solution)/shard_map/ppermute | solution.py:390
  50.6 2.4 %collective-permute-start.2 = (bf16[192,2048]{1,0:T(8,128)(2,1)S(1)}, bf16[192,2048]{1,0:T(8,128)(2,1)S(1)}, u32[]{:S(2)}, u32[]{:S(2)}) collective-permute-start(bf16[192,2048]{1,0:T(8,128)(2,1)S(1)} %get-tuple-element.39), channel_id=1, source_target_pairs={{0,14},{2,0},{4,2},{6,4},{8,6},{10,8},{12,10},{14,12},{1,15},{3,1}... | collective-permute-start | bytes 2359304 | tf_op jit(solution)/shard_map/ppermute | solution.py:391
  52.9 16.0 %collective-permute-done.1.wa = bf16[192,2048]{1,0:T(8,128)(2,1)S(1)} collective-permute-done((bf16[192,2048]{1,0:T(8,128)(2,1)S(1)}, bf16[192,2048]{1,0:T(8,128)(2,1)S(1)}, u32[]{:S(2)}, u32[]{:S(2)}) %collective-permute-start.1) | collective-permute-done | bytes 786464 | tf_op jit(solution)/shard_map/ppermute | solution.py:390
  68.9 3.2 %collective-permute-done.2.wb = bf16[192,2048]{1,0:T(8,128)(2,1)S(1)} collective-permute-done((bf16[192,2048]{1,0:T(8,128)(2,1)S(1)}, bf16[192,2048]{1,0:T(8,128)(2,1)S(1)}, u32[]{:S(2)}, u32[]{:S(2)}) %collective-permute-start.2) | collective-permute-done | bytes 786464 | tf_op jit(solution)/shard_map/ppermute | solution.py:391
  72.1 2.9 %shard_map.164 = (f32[3,256,256]{2,1,0:T(8,128)S(1)}, bf16[3,256,1024]{2,1,0:T(8,128)(2,1)S(1)}, bf16[3,256,1024]{2,1,0:T(8,128)(2,1)S(1)}) custom-call(s32[4]{0:T(128)S(1)} %pad_add_fusion.place, bf16[256,2048]{1,0:T(8,128)(2,1)S(1)} %bitcast.20, bf16[128,2048]{1,0:T(8,128)(2,1)} %bitcast.22, bf16[128,2048]{1,0:T(8,128)(2,1)} %bitcast.24, ...), custom_call_target="tpu_custom_call" | custom-call | tf_op jit(solution)/shard_map/pallas_call | solution.py:71
  75.1 0.0 collective-permute-done.par
  75.1 2.2 %shard_map.165 = (bf16[8,256,128]{2,1,0:T(8,128)(2,1)S(1)}, bf16[256,512]{1,0:T(8,128)(2,1)S(1)}, bf16[256,768]{1,0:T(8,128)(2,1)}) custom-call(s32[4]{0:T(128)S(1)} %pad_add_fusion.place, bf16[256,2048]{1,0:T(8,128)(2,1)S(1)} %collective-permute-done.par, f32[3,256,256]{2,1,0:T(8,128)S(1)} %get-tuple-element.40.part, ...), custom_call_target="tpu_custom_call" | custom-call | tf_op jit(solution)/shard_map/pallas_call | solution.py:71
  77.3 0.0 copy-start.4
  77.3 2.1 %collective-permute-start.5 = (bf16[8,256,128]{2,1,0:T(8,128)(2,1)S(1)}, bf16[8,256,128]{2,1,0:T(8,128)(2,1)S(1)}, u32[]{:S(2)}, u32[]{:S(2)}) collective-permute-start(bf16[8,256,128]{2,1,0:T(8,128)(2,1)S(1)} %get-tuple-element.53), channel_id=1, source_target_pairs={{0,1},{1,0},{2,3},{3,2},{4,5},{5,4},{6,7},{7,6},{8,9},{9,8},{10,11... | collective-permute-start | bytes 1572872 | tf_op jit(solution)/shard_map/ppermute | solution.py:423
  79.4 1.0 shard_map.169
  80.3 0.0 copy-start.3
  80.4 0.0 copy-start.5
  80.4 0.0 copy-start.6
  80.4 0.9 collective-permute-done.5
  81.2 0.9 add_convert_fusion
  82.1 7.8 %all-to-all-start.1 = ((bf16[8,256,128]{2,1,0:T(8,128)(2,1)}), bf16[8,256,128]{2,1,0:T(8,128)(2,1)S(1)}, u32[]{:S(2)}, u32[]{:S(2)}) async-start(bf16[8,256,128]{2,1,0:T(8,128)(2,1)} %add_convert_fusion), calls=%async_computation.1 | async-start | bytes 1048576 | tf_op jit(solution)/shard_map/all_to_all | solution.py:447
  89.9 0.0 copy-done.4
  89.9 3.2 %shard_map.166 = (f32[384,2048]{1,0:T(8,128)}, bf16[192,2048]{1,0:T(8,128)(2,1)}, bf16[192,2048]{1,0:T(8,128)(2,1)}) custom-call(s32[4]{0:T(128)S(1)} %pad_add_fusion.place, bf16[256,2048]{1,0:T(8,128)(2,1)S(1)} %bitcast.21, bf16[256,2048]{1,0:T(8,128)(2,1)S(1)} %collective-permute-done.par, bf16[256,768]{1,0:T(8,128)(2,1)S(1)} %copy-done.4), custom_call_target="tpu_custom_call" | custom-call | tf_op jit(solution)/shard_map/pallas_call | solution.py:71
  93.1 1.9 %collective-permute-start.3 = (bf16[192,2048]{1,0:T(8,128)(2,1)}, bf16[192,2048]{1,0:T(8,128)(2,1)}, u32[]{:S(2)}, u32[]{:S(2)}) collective-permute-start(bf16[192,2048]{1,0:T(8,128)(2,1)} %get-tuple-element.44), channel_id=1, source_target_pairs={{0,14},{2,0},{4,2},{6,4},{8,6},{10,8},{12,10},{14,12},{1,15},{3,1}... | collective-permute-start | bytes 2359304 | tf_op jit(solution)/shard_map/ppermute | solution.py:443
  95.1 12.2 %all-to-all-done.1.parts = bf16[8,256,128]{2,1,0:T(8,128)(2,1)S(1)} async-done(((bf16[8,256,128]{2,1,0:T(8,128)(2,1)}), bf16[8,256,128]{2,1,0:T(8,128)(2,1)S(1)}, u32[]{:S(2)}, u32[]{:S(2)}) %all-to-all-start.1) | async-done | bytes 524320 | tf_op jit(solution)/shard_map/all_to_all | solution.py:447
  107.3 1.3 shard_map.170
  108.5 5.6 %all-to-all-start.2 = ((bf16[32,16,128]{2,1,0:T(8,128)(2,1)}), bf16[32,16,128]{2,1,0:T(8,128)(2,1)S(1)}, u32[]{:S(2)}, u32[]{:S(2)}) async-start(bf16[32,16,128]{2,1,0:T(8,128)(2,1)} %shard_map.170), calls=%async_computation.2 | async-start | bytes 262144 | tf_op jit(solution)/shard_map/all_to_all | solution.py:449
  114.1 1.9 %collective-permute-start.4 = (bf16[192,2048]{1,0:T(8,128)(2,1)}, bf16[192,2048]{1,0:T(8,128)(2,1)}, u32[]{:S(2)}, u32[]{:S(2)}) collective-permute-start(bf16[192,2048]{1,0:T(8,128)(2,1)} %get-tuple-element.45), channel_id=1, source_target_pairs={{0,2},{2,4},{4,6},{6,8},{8,10},{10,12},{12,14},{14,0},{1,3},{3,5},... | collective-permute-start | bytes 2359304 | tf_op jit(solution)/shard_map/ppermute | solution.py:444
  116.0 0.0 copy-done.3
  116.0 3.7 %collective-permute-start.6 = (f32[1,128]{1,0:T(1,128)S(1)}, f32[1,128]{1,0:T(1,128)S(1)}, u32[]{:S(2)}, u32[]{:S(2)}) collective-permute-start(f32[1,128]{1,0:T(1,128)S(1)} %slice.39), channel_id=1, source_target_pairs={{0,16},{16,32},{32,48},{48,64},{64,80},{80,96},{96,112},{112,128},... | collective-permute-start | bytes 1544 | tf_op jit(solution)/shard_map/ppermute | solution.py:396
  119.7 0.0 copy-done.5
  119.7 0.0 copy-done.6
  119.8 0.6 shard_map.167
  120.3 0.0 copy-start.7
  120.4 0.6 copy-done.7
  121.0 0.0 copy-start.8
  121.0 0.6 copy-done.8
  121.6 0.0 copy-start.9
  121.6 0.6 copy-done.9
  122.2 1.7 shard_map.168
  123.9 0.7 all-to-all-done.2
  124.6 0.8 shard_map.171
  125.4 22.5 %all-gather = bf16[2048,128]{1,0:T(8,128)(2,1)S(1)} all-gather(bf16[128,128]{1,0:T(8,128)(2,1)S(1)} %shard_map.171), channel_id=2, replica_groups=mesh['z'=8,'x'=4,'yh'=4,'yl'=2,'c'=2] {'yh','yl','c'}, dimensions={0}, use_global_device_ids=true | all-gather | bytes 557056 | tf_op jit(solution)/shard_map/all_gather | solution.py:455
  147.9 1.8 %shard_map.172 = (bf16[32,72,128]{2,1,0:T(8,128)(2,1)}, f32[128,128]{1,0:T(8,128)S(1)}) custom-call(s32[4]{0:T(128)S(1)} %pad_add_fusion.place, bf16[16,128,128]{2,1,0:T(8,128)(2,1)S(1)} %bitcast.28, bf16[128,128]{1,0:T(8,128)(2,1)S(1)} %get-tuple-element.55.gated, bf16[2048,128]{1,0:T(8,128)(2,1)S(1)} %get-tuple-element.56.w, ...), custom_call_target="tpu_custom_call" | custom-call | tf_op jit(solution)/shard_map/pallas_call | solution.py:71
  149.7 9.5 %all-to-all-start.3 = ((bf16[32,72,128]{2,1,0:T(8,128)(2,1)}), bf16[32,72,128]{2,1,0:T(8,128)(2,1)S(1)}, u32[]{:S(2)}, u32[]{:S(2)}) async-start(bf16[32,72,128]{2,1,0:T(8,128)(2,1)} %get-tuple-element.59), calls=%async_computation.3 | async-start | bytes 1179648 | tf_op jit(solution)/shard_map/all_to_all | solution.py:472
  159.2 0.0 copy-start.10
  159.2 0.0 collective-permute-done.3
  159.2 1.3 fusion.3
  160.6 0.0 collective-permute-done.4
  160.6 1.2 fusion.4
  161.7 0.0 copy-done.10
  161.7 1.4 fusion.2
  163.1 1.2 shard_map.173
  164.3 0.0 collective-permute-done.6.before
  164.3 14.4 %all-to-all-done.3.got = bf16[32,72,128]{2,1,0:T(8,128)(2,1)S(1)} async-done(((bf16[32,72,128]{2,1,0:T(8,128)(2,1)}), bf16[32,72,128]{2,1,0:T(8,128)(2,1)S(1)}, u32[]{:S(2)}, u32[]{:S(2)}) %all-to-all-start.3) | async-done | bytes 589856 | tf_op jit(solution)/shard_map/all_to_all | solution.py:472
  178.7 1.3 shard_map.174
  (1 shorter events, 0.0 us)
Async XLA Ops:
  0.6 46.2 %copy-start = (bf16[1,128,2048]{2,1,0:T(8,128)(2,1)S(1)}, bf16[1,128,2048]{2,1,0:T(8,128)(2,1)}, u32[]{:S(2)}) copy-start(bf16[1,128,2048]{2,1,0:T(8,128)(2,1)} %param.19) | copy-start | bytes 1572868
  0.6 46.2 %copy-start.1 = (bf16[1,128,2048]{2,1,0:T(8,128)(2,1)S(1)}, bf16[1,128,2048]{2,1,0:T(8,128)(2,1)}, u32[]{:S(2)}) copy-start(bf16[1,128,2048]{2,1,0:T(8,128)(2,1)} %param.20) | copy-start | bytes 1572868
  0.7 46.2 %copy-start.2 = (bf16[1,128,2048]{2,1,0:T(8,128)(2,1)S(1)}, bf16[1,128,2048]{2,1,0:T(8,128)(2,1)}, u32[]{:S(2)}) copy-start(bf16[1,128,2048]{2,1,0:T(8,128)(2,1)} %param.21) | copy-start | bytes 1572868
  45.0 30.1 %collective-permute-start = (bf16[256,2048]{1,0:T(8,128)(2,1)S(1)}, bf16[256,2048]{1,0:T(8,128)(2,1)S(1)}, u32[]{:S(2)}, u32[]{:S(2)}) collective-permute-start(bf16[256,2048]{1,0:T(8,128)(2,1)S(1)} %bitcast.19), channel_id=1, source_target_pairs={{0,1},{1,0},{2,3},{3,2},{4,5},{5,4},{6,7},{7,6},{8,9},{9,8},{10,11... | collective-permute-start | bytes 3145736 | tf_op jit(solution)/shard_map/ppermute | solution.py:392
  47.1 21.8 %collective-permute-start.1 = (bf16[192,2048]{1,0:T(8,128)(2,1)S(1)}, bf16[192,2048]{1,0:T(8,128)(2,1)S(1)}, u32[]{:S(2)}, u32[]{:S(2)}) collective-permute-start(bf16[192,2048]{1,0:T(8,128)(2,1)S(1)} %get-tuple-element.38), channel_id=1, source_target_pairs={{0,2},{2,4},{4,6},{6,8},{8,10},{10,12},{12,14},{14,0},{1,3},{3,5},... | collective-permute-start | bytes 2359304 | tf_op jit(solution)/shard_map/ppermute | solution.py:390
  50.6 21.6 %collective-permute-start.2 = (bf16[192,2048]{1,0:T(8,128)(2,1)S(1)}, bf16[192,2048]{1,0:T(8,128)(2,1)S(1)}, u32[]{:S(2)}, u32[]{:S(2)}) collective-permute-start(bf16[192,2048]{1,0:T(8,128)(2,1)S(1)} %get-tuple-element.39), channel_id=1, source_target_pairs={{0,14},{2,0},{4,2},{6,4},{8,6},{10,8},{12,10},{14,12},{1,15},{3,1}... | collective-permute-start | bytes 2359304 | tf_op jit(solution)/shard_map/ppermute | solution.py:391
  77.3 12.6 %copy-start.4 = (bf16[256,768]{1,0:T(8,128)(2,1)S(1)}, bf16[256,768]{1,0:T(8,128)(2,1)}, u32[]{:S(2)}) copy-start(bf16[256,768]{1,0:T(8,128)(2,1)} %get-tuple-element.42.mix) | copy-start | bytes 1179652
  77.3 3.9 %collective-permute-start.5 = (bf16[8,256,128]{2,1,0:T(8,128)(2,1)S(1)}, bf16[8,256,128]{2,1,0:T(8,128)(2,1)S(1)}, u32[]{:S(2)}, u32[]{:S(2)}) collective-permute-start(bf16[8,256,128]{2,1,0:T(8,128)(2,1)S(1)} %get-tuple-element.53), channel_id=1, source_target_pairs={{0,1},{1,0},{2,3},{3,2},{4,5},{5,4},{6,7},{7,6},{8,9},{9,8},{10,11... | collective-permute-start | bytes 1572872 | tf_op jit(solution)/shard_map/ppermute | solution.py:423
  80.3 35.7 %copy-start.3 = (f32[128,128]{1,0:T(8,128)S(1)}, f32[128,128]{1,0:T(8,128)}, u32[]{:S(2)}) copy-start(f32[128,128]{1,0:T(8,128)} %states.5) | copy-start | bytes 196612
  80.4 39.4 %copy-start.5 = (f32[128,128]{1,0:T(8,128)S(1)}, f32[128,128]{1,0:T(8,128)}, u32[]{:S(2)}) copy-start(f32[128,128]{1,0:T(8,128)} %decay.3) | copy-start | bytes 196612
  80.4 39.4 %copy-start.6 = (bf16[128,128]{1,0:T(8,128)(2,1)S(1)}, bf16[128,128]{1,0:T(8,128)(2,1)}, u32[]{:S(2)}) copy-start(bf16[128,128]{1,0:T(8,128)(2,1)} %gate.3) | copy-start | bytes 98308
  82.1 25.1 %all-to-all-start.1 = ((bf16[8,256,128]{2,1,0:T(8,128)(2,1)}), bf16[8,256,128]{2,1,0:T(8,128)(2,1)S(1)}, u32[]{:S(2)}, u32[]{:S(2)}) async-start(bf16[8,256,128]{2,1,0:T(8,128)(2,1)} %add_convert_fusion), calls=%async_computation.1 | async-start | bytes 1048576 | tf_op jit(solution)/shard_map/all_to_all | solution.py:447
  93.1 66.1 %collective-permute-start.3 = (bf16[192,2048]{1,0:T(8,128)(2,1)}, bf16[192,2048]{1,0:T(8,128)(2,1)}, u32[]{:S(2)}, u32[]{:S(2)}) collective-permute-start(bf16[192,2048]{1,0:T(8,128)(2,1)} %get-tuple-element.44), channel_id=1, source_target_pairs={{0,14},{2,0},{4,2},{6,4},{8,6},{10,8},{12,10},{14,12},{1,15},{3,1}... | collective-permute-start | bytes 2359304 | tf_op jit(solution)/shard_map/ppermute | solution.py:443
  108.5 16.1 %all-to-all-start.2 = ((bf16[32,16,128]{2,1,0:T(8,128)(2,1)}), bf16[32,16,128]{2,1,0:T(8,128)(2,1)S(1)}, u32[]{:S(2)}, u32[]{:S(2)}) async-start(bf16[32,16,128]{2,1,0:T(8,128)(2,1)} %shard_map.170), calls=%async_computation.2 | async-start | bytes 262144 | tf_op jit(solution)/shard_map/all_to_all | solution.py:449
  114.1 46.5 %collective-permute-start.4 = (bf16[192,2048]{1,0:T(8,128)(2,1)}, bf16[192,2048]{1,0:T(8,128)(2,1)}, u32[]{:S(2)}, u32[]{:S(2)}) collective-permute-start(bf16[192,2048]{1,0:T(8,128)(2,1)} %get-tuple-element.45), channel_id=1, source_target_pairs={{0,2},{2,4},{4,6},{6,8},{8,10},{10,12},{12,14},{14,0},{1,3},{3,5},... | collective-permute-start | bytes 2359304 | tf_op jit(solution)/shard_map/ppermute | solution.py:444
  116.0 48.3 %collective-permute-start.6 = (f32[1,128]{1,0:T(1,128)S(1)}, f32[1,128]{1,0:T(1,128)S(1)}, u32[]{:S(2)}, u32[]{:S(2)}) collective-permute-start(f32[1,128]{1,0:T(1,128)S(1)} %slice.39), channel_id=1, source_target_pairs={{0,16},{16,32},{32,48},{48,64},{64,80},{80,96},{96,112},{112,128},... | collective-permute-start | bytes 1544 | tf_op jit(solution)/shard_map/ppermute | solution.py:396
  120.3 0.6 copy-start.7
  121.0 0.6 copy-start.8
  121.6 0.6 copy-start.9
  149.7 29.0 %all-to-all-start.3 = ((bf16[32,72,128]{2,1,0:T(8,128)(2,1)}), bf16[32,72,128]{2,1,0:T(8,128)(2,1)S(1)}, u32[]{:S(2)}, u32[]{:S(2)}) async-start(bf16[32,72,128]{2,1,0:T(8,128)(2,1)} %get-tuple-element.59), calls=%async_computation.3 | async-start | bytes 1179648 | tf_op jit(solution)/shard_map/all_to_all | solution.py:472
  159.2 2.5 %copy-start.10 = (f32[384,2048]{1,0:T(8,128)S(1)}, f32[384,2048]{1,0:T(8,128)}, u32[]{:S(2)}) copy-start(f32[384,2048]{1,0:T(8,128)} %get-tuple-element.43) | copy-start | bytes 9437188

commit v8 on v7

--- a/solution.py
+++ b/solution.py
@@ -85,28 +85,37 @@
     return result if isinstance(out_shape, (list, tuple)) else result[0]
 
 
-def dispatch_body(experts, cap, place, ids_h, wts_h, x_h, og_h, send_h, pick_h, ids, wts, x, og, send, pick, sems):
+def positions(ids, experts):
+    n = ids.shape[1]
+    before = lax.broadcasted_iota(jnp.int32, (n, n), 0) < lax.broadcasted_iota(
+        jnp.int32, (n, n), 1
+    )
+    before = jnp.where(before, 1.0, 0.0).astype(BF16)
+    row = lax.broadcasted_iota(jnp.int32, (experts, n), 0)
+    m0, m1 = ids[0:1, :] == row, ids[1:2, :] == row
+    named = jnp.where(m0 | m1, 1.0, 0.0).astype(F32)
+    position = jnp.where(named > 0.0, nn(named.astype(BF16), before), -1.0)
+    return m0, m1, position
+
+
+def one_hot(position, first, count):
+    experts, n = position.shape
+    slot = lax.broadcasted_iota(jnp.int32, (experts, count, n), 1).astype(F32)
+    return jnp.where(position[:, None, :] == slot + first, 1.0, 0.0).astype(F32)
+
+
+def dispatch_body(experts, cap, place, ids_h, wts_h, x_h, og_h, send_h, ids, wts, x, og, send, sems):
     n, cols = x.shape
     half = cap // 2
     mine = pl.ds(pl.multiple_of(place[0] * cols, cols), cols)
     got = copies(
         ((ids_h, ids), (wts_h, wts), (x_h.at[:, mine], x), (og_h.at[:, mine], og)), sems
     )
-    before = lax.broadcasted_iota(jnp.int32, (n, n), 0) < lax.broadcasted_iota(
-        jnp.int32, (n, n), 1
-    )
-    before = jnp.where(before, 1.0, 0.0).astype(BF16)
-    row = lax.broadcasted_iota(jnp.int32, (experts, n), 0)
     got[0].wait()
     got[1].wait()
-    m0, m1 = ids[0:1, :] == row, ids[1:2, :] == row
-    named = jnp.where(m0 | m1, 1.0, 0.0).astype(F32)
+    m0, m1, position = positions(ids[...], experts)
     wt = jnp.where(m0, wts[0:1, :], 0.0) + jnp.where(m1, wts[1:2, :], 0.0)
-    position = nn(named.astype(BF16), before)
-    position = jnp.where(named > 0.0, position, -1.0)
-    slot = lax.broadcasted_iota(jnp.int32, (experts, half, n), 1).astype(F32)
-    at = lambda first: jnp.where(position[:, None, :] == slot + first, 1.0, 0.0).astype(F32)
-    hot = at((place[1] * half).astype(F32))
+    hot = one_hot(position, (place[1] * half).astype(F32), half)
     scale = jnp.sum(hot * wt[:, None, :], axis=2, keepdims=True).reshape(experts * half, 1)
     hot = hot.reshape(experts * half, n).astype(BF16)
     got[2].wait()
@@ -123,14 +132,7 @@
             )
             copy.start()
             out.append(copy)
-    pick[...] = (
-        jnp.concatenate([at(0.0), at(float(half))], axis=1)
-        .reshape(experts * cap, n)
-        .astype(BF16)
-    )
-    kept = pltpu.make_async_copy(pick, pick_h, sems.at[8])
-    kept.start()
-    for copy in (*out, kept):
+    for copy in out:
         copy.wait()
 
 
@@ -226,15 +228,22 @@
     partials(pkeep, pair[:, 0:units], pair[:, units:], w_s)
 
 
-def fetch_body(place, pick_h, og_h, w_h, gated_h, weight_h, tail_h, pick, og, w, gated, weight, tail, sems):
+def fetch_body(
+    experts, place, ids_h, og_h, w_h, gated_h, weight_h, tail_h,
+    pick, og, w, gated, weight, tail, ids, sems,
+):
     there = og_h.at[:, columns(place[3], og.shape[1])]
-    for copy in copies(
+    got = copies(
         (
-            (pick_h, pick), (there, og), (w_h, w),
+            (ids_h, ids), (there, og), (w_h, w),
             (gated_h, gated), (weight_h, weight), (tail_h, tail),
         ),
         sems,
-    ):
+    )
+    got[0].wait()
+    position = positions(ids[...], experts)[2]
+    pick[...] = one_hot(position, 0.0, pick.shape[0] // experts).reshape(pick.shape).astype(BF16)
+    for copy in got[1:]:
         copy.wait()
 
 
@@ -283,12 +292,8 @@
     pieces = mid.shape[0]
     ys = pieces // 2
     full = jnp.concatenate([mid[(b % ys) * 2 + b // ys] for b in range(pieces)], axis=1)
-    dests, rows = out.shape[0], full.shape[1] // out.shape[0]
-    grad = tn(full, gated[...]).astype(BF16)
-    for d in range(dests):
-        out[d, 0:rows, :] = grad[d * rows : (d + 1) * rows]
-    head, rest = pl.ds(0, rows), pl.ds(rows, out.shape[1] - rows)
-    sent = copies(((out.at[:, head], out_h.at[:, head]),), sems.at[pl.ds(0, 1)])
+    dests = out.shape[0]
+    rows = full.shape[1] // dests
     act = nn(full, w[...])
     act_o[...] = act
     total = jnp.sum(weight[...] * act, axis=0, keepdims=True)
@@ -297,9 +302,16 @@
     for k, v in enumerate(split3(total)):
         extra = jnp.where(line == k, jnp.broadcast_to(v, extra.shape), extra)
     extra = extra.astype(BF16)
-    for d in range(dests):
-        out[d, rows:, :] = extra
-    sent += copies(((out.at[:, rest], out_h.at[:, rest]),), sems.at[pl.ds(1, 1)])
+    sent, steps = [], 4
+    each = dests // steps
+    for k in range(steps):
+        first = k * each
+        grad = tn(full[:, first * rows : (first + each) * rows], gated[...]).astype(BF16)
+        for d in range(each):
+            out[first + d, 0:rows, :] = grad[d * rows : (d + 1) * rows]
+            out[first + d, rows:, :] = extra
+        part = pl.ds(first, each)
+        sent += copies(((out.at[part], out_h.at[part]),), sems.at[pl.ds(k, 1)])
     for copy in sent:
         copy.wait()
 
@@ -363,18 +375,16 @@
     cols = width // 2
     small = pltpu.VMEM((2, tokens), jnp.int32), pltpu.VMEM((2, tokens), F32)
     block = pltpu.VMEM((tokens, cols), BF16)
-    send, pick = call(
+    send = call(
         functools.partial(dispatch_body, n_sp, cap),
-        [shape((n_sp * half, width), BF16), shape((n_sp * cap, tokens), BF16)],
+        [shape((n_sp * half, width), BF16)],
         place, route_ids.T, route_weights.T, mixer_out, out_grad,
-        specs=(0, 1, 2, 3), outs_in=(0, 1),
+        specs=(0, 1, 2, 3), outs_in=(0,),
         scratch=[
             *small, block, block,
-            pltpu.VMEM((n_sp * half, width), BF16),
-            pltpu.VMEM((n_sp * cap, tokens), BF16),
-            pltpu.SemaphoreType.DMA((9,)),
+            pltpu.VMEM((n_sp * half, width), BF16), pltpu.SemaphoreType.DMA((8,)),
         ],
-    )
+    )[0]
     own = lax.all_to_all(send.reshape(n_sp, half, width), SP, 0, 0, tiled=True)
     own = own.reshape(n_sp * half, width)
 
@@ -432,13 +442,14 @@
         ],
     )
     pick, og, w_p, gated, weight, tails = call(
-        fetch_body,
+        functools.partial(fetch_body, n_sp),
         [
-            shape(pick.shape, BF16), shape((tokens, ch), BF16), shape(w_proj.shape, BF16),
+            shape((n_sp * cap, tokens), BF16), shape((tokens, ch), BF16),
+            shape(w_proj.shape, BF16),
             shape(gated.shape, BF16), shape(weight.shape, F32), shape(tails.shape, F32),
         ],
-        place, pick, out_grad, w_proj, gated, weight, tails,
-        specs=tuple(range(6)), scratch=[pltpu.SemaphoreType.DMA((6,))],
+        place, route_ids.T, out_grad, w_proj, gated, weight, tails,
+        specs=tuple(range(6)), scratch=[small[0], pltpu.SemaphoreType.DMA((6,))],
     )
     back_lo = lax.ppermute(ga, Y, ring(-1))
     back_hi = lax.ppermute(gb, Y, ring(1))
@@ -462,7 +473,7 @@
         place, mid, gated, w_p, weight, tails,
         outs_in=(0,),
         scratch=[
-            pltpu.VMEM((n_sp, rows + tail, ch), BF16), pltpu.SemaphoreType.DMA((2,)),
+            pltpu.VMEM((n_sp, rows + tail, ch), BF16), pltpu.SemaphoreType.DMA((4,)),
         ],
     )
     branch, loc, prod = call(

time: 181 us -> 181 us (level)
  no operation moved by 1% of the time
where the time goes in v8:
time: 181 us; the launch traced here: 180 us
  blocking collectives  63.7 us (35%)
  waiting for transfers between devices  47.4 us (26%)
  starting transfers between devices  40.2 us (22%)
  Pallas kernels  21 us (12%)
  local copies, waits for them, and re-layouts  4.35 us (2%)
  other arithmetic  2.38 us (1%)
    all_to_all x1, blocking collectives, local(): own = lax.all_to_all(send.reshape(n_sp, half, width), SP, 0, 0, tiled=True)  41.2 us
    all_gather x1, blocking collectives, local(): mid = lax.all_gather(mid, TP)  22.5 us
    pallas_call x12, Pallas kernels, call(): pl.pallas_call(body, grid_spec=pltpu.PrefetchScalarGridSpec(num_scalar_pr...  20.9 us
    ppermute x1, waiting for transfers between devices, local(): wa = lax.ppermute(w_lo, Y, ring(1))  16 us
    all_to_all x1, waiting for transfers between devices, local(): got = lax.all_to_all(out, SP, 0, 0, tiled=True)  14.4 us
    all_to_all x1, waiting for transfers between devices, local(): parts = lax.all_to_all(psum, Y, 0, 0, tiled=True)  12.2 us
    all_to_all x1, starting transfers between devices, local(): got = lax.all_to_all(out, SP, 0, 0, tiled=True)  9.51 us
    all_to_all x1, starting transfers between devices, local(): parts = lax.all_to_all(psum, Y, 0, 0, tiled=True)  7.75 us
  transfers between devices with their start and end apart: 10, of which 6 were waited for; matrix products, arithmetic and copies ran while one was open for 2% of the time, Pallas kernels for 8%

profile of v8, /device:TPU:8, one launch (start us, length us, event | category | flops | bytes accessed | tf_op | source)
XLA Modules:
  0.0 180.0 jit_solution(1059292071784909368)
XLA Ops:
  0.6 0.0 copy-start
  0.6 0.0 copy-start.1
  0.7 0.0 copy-start.2
  0.7 0.1 pad_add_fusion.place
  0.8 3.0 %shard_map.162 = bf16[256,2048]{1,0:T(8,128)(2,1)} custom-call(s32[4]{0:T(128)S(1)} %pad_add_fusion.place, s32[2,128]{1,0:T(2,128)} %bitcast.31, f32[2,128]{1,0:T(2,128)} %bitcast.33, bf16[128,2048]{1,0:T(8,128)(2,1)} %x_h.1, bf16[128,2048]{1,0:T(8,128)(2,1)} %og_h.3), custom_call_target="tpu_custom_call" | custom-call | tf_op jit(solution)/shard_map/pallas_call | solution.py:71
  3.7 41.2 %all_to_all.20 = bf16[32,8,2048]{2,1,0:T(8,128)(2,1)S(1)} all-to-all(bf16[32,8,2048]{2,1,0:T(8,128)(2,1)} %bitcast.30), channel_id=1, replica_groups=mesh['z'=8,'x'=4,'yh'=4,'yl'=2,'c'=2] {'z','x'}, dimensions={0} | all-to-all | bytes 2097152 | tf_op jit(solution)/shard_map/all_to_all | solution.py:388
  44.9 1.9 %collective-permute-start = (bf16[256,2048]{1,0:T(8,128)(2,1)S(1)}, bf16[256,2048]{1,0:T(8,128)(2,1)S(1)}, u32[]{:S(2)}, u32[]{:S(2)}) collective-permute-start(bf16[256,2048]{1,0:T(8,128)(2,1)S(1)} %bitcast.19), channel_id=1, source_target_pairs={{0,1},{1,0},{2,3},{3,2},{4,5},{5,4},{6,7},{7,6},{8,9},{9,8},{10,11... | collective-permute-start | bytes 3145736 | tf_op jit(solution)/shard_map/ppermute | solution.py:402
  46.9 0.0 copy-done
  46.9 0.0 copy-done.1
  46.9 0.0 copy-done.2
  46.9 0.2 shard_map.163
  47.1 3.5 %collective-permute-start.1 = (bf16[192,2048]{1,0:T(8,128)(2,1)S(1)}, bf16[192,2048]{1,0:T(8,128)(2,1)S(1)}, u32[]{:S(2)}, u32[]{:S(2)}) collective-permute-start(bf16[192,2048]{1,0:T(8,128)(2,1)S(1)} %get-tuple-element.35), channel_id=1, source_target_pairs={{0,2},{2,4},{4,6},{6,8},{8,10},{10,12},{12,14},{14,0},{1,3},{3,5},... | collective-permute-start | bytes 2359304 | tf_op jit(solution)/shard_map/ppermute | solution.py:400
  50.6 2.4 %collective-permute-start.2 = (bf16[192,2048]{1,0:T(8,128)(2,1)S(1)}, bf16[192,2048]{1,0:T(8,128)(2,1)S(1)}, u32[]{:S(2)}, u32[]{:S(2)}) collective-permute-start(bf16[192,2048]{1,0:T(8,128)(2,1)S(1)} %get-tuple-element.36), channel_id=1, source_target_pairs={{0,14},{2,0},{4,2},{6,4},{8,6},{10,8},{12,10},{14,12},{1,15},{3,1}... | collective-permute-start | bytes 2359304 | tf_op jit(solution)/shard_map/ppermute | solution.py:401
  52.9 16.0 %collective-permute-done.1.wa = bf16[192,2048]{1,0:T(8,128)(2,1)S(1)} collective-permute-done((bf16[192,2048]{1,0:T(8,128)(2,1)S(1)}, bf16[192,2048]{1,0:T(8,128)(2,1)S(1)}, u32[]{:S(2)}, u32[]{:S(2)}) %collective-permute-start.1) | collective-permute-done | bytes 786464 | tf_op jit(solution)/shard_map/ppermute | solution.py:400
  68.9 3.2 %collective-permute-done.2.wb = bf16[192,2048]{1,0:T(8,128)(2,1)S(1)} collective-permute-done((bf16[192,2048]{1,0:T(8,128)(2,1)S(1)}, bf16[192,2048]{1,0:T(8,128)(2,1)S(1)}, u32[]{:S(2)}, u32[]{:S(2)}) %collective-permute-start.2) | collective-permute-done | bytes 786464 | tf_op jit(solution)/shard_map/ppermute | solution.py:401
  72.1 2.9 %shard_map.164 = (f32[3,256,256]{2,1,0:T(8,128)S(1)}, bf16[3,256,1024]{2,1,0:T(8,128)(2,1)S(1)}, bf16[3,256,1024]{2,1,0:T(8,128)(2,1)S(1)}) custom-call(s32[4]{0:T(128)S(1)} %pad_add_fusion.place, bf16[256,2048]{1,0:T(8,128)(2,1)S(1)} %bitcast.20, bf16[128,2048]{1,0:T(8,128)(2,1)} %bitcast.22, bf16[128,2048]{1,0:T(8,128)(2,1)} %bitcast.24, ...), custom_call_target="tpu_custom_call" | custom-call | tf_op jit(solution)/shard_map/pallas_call | solution.py:71
  75.1 0.0 collective-permute-done.par
  75.1 2.2 %shard_map.165 = (bf16[8,256,128]{2,1,0:T(8,128)(2,1)S(1)}, bf16[256,512]{1,0:T(8,128)(2,1)S(1)}, bf16[256,768]{1,0:T(8,128)(2,1)}) custom-call(s32[4]{0:T(128)S(1)} %pad_add_fusion.place, bf16[256,2048]{1,0:T(8,128)(2,1)S(1)} %collective-permute-done.par, f32[3,256,256]{2,1,0:T(8,128)S(1)} %get-tuple-element.37.part, ...), custom_call_target="tpu_custom_call" | custom-call | tf_op jit(solution)/shard_map/pallas_call | solution.py:71
  77.3 0.0 copy-start.4
  77.3 2.1 %collective-permute-start.5 = (bf16[8,256,128]{2,1,0:T(8,128)(2,1)S(1)}, bf16[8,256,128]{2,1,0:T(8,128)(2,1)S(1)}, u32[]{:S(2)}, u32[]{:S(2)}) collective-permute-start(bf16[8,256,128]{2,1,0:T(8,128)(2,1)S(1)} %get-tuple-element.49), channel_id=1, source_target_pairs={{0,1},{1,0},{2,3},{3,2},{4,5},{5,4},{6,7},{7,6},{8,9},{9,8},{10,11... | collective-permute-start | bytes 1572872 | tf_op jit(solution)/shard_map/ppermute | solution.py:433
  79.4 1.0 shard_map.169
  80.4 0.0 copy-start.3
  80.4 0.0 copy-start.5
  80.4 0.0 copy-start.6
  80.4 0.9 collective-permute-done.5
  81.2 0.9 add_convert_fusion
  82.1 7.7 %all-to-all-start.1 = ((bf16[8,256,128]{2,1,0:T(8,128)(2,1)}), bf16[8,256,128]{2,1,0:T(8,128)(2,1)S(1)}, u32[]{:S(2)}, u32[]{:S(2)}) async-start(bf16[8,256,128]{2,1,0:T(8,128)(2,1)} %add_convert_fusion), calls=%async_computation.1 | async-start | bytes 1048576 | tf_op jit(solution)/shard_map/all_to_all | solution.py:458
  89.9 0.0 copy-done.4
  89.9 3.2 %shard_map.166 = (f32[384,2048]{1,0:T(8,128)}, bf16[192,2048]{1,0:T(8,128)(2,1)}, bf16[192,2048]{1,0:T(8,128)(2,1)}) custom-call(s32[4]{0:T(128)S(1)} %pad_add_fusion.place, bf16[256,2048]{1,0:T(8,128)(2,1)S(1)} %bitcast.21, bf16[256,2048]{1,0:T(8,128)(2,1)S(1)} %collective-permute-done.par, bf16[256,768]{1,0:T(8,128)(2,1)S(1)} %copy-done.4), custom_call_target="tpu_custom_call" | custom-call | tf_op jit(solution)/shard_map/pallas_call | solution.py:71
  93.1 1.9 %collective-permute-start.3 = (bf16[192,2048]{1,0:T(8,128)(2,1)}, bf16[192,2048]{1,0:T(8,128)(2,1)}, u32[]{:S(2)}, u32[]{:S(2)}) collective-permute-start(bf16[192,2048]{1,0:T(8,128)(2,1)} %get-tuple-element.41), channel_id=1, source_target_pairs={{0,14},{2,0},{4,2},{6,4},{8,6},{10,8},{12,10},{14,12},{1,15},{3,1}... | collective-permute-start | bytes 2359304 | tf_op jit(solution)/shard_map/ppermute | solution.py:454
  95.0 12.2 %all-to-all-done.1.parts = bf16[8,256,128]{2,1,0:T(8,128)(2,1)S(1)} async-done(((bf16[8,256,128]{2,1,0:T(8,128)(2,1)}), bf16[8,256,128]{2,1,0:T(8,128)(2,1)S(1)}, u32[]{:S(2)}, u32[]{:S(2)}) %all-to-all-start.1) | async-done | bytes 524320 | tf_op jit(solution)/shard_map/all_to_all | solution.py:458
  107.2 1.3 shard_map.170
  108.5 5.6 %all-to-all-start.2 = ((bf16[32,16,128]{2,1,0:T(8,128)(2,1)}), bf16[32,16,128]{2,1,0:T(8,128)(2,1)S(1)}, u32[]{:S(2)}, u32[]{:S(2)}) async-start(bf16[32,16,128]{2,1,0:T(8,128)(2,1)} %shard_map.170), calls=%async_computation.2 | async-start | bytes 262144 | tf_op jit(solution)/shard_map/all_to_all | solution.py:460
  114.1 1.9 %collective-permute-start.4 = (bf16[192,2048]{1,0:T(8,128)(2,1)}, bf16[192,2048]{1,0:T(8,128)(2,1)}, u32[]{:S(2)}, u32[]{:S(2)}) collective-permute-start(bf16[192,2048]{1,0:T(8,128)(2,1)} %get-tuple-element.42), channel_id=1, source_target_pairs={{0,2},{2,4},{4,6},{6,8},{8,10},{10,12},{12,14},{14,0},{1,3},{3,5},... | collective-permute-start | bytes 2359304 | tf_op jit(solution)/shard_map/ppermute | solution.py:455
  116.0 0.0 copy-done.3
  116.0 3.7 %collective-permute-start.6 = (f32[1,128]{1,0:T(1,128)S(1)}, f32[1,128]{1,0:T(1,128)S(1)}, u32[]{:S(2)}, u32[]{:S(2)}) collective-permute-start(f32[1,128]{1,0:T(1,128)S(1)} %slice.39), channel_id=1, source_target_pairs={{0,16},{16,32},{32,48},{48,64},{64,80},{80,96},{96,112},{112,128},... | collective-permute-start | bytes 1544 | tf_op jit(solution)/shard_map/ppermute | solution.py:406
  119.7 0.0 copy-done.5
  119.8 0.0 copy-done.6
  119.8 0.6 shard_map.167
  120.4 0.0 copy-start.7
  120.4 0.6 copy-done.7
  121.0 0.0 copy-start.8
  121.0 0.6 copy-done.8
  121.6 0.0 copy-start.9
  121.6 0.6 copy-done.9
  122.2 1.7 shard_map.168
  123.9 0.7 all-to-all-done.2
  124.6 0.8 shard_map.171
  125.4 22.5 %all-gather = bf16[2048,128]{1,0:T(8,128)(2,1)S(1)} all-gather(bf16[128,128]{1,0:T(8,128)(2,1)S(1)} %shard_map.171), channel_id=2, replica_groups=mesh['z'=8,'x'=4,'yh'=4,'yl'=2,'c'=2] {'yh','yl','c'}, dimensions={0}, use_global_device_ids=true | all-gather | bytes 557056 | tf_op jit(solution)/shard_map/all_gather | solution.py:466
  147.9 1.8 shard_map.172
  149.6 9.5 %all-to-all-start.3 = ((bf16[32,72,128]{2,1,0:T(8,128)(2,1)}), bf16[32,72,128]{2,1,0:T(8,128)(2,1)S(1)}, u32[]{:S(2)}, u32[]{:S(2)}) async-start(bf16[32,72,128]{2,1,0:T(8,128)(2,1)} %get-tuple-element.55), calls=%async_computation.3 | async-start | bytes 1179648 | tf_op jit(solution)/shard_map/all_to_all | solution.py:483
  159.2 0.0 copy-start.10
  159.2 0.0 collective-permute-done.3
  159.2 1.3 fusion.3
  160.5 0.0 collective-permute-done.4
  160.5 1.2 fusion.4
  161.7 0.0 copy-done.10
  161.7 1.4 fusion.2
  163.1 1.2 shard_map.173
  164.3 0.0 collective-permute-done.6.before
  164.3 14.4 %all-to-all-done.3.got = bf16[32,72,128]{2,1,0:T(8,128)(2,1)S(1)} async-done(((bf16[32,72,128]{2,1,0:T(8,128)(2,1)}), bf16[32,72,128]{2,1,0:T(8,128)(2,1)S(1)}, u32[]{:S(2)}, u32[]{:S(2)}) %all-to-all-start.3) | async-done | bytes 589856 | tf_op jit(solution)/shard_map/all_to_all | solution.py:483
  178.6 1.3 shard_map.174
  (1 shorter events, 0.0 us)
Async XLA Ops:
  0.6 46.2 %copy-start = (bf16[1,128,2048]{2,1,0:T(8,128)(2,1)S(1)}, bf16[1,128,2048]{2,1,0:T(8,128)(2,1)}, u32[]{:S(2)}) copy-start(bf16[1,128,2048]{2,1,0:T(8,128)(2,1)} %param.19) | copy-start | bytes 1572868
  0.6 46.2 %copy-start.1 = (bf16[1,128,2048]{2,1,0:T(8,128)(2,1)S(1)}, bf16[1,128,2048]{2,1,0:T(8,128)(2,1)}, u32[]{:S(2)}) copy-start(bf16[1,128,2048]{2,1,0:T(8,128)(2,1)} %param.20) | copy-start | bytes 1572868
  0.7 46.2 %copy-start.2 = (bf16[1,128,2048]{2,1,0:T(8,128)(2,1)S(1)}, bf16[1,128,2048]{2,1,0:T(8,128)(2,1)}, u32[]{:S(2)}) copy-start(bf16[1,128,2048]{2,1,0:T(8,128)(2,1)} %param.21) | copy-start | bytes 1572868
  44.9 30.1 %collective-permute-start = (bf16[256,2048]{1,0:T(8,128)(2,1)S(1)}, bf16[256,2048]{1,0:T(8,128)(2,1)S(1)}, u32[]{:S(2)}, u32[]{:S(2)}) collective-permute-start(bf16[256,2048]{1,0:T(8,128)(2,1)S(1)} %bitcast.19), channel_id=1, source_target_pairs={{0,1},{1,0},{2,3},{3,2},{4,5},{5,4},{6,7},{7,6},{8,9},{9,8},{10,11... | collective-permute-start | bytes 3145736 | tf_op jit(solution)/shard_map/ppermute | solution.py:402
  47.1 21.8 %collective-permute-start.1 = (bf16[192,2048]{1,0:T(8,128)(2,1)S(1)}, bf16[192,2048]{1,0:T(8,128)(2,1)S(1)}, u32[]{:S(2)}, u32[]{:S(2)}) collective-permute-start(bf16[192,2048]{1,0:T(8,128)(2,1)S(1)} %get-tuple-element.35), channel_id=1, source_target_pairs={{0,2},{2,4},{4,6},{6,8},{8,10},{10,12},{12,14},{14,0},{1,3},{3,5},... | collective-permute-start | bytes 2359304 | tf_op jit(solution)/shard_map/ppermute | solution.py:400
  50.6 21.6 %collective-permute-start.2 = (bf16[192,2048]{1,0:T(8,128)(2,1)S(1)}, bf16[192,2048]{1,0:T(8,128)(2,1)S(1)}, u32[]{:S(2)}, u32[]{:S(2)}) collective-permute-start(bf16[192,2048]{1,0:T(8,128)(2,1)S(1)} %get-tuple-element.36), channel_id=1, source_target_pairs={{0,14},{2,0},{4,2},{6,4},{8,6},{10,8},{12,10},{14,12},{1,15},{3,1}... | collective-permute-start | bytes 2359304 | tf_op jit(solution)/shard_map/ppermute | solution.py:401
  77.3 12.6 %copy-start.4 = (bf16[256,768]{1,0:T(8,128)(2,1)S(1)}, bf16[256,768]{1,0:T(8,128)(2,1)}, u32[]{:S(2)}) copy-start(bf16[256,768]{1,0:T(8,128)(2,1)} %get-tuple-element.39.mix) | copy-start | bytes 1179652
  77.3 3.9 %collective-permute-start.5 = (bf16[8,256,128]{2,1,0:T(8,128)(2,1)S(1)}, bf16[8,256,128]{2,1,0:T(8,128)(2,1)S(1)}, u32[]{:S(2)}, u32[]{:S(2)}) collective-permute-start(bf16[8,256,128]{2,1,0:T(8,128)(2,1)S(1)} %get-tuple-element.49), channel_id=1, source_target_pairs={{0,1},{1,0},{2,3},{3,2},{4,5},{5,4},{6,7},{7,6},{8,9},{9,8},{10,11... | collective-permute-start | bytes 1572872 | tf_op jit(solution)/shard_map/ppermute | solution.py:433
  80.4 35.7 %copy-start.3 = (f32[128,128]{1,0:T(8,128)S(1)}, f32[128,128]{1,0:T(8,128)}, u32[]{:S(2)}) copy-start(f32[128,128]{1,0:T(8,128)} %states.5) | copy-start | bytes 196612
  80.4 39.4 %copy-start.5 = (f32[128,128]{1,0:T(8,128)S(1)}, f32[128,128]{1,0:T(8,128)}, u32[]{:S(2)}) copy-start(f32[128,128]{1,0:T(8,128)} %decay.3) | copy-start | bytes 196612
  80.4 39.4 %copy-start.6 = (bf16[128,128]{1,0:T(8,128)(2,1)S(1)}, bf16[128,128]{1,0:T(8,128)(2,1)}, u32[]{:S(2)}) copy-start(bf16[128,128]{1,0:T(8,128)(2,1)} %gate.3) | copy-start | bytes 98308
  82.1 25.1 %all-to-all-start.1 = ((bf16[8,256,128]{2,1,0:T(8,128)(2,1)}), bf16[8,256,128]{2,1,0:T(8,128)(2,1)S(1)}, u32[]{:S(2)}, u32[]{:S(2)}) async-start(bf16[8,256,128]{2,1,0:T(8,128)(2,1)} %add_convert_fusion), calls=%async_computation.1 | async-start | bytes 1048576 | tf_op jit(solution)/shard_map/all_to_all | solution.py:458
  93.1 66.1 %collective-permute-start.3 = (bf16[192,2048]{1,0:T(8,128)(2,1)}, bf16[192,2048]{1,0:T(8,128)(2,1)}, u32[]{:S(2)}, u32[]{:S(2)}) collective-permute-start(bf16[192,2048]{1,0:T(8,128)(2,1)} %get-tuple-element.41), channel_id=1, source_target_pairs={{0,14},{2,0},{4,2},{6,4},{8,6},{10,8},{12,10},{14,12},{1,15},{3,1}... | collective-permute-start | bytes 2359304 | tf_op jit(solution)/shard_map/ppermute | solution.py:454
  108.5 16.1 %all-to-all-start.2 = ((bf16[32,16,128]{2,1,0:T(8,128)(2,1)}), bf16[32,16,128]{2,1,0:T(8,128)(2,1)S(1)}, u32[]{:S(2)}, u32[]{:S(2)}) async-start(bf16[32,16,128]{2,1,0:T(8,128)(2,1)} %shard_map.170), calls=%async_computation.2 | async-start | bytes 262144 | tf_op jit(solution)/shard_map/all_to_all | solution.py:460
  114.1 46.4 %collective-permute-start.4 = (bf16[192,2048]{1,0:T(8,128)(2,1)}, bf16[192,2048]{1,0:T(8,128)(2,1)}, u32[]{:S(2)}, u32[]{:S(2)}) collective-permute-start(bf16[192,2048]{1,0:T(8,128)(2,1)} %get-tuple-element.42), channel_id=1, source_target_pairs={{0,2},{2,4},{4,6},{6,8},{8,10},{10,12},{12,14},{14,0},{1,3},{3,5},... | collective-permute-start | bytes 2359304 | tf_op jit(solution)/shard_map/ppermute | solution.py:455
  116.0 48.2 %collective-permute-start.6 = (f32[1,128]{1,0:T(1,128)S(1)}, f32[1,128]{1,0:T(1,128)S(1)}, u32[]{:S(2)}, u32[]{:S(2)}) collective-permute-start(f32[1,128]{1,0:T(1,128)S(1)} %slice.39), channel_id=1, source_target_pairs={{0,16},{16,32},{32,48},{48,64},{64,80},{80,96},{96,112},{112,128},... | collective-permute-start | bytes 1544 | tf_op jit(solution)/shard_map/ppermute | solution.py:406
  120.4 0.6 copy-start.7
  121.0 0.6 copy-start.8
  121.6 0.6 copy-start.9
  149.6 29.0 %all-to-all-start.3 = ((bf16[32,72,128]{2,1,0:T(8,128)(2,1)}), bf16[32,72,128]{2,1,0:T(8,128)(2,1)S(1)}, u32[]{:S(2)}, u32[]{:S(2)}) async-start(bf16[32,72,128]{2,1,0:T(8,128)(2,1)} %get-tuple-element.55), calls=%async_computation.3 | async-start | bytes 1179648 | tf_op jit(solution)/shard_map/all_to_all | solution.py:483
  159.2 2.5 %copy-start.10 = (f32[384,2048]{1,0:T(8,128)S(1)}, f32[384,2048]{1,0:T(8,128)}, u32[]{:S(2)}) copy-start(f32[384,2048]{1,0:T(8,128)} %get-tuple-element.40) | copy-start | bytes 9437188

commit v9 on v7

--- a/solution.py
+++ b/solution.py
@@ -276,20 +276,25 @@
 
 
 def combine_body(place, pick, back, og, mid):
-    mid[...] = (og[...].astype(F32) + tn(pick[...], back[...])).astype(BF16)
-
-
-def project_body(place, mid, gated, w, weight, tail, out_h, act_o, out, sems):
-    pieces = mid.shape[0]
-    ys = pieces // 2
-    full = jnp.concatenate([mid[(b % ys) * 2 + b // ys] for b in range(pieces)], axis=1)
-    dests, rows = out.shape[0], full.shape[1] // out.shape[0]
-    grad = tn(full, gated[...]).astype(BF16)
-    for d in range(dests):
-        out[d, 0:rows, :] = grad[d * rows : (d + 1) * rows]
-    head, rest = pl.ds(0, rows), pl.ds(rows, out.shape[1] - rows)
-    sent = copies(((out.at[:, head], out_h.at[:, head]),), sems.at[pl.ds(0, 1)])
-    act = nn(full, w[...])
+    block = (og[...].astype(F32) + tn(pick[...], back[...])).astype(BF16)
+    for k in range(mid.shape[0]):
+        mid[k] = block
+
+
+def half_body(place, mid, gated, w, grad, act):
+    full = jnp.concatenate([mid[k] for k in range(mid.shape[0])], axis=1)
+    grad[...] = tn(full, gated[...]).astype(BF16)
+    act[...] = nn(full, w[columns(place[0], full.shape[1]), :])
+
+
+def project_body(
+    place, mid, grad_mine, act_mine, gated, w, weight, tail, out_h, act_o, out, sems
+):
+    c = place[0]
+    full = jnp.concatenate([mid[k] for k in range(mid.shape[0])], axis=1)
+    each = out.shape[0] // 2
+    rows = full.shape[1] // each
+    act = act_mine[...] + nn(full, w[columns(1 - c, full.shape[1]), :])
     act_o[...] = act
     total = jnp.sum(weight[...] * act, axis=0, keepdims=True)
     extra = tail[...]
@@ -297,9 +302,15 @@
     for k, v in enumerate(split3(total)):
         extra = jnp.where(line == k, jnp.broadcast_to(v, extra.shape), extra)
     extra = extra.astype(BF16)
-    for d in range(dests):
-        out[d, rows:, :] = extra
-    sent += copies(((out.at[:, rest], out_h.at[:, rest]),), sems.at[pl.ds(1, 1)])
+    sent = []
+    for k, core in enumerate((c, 1 - c)):
+        grad = grad_mine[...] if k == 0 else tn(full, gated[...]).astype(BF16)
+        first = core * each
+        for d in range(each):
+            out[first + d, 0:rows, :] = grad[d * rows : (d + 1) * rows]
+            out[first + d, rows:, :] = extra
+        part = pl.ds(first, each)
+        sent += copies(((out.at[part], out_h.at[part]),), sems.at[pl.ds(k, 1)])
     for copy in sent:
         copy.wait()
 
@@ -449,17 +460,21 @@
     back = lax.all_to_all(ret, SP, 0, 0, tiled=True)
     mid = call(
         combine_body,
-        shape((tokens, ch), BF16),
+        shape((n_y, tokens, ch), BF16),
         place, pick, back.reshape(n_sp * cap, wide), og,
     )
-    mid = lax.all_gather(mid, TP)
+    mid = lax.all_to_all(mid, Y, 0, 0, tiled=True)
+    mid_other = lax.ppermute(mid, "c", swap)
 
     rows = width // n_sp
     row = lambda t: shape((tokens, ch), t)
+    grad_half, act_half = call(
+        half_body, [shape((cols, ch), BF16), row(F32)], place, mid, gated, w_p,
+    )
     out, act = call(
         project_body,
         [shape((n_sp, rows + tail, ch), BF16), row(F32)],
-        place, mid, gated, w_p, weight, tails,
+        place, mid_other, grad_half, act_half, gated, w_p, weight, tails,
         outs_in=(0,),
         scratch=[
             pltpu.VMEM((n_sp, rows + tail, ch), BF16), pltpu.SemaphoreType.DMA((2,)),

time: 181 us -> 181 us (level)
  waiting for transfers between devices: 47.3 us -> 44.5 us
    all_to_all x0 -> x1, blocking collectives: none -> 23.9 us  [local(): parts = lax.all_to_all(psum, Y, 0, 0, tiled=True)]
    all_gather x1 -> x0, blocking collectives: 22.5 us -> none  [local(): mid = lax.all_gather(mid, TP)]
    all_to_all x1, starting transfers between devices: 7.76 us -> 4.6 us  [local(): mid = lax.all_to_all(mid, Y, 0, 0, tiled=True)]
    all_to_all x1, waiting for transfers between devices: 12.2 us -> 9.77 us  [local(): mid = lax.all_to_all(mid, Y, 0, 0, tiled=True)]
    ppermute x0 -> x1, starting transfers between devices: none -> 1.91 us  [local(): mid_other = lax.ppermute(mid, 'c', swap)]
    pallas_call x12 -> x13, Pallas kernels: 21 us -> 22.4 us  [call(): pl.pallas_call(body, grid_spec=pltpu.PrefetchScalarGridSpec(num_scalar_pr...]
  transfers between devices with their start and end apart: 10 -> 11, of which waited for: 6 -> 5; matrix products, arithmetic and copies ran while one was open for 2% -> 2% of each run, Pallas kernels for 8% -> 8%
where the time goes in v9:
time: 181 us; the launch traced here: 180 us
  blocking collectives  65.1 us (36%)
  waiting for transfers between devices  44.5 us (25%)
  starting transfers between devices  41.1 us (23%)
  Pallas kernels  22.5 us (12%)
  local copies, waits for them, and re-layouts  3.96 us (2%)
    all_to_all x1, blocking collectives, local(): own = lax.all_to_all(send.reshape(n_sp, half, width), SP, 0, 0, tiled=True)  41.2 us
    all_to_all x1, blocking collectives, local(): parts = lax.all_to_all(psum, Y, 0, 0, tiled=True)  23.9 us
    pallas_call x13, Pallas kernels, call(): pl.pallas_call(body, grid_spec=pltpu.PrefetchScalarGridSpec(num_scalar_pr...  22.4 us
    ppermute x1, waiting for transfers between devices, local(): wa = lax.ppermute(w_lo, Y, ring(1))  16 us
    all_to_all x1, waiting for transfers between devices, local(): got = lax.all_to_all(out, SP, 0, 0, tiled=True)  14.7 us
    all_to_all x1, waiting for transfers between devices, local(): mid = lax.all_to_all(mid, Y, 0, 0, tiled=True)  9.77 us
    all_to_all x1, starting transfers between devices, local(): got = lax.all_to_all(out, SP, 0, 0, tiled=True)  9.18 us
    all_to_all x1, starting transfers between devices, local(): back = lax.all_to_all(ret, SP, 0, 0, tiled=True)  5.55 us
  transfers between devices with their start and end apart: 11, of which 5 were waited for; matrix products, arithmetic and copies ran while one was open for 2% of the time, Pallas kernels for 8%

profile of v9, /device:TPU:8, one launch (start us, length us, event | category | flops | bytes accessed | tf_op | source)
XLA Modules:
  0.0 179.7 jit_solution(3197567334800551120)
XLA Ops:
  0.6 0.0 copy-start
  0.6 0.0 copy-start.1
  0.7 0.0 copy-start.2
  0.7 0.1 pad_add_fusion.place
  0.8 3.0 %shard_map.162 = (bf16[256,2048]{1,0:T(8,128)(2,1)}, bf16[512,128]{1,0:T(8,128)(2,1)}) custom-call(s32[4]{0:T(128)S(1)} %pad_add_fusion.place, s32[2,128]{1,0:T(2,128)} %bitcast.29, f32[2,128]{1,0:T(2,128)} %bitcast.30, bf16[128,2048]{1,0:T(8,128)(2,1)} %x_h.1, bf16[128,2048]{1,0:T(8,128)(2,1)} %og_h.3), custom_call_target="tpu_custom_call" | custom-call | tf_op jit(solution)/shard_map/pallas_call | solution.py:71
  3.7 41.2 %all_to_all.25 = bf16[32,8,2048]{2,1,0:T(8,128)(2,1)S(1)} all-to-all(bf16[32,8,2048]{2,1,0:T(8,128)(2,1)} %bitcast.28), channel_id=1, replica_groups=mesh['z'=8,'x'=4,'yh'=4,'yl'=2,'c'=2] {'z','x'}, dimensions={0} | all-to-all | bytes 2097152 | tf_op jit(solution)/shard_map/all_to_all | solution.py:389
  45.0 1.9 %collective-permute-start = (bf16[256,2048]{1,0:T(8,128)(2,1)S(1)}, bf16[256,2048]{1,0:T(8,128)(2,1)S(1)}, u32[]{:S(2)}, u32[]{:S(2)}) collective-permute-start(bf16[256,2048]{1,0:T(8,128)(2,1)S(1)} %bitcast.18), channel_id=1, source_target_pairs={{0,1},{1,0},{2,3},{3,2},{4,5},{5,4},{6,7},{7,6},{8,9},{9,8},{10,11... | collective-permute-start | bytes 3145736 | tf_op jit(solution)/shard_map/ppermute | solution.py:403
  46.9 0.0 copy-done
  46.9 0.0 copy-done.1
  46.9 0.0 copy-done.2
  46.9 0.2 shard_map.163
  47.1 3.5 %collective-permute-start.1 = (bf16[192,2048]{1,0:T(8,128)(2,1)S(1)}, bf16[192,2048]{1,0:T(8,128)(2,1)S(1)}, u32[]{:S(2)}, u32[]{:S(2)}) collective-permute-start(bf16[192,2048]{1,0:T(8,128)(2,1)S(1)} %get-tuple-element.40), channel_id=1, source_target_pairs={{0,2},{2,4},{4,6},{6,8},{8,10},{10,12},{12,14},{14,0},{1,3},{3,5},... | collective-permute-start | bytes 2359304 | tf_op jit(solution)/shard_map/ppermute | solution.py:401
  50.6 2.4 %collective-permute-start.2 = (bf16[192,2048]{1,0:T(8,128)(2,1)S(1)}, bf16[192,2048]{1,0:T(8,128)(2,1)S(1)}, u32[]{:S(2)}, u32[]{:S(2)}) collective-permute-start(bf16[192,2048]{1,0:T(8,128)(2,1)S(1)} %get-tuple-element.41), channel_id=1, source_target_pairs={{0,14},{2,0},{4,2},{6,4},{8,6},{10,8},{12,10},{14,12},{1,15},{3,1}... | collective-permute-start | bytes 2359304 | tf_op jit(solution)/shard_map/ppermute | solution.py:402
  52.9 16.0 %collective-permute-done.1.wa = bf16[192,2048]{1,0:T(8,128)(2,1)S(1)} collective-permute-done((bf16[192,2048]{1,0:T(8,128)(2,1)S(1)}, bf16[192,2048]{1,0:T(8,128)(2,1)S(1)}, u32[]{:S(2)}, u32[]{:S(2)}) %collective-permute-start.1) | collective-permute-done | bytes 786464 | tf_op jit(solution)/shard_map/ppermute | solution.py:401
  68.9 3.2 %collective-permute-done.2.wb = bf16[192,2048]{1,0:T(8,128)(2,1)S(1)} collective-permute-done((bf16[192,2048]{1,0:T(8,128)(2,1)S(1)}, bf16[192,2048]{1,0:T(8,128)(2,1)S(1)}, u32[]{:S(2)}, u32[]{:S(2)}) %collective-permute-start.2) | collective-permute-done | bytes 786464 | tf_op jit(solution)/shard_map/ppermute | solution.py:402
  72.1 2.9 %shard_map.164 = (f32[3,256,256]{2,1,0:T(8,128)S(1)}, bf16[3,256,1024]{2,1,0:T(8,128)(2,1)S(1)}, bf16[3,256,1024]{2,1,0:T(8,128)(2,1)S(1)}) custom-call(s32[4]{0:T(128)S(1)} %pad_add_fusion.place, bf16[256,2048]{1,0:T(8,128)(2,1)S(1)} %bitcast.19, bf16[128,2048]{1,0:T(8,128)(2,1)} %bitcast.21, bf16[128,2048]{1,0:T(8,128)(2,1)} %bitcast.23, ...), custom_call_target="tpu_custom_call" | custom-call | tf_op jit(solution)/shard_map/pallas_call | solution.py:71
  75.1 0.0 collective-permute-done.par
  75.1 2.2 %shard_map.165 = (bf16[8,256,128]{2,1,0:T(8,128)(2,1)S(1)}, bf16[256,512]{1,0:T(8,128)(2,1)S(1)}, bf16[256,768]{1,0:T(8,128)(2,1)}) custom-call(s32[4]{0:T(128)S(1)} %pad_add_fusion.place, bf16[256,2048]{1,0:T(8,128)(2,1)S(1)} %collective-permute-done.par, f32[3,256,256]{2,1,0:T(8,128)S(1)} %get-tuple-element.42.part, ...), custom_call_target="tpu_custom_call" | custom-call | tf_op jit(solution)/shard_map/pallas_call | solution.py:71
  77.3 1.9 %collective-permute-start.5 = (bf16[8,256,128]{2,1,0:T(8,128)(2,1)S(1)}, bf16[8,256,128]{2,1,0:T(8,128)(2,1)S(1)}, u32[]{:S(2)}, u32[]{:S(2)}) collective-permute-start(bf16[8,256,128]{2,1,0:T(8,128)(2,1)S(1)} %get-tuple-element.55), channel_id=1, source_target_pairs={{0,1},{1,0},{2,3},{3,2},{4,5},{5,4},{6,7},{7,6},{8,9},{9,8},{10,11... | collective-permute-start | bytes 1572872 | tf_op jit(solution)/shard_map/ppermute | solution.py:434
  79.2 0.0 copy-start.4
  79.2 1.0 shard_map.169
  80.2 0.0 copy-start.3
  80.2 0.0 copy-start.5
  80.2 0.0 copy-start.6
  80.3 0.8 collective-permute-done.5
  81.1 0.1 add_convert_fusion
  81.2 23.9 %all_to_all.26.parts = bf16[8,256,128]{2,1,0:T(8,128)(2,1)S(1)} all-to-all(bf16[8,256,128]{2,1,0:T(8,128)(2,1)S(1)} %add_convert_fusion), channel_id=1, replica_groups=mesh['z'=8,'x'=4,'yh'=4,'yl'=2,'c'=2] {'yh','yl'}, dimensions={0} | all-to-all | bytes 1048576 | tf_op jit(solution)/shard_map/all_to_all | solution.py:458
  105.1 1.3 shard_map.170
  106.4 5.6 %all-to-all-start.2 = ((bf16[32,16,128]{2,1,0:T(8,128)(2,1)}), bf16[32,16,128]{2,1,0:T(8,128)(2,1)S(1)}, u32[]{:S(2)}, u32[]{:S(2)}) async-start(bf16[32,16,128]{2,1,0:T(8,128)(2,1)} %shard_map.170), calls=%async_computation.2 | async-start | bytes 262144 | tf_op jit(solution)/shard_map/all_to_all | solution.py:460
  111.9 0.0 copy-done.4
  112.0 3.2 %shard_map.166 = (f32[384,2048]{1,0:T(8,128)}, bf16[192,2048]{1,0:T(8,128)(2,1)}, bf16[192,2048]{1,0:T(8,128)(2,1)}) custom-call(s32[4]{0:T(128)S(1)} %pad_add_fusion.place, bf16[256,2048]{1,0:T(8,128)(2,1)S(1)} %bitcast.20, bf16[256,2048]{1,0:T(8,128)(2,1)S(1)} %collective-permute-done.par, bf16[256,768]{1,0:T(8,128)(2,1)S(1)} %copy-done.4), custom_call_target="tpu_custom_call" | custom-call | tf_op jit(solution)/shard_map/pallas_call | solution.py:71
  115.2 3.4 %collective-permute-start.3 = (bf16[192,2048]{1,0:T(8,128)(2,1)}, bf16[192,2048]{1,0:T(8,128)(2,1)S(1)}, u32[]{:S(2)}, u32[]{:S(2)}) collective-permute-start(bf16[192,2048]{1,0:T(8,128)(2,1)} %get-tuple-element.46), channel_id=1, source_target_pairs={{0,14},{2,0},{4,2},{6,4},{8,6},{10,8},{12,10},{14,12},{1,15},{3,1}... | collective-permute-start | bytes 2359304 | tf_op jit(solution)/shard_map/ppermute | solution.py:454
  118.5 0.0 copy-done.3
  118.6 0.0 copy-done.5
  118.6 0.0 copy-done.6
  118.6 0.6 shard_map.167
  119.2 0.0 copy-start.7
  119.2 0.6 copy-done.7
  119.8 0.6 copy-done.8
  120.4 0.0 copy-start.9
  120.4 0.6 copy-done.9
  121.0 1.7 shard_map.168
  122.7 0.0 all-to-all-done.2
  122.8 1.5 shard_map.171
  124.2 4.6 %all-to-all-start.3 = ((bf16[8,128,128]{2,1,0:T(8,128)(2,1)}), bf16[8,128,128]{2,1,0:T(8,128)(2,1)S(1)}, u32[]{:S(2)}, u32[]{:S(2)}) async-start(bf16[8,128,128]{2,1,0:T(8,128)(2,1)} %shard_map.171), calls=%async_computation.3 | async-start | bytes 524288 | tf_op jit(solution)/shard_map/all_to_all | solution.py:466
  128.8 3.4 %collective-permute-start.4 = (bf16[192,2048]{1,0:T(8,128)(2,1)}, bf16[192,2048]{1,0:T(8,128)(2,1)}, u32[]{:S(2)}, u32[]{:S(2)}) collective-permute-start(bf16[192,2048]{1,0:T(8,128)(2,1)} %get-tuple-element.47), channel_id=1, source_target_pairs={{0,2},{2,4},{4,6},{6,8},{8,10},{10,12},{12,14},{14,0},{1,3},{3,5},... | collective-permute-start | bytes 2359304 | tf_op jit(solution)/shard_map/ppermute | solution.py:455
  132.2 9.8 %all-to-all-done.3.mid = bf16[8,128,128]{2,1,0:T(8,128)(2,1)S(1)} async-done(((bf16[8,128,128]{2,1,0:T(8,128)(2,1)}), bf16[8,128,128]{2,1,0:T(8,128)(2,1)S(1)}, u32[]{:S(2)}, u32[]{:S(2)}) %all-to-all-start.3) | async-done | bytes 262176 | tf_op jit(solution)/shard_map/all_to_all | solution.py:466
  142.0 1.9 %collective-permute-start.6 = (bf16[8,128,128]{2,1,0:T(8,128)(2,1)S(1)}, bf16[8,128,128]{2,1,0:T(8,128)(2,1)S(1)}, u32[]{:S(2)}, u32[]{:S(2)}) collective-permute-start(bf16[8,128,128]{2,1,0:T(8,128)(2,1)S(1)} %all-to-all-done.3.mid), channel_id=1, source_target_pairs={{0,1},{1,0},{2,3},{3,2},{4,5},{5,4},{6,7},{7,6},{8,9},{9,8},{10,11... | collective-permute-start | bytes 786440 | tf_op jit(solution)/shard_map/ppermute | solution.py:467
  143.9 3.4 %collective-permute-start.7 = (f32[1,128]{1,0:T(1,128)S(1)}, f32[1,128]{1,0:T(1,128)S(1)}, u32[]{:S(2)}, u32[]{:S(2)}) collective-permute-start(f32[1,128]{1,0:T(1,128)S(1)} %slice.39), channel_id=1, source_target_pairs={{0,16},{16,32},{32,48},{48,64},{64,80},{80,96},{96,112},{112,128},... | collective-permute-start | bytes 1544 | tf_op jit(solution)/shard_map/ppermute | solution.py:407
  147.3 0.9 shard_map.172
  148.2 0.0 collective-permute-done.6.mid
  148.2 1.6 shard_map.173
  149.8 9.2 %all-to-all-start.4 = ((bf16[32,72,128]{2,1,0:T(8,128)(2,1)}), bf16[32,72,128]{2,1,0:T(8,128)(2,1)S(1)}, u32[]{:S(2)}, u32[]{:S(2)}) async-start(bf16[32,72,128]{2,1,0:T(8,128)(2,1)} %get-tuple-element.63), calls=%async_computation.4 | async-start | bytes 1179648 | tf_op jit(solution)/shard_map/all_to_all | solution.py:487
  159.0 0.0 copy-start.10
  159.0 0.0 collective-permute-done.3
  159.1 0.1 fusion.3
  159.1 0.0 collective-permute-done.4
  159.1 1.3 fusion.4
  160.4 0.7 copy-done.10
  161.2 1.4 fusion.2
  162.5 1.2 shard_map.174
  163.7 0.0 collective-permute-done.7.before
  163.7 14.7 %all-to-all-done.4.got = bf16[32,72,128]{2,1,0:T(8,128)(2,1)S(1)} async-done(((bf16[32,72,128]{2,1,0:T(8,128)(2,1)}), bf16[32,72,128]{2,1,0:T(8,128)(2,1)S(1)}, u32[]{:S(2)}, u32[]{:S(2)}) %all-to-all-start.4) | async-done | bytes 589856 | tf_op jit(solution)/shard_map/all_to_all | solution.py:487
  178.4 1.3 shard_map.175
  (2 shorter events, 0.0 us)
Async XLA Ops:
  0.6 46.2 %copy-start = (bf16[1,128,2048]{2,1,0:T(8,128)(2,1)S(1)}, bf16[1,128,2048]{2,1,0:T(8,128)(2,1)}, u32[]{:S(2)}) copy-start(bf16[1,128,2048]{2,1,0:T(8,128)(2,1)} %param.19) | copy-start | bytes 1572868
  0.6 46.2 %copy-start.1 = (bf16[1,128,2048]{2,1,0:T(8,128)(2,1)S(1)}, bf16[1,128,2048]{2,1,0:T(8,128)(2,1)}, u32[]{:S(2)}) copy-start(bf16[1,128,2048]{2,1,0:T(8,128)(2,1)} %param.20) | copy-start | bytes 1572868
  0.7 46.2 %copy-start.2 = (bf16[1,128,2048]{2,1,0:T(8,128)(2,1)S(1)}, bf16[1,128,2048]{2,1,0:T(8,128)(2,1)}, u32[]{:S(2)}) copy-start(bf16[1,128,2048]{2,1,0:T(8,128)(2,1)} %param.21) | copy-start | bytes 1572868
  45.0 30.1 %collective-permute-start = (bf16[256,2048]{1,0:T(8,128)(2,1)S(1)}, bf16[256,2048]{1,0:T(8,128)(2,1)S(1)}, u32[]{:S(2)}, u32[]{:S(2)}) collective-permute-start(bf16[256,2048]{1,0:T(8,128)(2,1)S(1)} %bitcast.18), channel_id=1, source_target_pairs={{0,1},{1,0},{2,3},{3,2},{4,5},{5,4},{6,7},{7,6},{8,9},{9,8},{10,11... | collective-permute-start | bytes 3145736 | tf_op jit(solution)/shard_map/ppermute | solution.py:403
  47.1 21.8 %collective-permute-start.1 = (bf16[192,2048]{1,0:T(8,128)(2,1)S(1)}, bf16[192,2048]{1,0:T(8,128)(2,1)S(1)}, u32[]{:S(2)}, u32[]{:S(2)}) collective-permute-start(bf16[192,2048]{1,0:T(8,128)(2,1)S(1)} %get-tuple-element.40), channel_id=1, source_target_pairs={{0,2},{2,4},{4,6},{6,8},{8,10},{10,12},{12,14},{14,0},{1,3},{3,5},... | collective-permute-start | bytes 2359304 | tf_op jit(solution)/shard_map/ppermute | solution.py:401
  50.6 21.6 %collective-permute-start.2 = (bf16[192,2048]{1,0:T(8,128)(2,1)S(1)}, bf16[192,2048]{1,0:T(8,128)(2,1)S(1)}, u32[]{:S(2)}, u32[]{:S(2)}) collective-permute-start(bf16[192,2048]{1,0:T(8,128)(2,1)S(1)} %get-tuple-element.41), channel_id=1, source_target_pairs={{0,14},{2,0},{4,2},{6,4},{8,6},{10,8},{12,10},{14,12},{1,15},{3,1}... | collective-permute-start | bytes 2359304 | tf_op jit(solution)/shard_map/ppermute | solution.py:402
  77.3 3.8 %collective-permute-start.5 = (bf16[8,256,128]{2,1,0:T(8,128)(2,1)S(1)}, bf16[8,256,128]{2,1,0:T(8,128)(2,1)S(1)}, u32[]{:S(2)}, u32[]{:S(2)}) collective-permute-start(bf16[8,256,128]{2,1,0:T(8,128)(2,1)S(1)} %get-tuple-element.55), channel_id=1, source_target_pairs={{0,1},{1,0},{2,3},{3,2},{4,5},{5,4},{6,7},{7,6},{8,9},{9,8},{10,11... | collective-permute-start | bytes 1572872 | tf_op jit(solution)/shard_map/ppermute | solution.py:434
  79.2 32.7 %copy-start.4 = (bf16[256,768]{1,0:T(8,128)(2,1)S(1)}, bf16[256,768]{1,0:T(8,128)(2,1)}, u32[]{:S(2)}) copy-start(bf16[256,768]{1,0:T(8,128)(2,1)} %get-tuple-element.44.mix) | copy-start | bytes 1179652
  80.2 38.3 %copy-start.3 = (f32[128,128]{1,0:T(8,128)S(1)}, f32[128,128]{1,0:T(8,128)}, u32[]{:S(2)}) copy-start(f32[128,128]{1,0:T(8,128)} %states.5) | copy-start | bytes 196612
  80.2 38.3 %copy-start.5 = (f32[128,128]{1,0:T(8,128)S(1)}, f32[128,128]{1,0:T(8,128)}, u32[]{:S(2)}) copy-start(f32[128,128]{1,0:T(8,128)} %decay.3) | copy-start | bytes 196612
  80.2 38.3 %copy-start.6 = (bf16[128,128]{1,0:T(8,128)(2,1)S(1)}, bf16[128,128]{1,0:T(8,128)(2,1)}, u32[]{:S(2)}) copy-start(bf16[128,128]{1,0:T(8,128)(2,1)} %gate.3) | copy-start | bytes 98308
  106.4 16.4 %all-to-all-start.2 = ((bf16[32,16,128]{2,1,0:T(8,128)(2,1)}), bf16[32,16,128]{2,1,0:T(8,128)(2,1)S(1)}, u32[]{:S(2)}, u32[]{:S(2)}) async-start(bf16[32,16,128]{2,1,0:T(8,128)(2,1)} %shard_map.170), calls=%async_computation.2 | async-start | bytes 262144 | tf_op jit(solution)/shard_map/all_to_all | solution.py:460
  115.2 43.9 %collective-permute-start.3 = (bf16[192,2048]{1,0:T(8,128)(2,1)}, bf16[192,2048]{1,0:T(8,128)(2,1)S(1)}, u32[]{:S(2)}, u32[]{:S(2)}) collective-permute-start(bf16[192,2048]{1,0:T(8,128)(2,1)} %get-tuple-element.46), channel_id=1, source_target_pairs={{0,14},{2,0},{4,2},{6,4},{8,6},{10,8},{12,10},{14,12},{1,15},{3,1}... | collective-permute-start | bytes 2359304 | tf_op jit(solution)/shard_map/ppermute | solution.py:454
  119.2 0.6 copy-start.7
  119.8 0.6 copy-start.8
  120.4 0.6 copy-start.9
  124.2 17.7 %all-to-all-start.3 = ((bf16[8,128,128]{2,1,0:T(8,128)(2,1)}), bf16[8,128,128]{2,1,0:T(8,128)(2,1)S(1)}, u32[]{:S(2)}, u32[]{:S(2)}) async-start(bf16[8,128,128]{2,1,0:T(8,128)(2,1)} %shard_map.171), calls=%async_computation.3 | async-start | bytes 524288 | tf_op jit(solution)/shard_map/all_to_all | solution.py:466
  128.8 30.3 %collective-permute-start.4 = (bf16[192,2048]{1,0:T(8,128)(2,1)}, bf16[192,2048]{1,0:T(8,128)(2,1)}, u32[]{:S(2)}, u32[]{:S(2)}) collective-permute-start(bf16[192,2048]{1,0:T(8,128)(2,1)} %get-tuple-element.47), channel_id=1, source_target_pairs={{0,2},{2,4},{4,6},{6,8},{8,10},{10,12},{12,14},{14,0},{1,3},{3,5},... | collective-permute-start | bytes 2359304 | tf_op jit(solution)/shard_map/ppermute | solution.py:455
  142.0 6.2 %collective-permute-start.6 = (bf16[8,128,128]{2,1,0:T(8,128)(2,1)S(1)}, bf16[8,128,128]{2,1,0:T(8,128)(2,1)S(1)}, u32[]{:S(2)}, u32[]{:S(2)}) collective-permute-start(bf16[8,128,128]{2,1,0:T(8,128)(2,1)S(1)} %all-to-all-done.3.mid), channel_id=1, source_target_pairs={{0,1},{1,0},{2,3},{3,2},{4,5},{5,4},{6,7},{7,6},{8,9},{9,8},{10,11... | collective-permute-start | bytes 786440 | tf_op jit(solution)/shard_map/ppermute | solution.py:467
  143.9 19.8 %collective-permute-start.7 = (f32[1,128]{1,0:T(1,128)S(1)}, f32[1,128]{1,0:T(1,128)S(1)}, u32[]{:S(2)}, u32[]{:S(2)}) collective-permute-start(f32[1,128]{1,0:T(1,128)S(1)} %slice.39), channel_id=1, source_target_pairs={{0,16},{16,32},{32,48},{48,64},{64,80},{80,96},{96,112},{112,128},... | collective-permute-start | bytes 1544 | tf_op jit(solution)/shard_map/ppermute | solution.py:407
  149.8 28.6 %all-to-all-start.4 = ((bf16[32,72,128]{2,1,0:T(8,128)(2,1)}), bf16[32,72,128]{2,1,0:T(8,128)(2,1)S(1)}, u32[]{:S(2)}, u32[]{:S(2)}) async-start(bf16[32,72,128]{2,1,0:T(8,128)(2,1)} %get-tuple-element.63), calls=%async_computation.4 | async-start | bytes 1179648 | tf_op jit(solution)/shard_map/all_to_all | solution.py:487
  159.0 2.1 %copy-start.10 = (f32[384,2048]{1,0:T(8,128)S(1)}, f32[384,2048]{1,0:T(8,128)}, u32[]{:S(2)}) copy-start(f32[384,2048]{1,0:T(8,128)} %get-tuple-element.45) | copy-start | bytes 9437188
